TPU v7x, 512 devices: a whole 4x4x16 slice. The times are simulated.
512 devices in a mesh: kv: 16 (over y, x), tp: 32 (over z, core).
Axes of the slice: x: 4, y: 4, z: 16, core: 2. Of those that a mesh axis runs over, the one named last changes fastest.
Arguments:
- hidden_in: bfloat16 [64, 4096], P('kv', 'tp'), may hold values from -12 to 12
- mixer_gain: float32 [4096], P('tp'), may hold values from 0.1 to 1.9
- query_weight: bfloat16 [4096, 4096], P('tp', 'kv'), may hold values from -0.09375 to 0.09375
- key_weight: bfloat16 [4096, 4096], P('tp', 'kv'), may hold values from -0.09375 to 0.09375
- value_weight: bfloat16 [4096, 8192], P('tp', 'kv'), may hold values from -0.09375 to 0.09375
- gate_weight: bfloat16 [4096, 8192], P('tp', 'kv'), may hold values from -0.09375 to 0.09375
- decay_rate: float32 [16], P('kv'), may hold values from 0.0005 to 0.15
- prior_state: float32 [64, 16, 256, 512], P('tp', 'kv'), may hold values from -2.5 to 2.5
- key_block: bfloat16 [64, 16, 128, 256], P('tp', 'kv'), may hold values from -1 to 1
- value_block: bfloat16 [64, 16, 128, 512], P('tp', 'kv'), may hold values from -6 to 6
- lengths: int32 [64], P('tp'), may hold values from 1 to 16384, 262144 in all
- group_gain: float32 [8192], P('kv'), may hold values from 0.1 to 1.9
- output_weight: bfloat16 [8192, 4096], P('kv', 'tp'), may hold values from -0.0625 to 0.0625
- channel_gain: float32 [4096], P('tp'), may hold values from 0.1 to 1.9
- hidden_gate: bfloat16 [4096, 11264], P('tp', 'kv'), may hold values from -0.09375 to 0.09375
- hidden_up: bfloat16 [4096, 11264], P('tp', 'kv'), may hold values from -0.09375 to 0.09375
- hidden_down: bfloat16 [11264, 4096], P('kv', 'tp'), may hold values from -0.0546875 to 0.0546875
Outputs:
- layer_out: bfloat16 [64, 4096], P('kv', 'tp')
Inputs may be any that keep to these rules, and one draw needn't show every extreme that they name: Sequence s has lengths[s] earlier positions; slots 0 to (lengths[s] mod 128) - 1 of key_block and value_block hold the turned, scaled keys and the values of its positions from 128 * floor(lengths[s] / 128) on, prior_state holds the state of the positions before them, and the other slots take no part.
All inputs are finite; a program needn't handle non-finite values. No bound on the sum of `lengths` on one device may be relied on, other than what follows from the above.
Results may differ from a plain program's by a relative error of at most 0.029.
Values may be sent and summed in bfloat16 or wider, within the bound.
No kernel may reach another device: no remote copies, remote signals or barrier semaphores. Data moves between devices by JAX's collectives and lax.ppermute only.
A program may use at most 64 MiB of HBM per device.

v0:
```python
import jax
import jax.numpy as jnp
from jax import lax
from jax.sharding import PartitionSpec as P

D = 4096


epsilon = 1e-06


def from_everyone(value, axis):
    copies = jnp.broadcast_to(value, (lax.axis_size(axis), *value.shape))
    return lax.all_to_all(copies, axis, split_axis=0, concat_axis=0, tiled=True)


def over_copies(value, axis):
    return from_everyone(value, axis).sum(axis=0)


def in_order(parts, dim):
    shape = list(parts.shape[1:])
    shape[dim] *= parts.shape[0]
    return jnp.moveaxis(parts, 0, dim).reshape(shape)


def gathered_copies(value, axis, dim):
    parts = from_everyone(value, axis)
    return in_order(parts, dim)


def split_up(value, dim, count):
    shape = value.shape
    parts = value.reshape(*shape[:dim], count, shape[dim] // count, *shape[dim + 1 :])
    return jnp.moveaxis(parts, dim, 0)


def summed_on_arrival(value, axis, dim):
    count = lax.axis_size(axis)
    parts = lax.all_to_all(split_up(value, dim, count), axis, 0, 0, tiled=True)
    return jnp.sum(parts.astype(jnp.float32), axis=0)


def as_sent(value):
    return jax.tree.map(lambda a: a.astype(jnp.bfloat16) if a.dtype == jnp.float32 else a, value)


def side_by_side(arrays, axis, dim, along):
    ends, at = ([], 0)
    for a in arrays[:-1]:
        at += a.shape[along]
        ends.append(at)
    both = jnp.concatenate(arrays, axis=along)
    return tuple(jnp.split(summed_on_arrival(both, axis, dim), ends, axis=along))


def rotate(vectors, position):
    half_dim = vectors.shape[-1] // 2
    inverse = 10000.0 ** (-jnp.arange(half_dim, dtype=jnp.float32) / half_dim)
    angles = position.astype(jnp.float32)[:, None, None] * inverse
    cosine_part = jnp.cos(angles)
    sine_part = jnp.sin(angles)
    front_half = vectors[..., :half_dim]
    back_half = vectors[..., half_dim:]
    return jnp.concatenate(
        [
            front_half * cosine_part - back_half * sine_part,
            front_half * sine_part + back_half * cosine_part,
        ],
        axis=-1,
    )


def retain(
    queries,
    keys_new,
    values_new,
    gates,
    decay_rate,
    prior_state,
    key_block,
    value_block,
    lengths,
    group_gain,
):
    batch_rows = queries.shape[0]
    heads_here = decay_rate.shape[0]
    key_width = prior_state.shape[2]
    value_width = prior_state.shape[3]
    block_len = key_block.shape[2]
    rotated = rotate(
        queries.astype(jnp.float32).reshape(batch_rows, heads_here, key_width), lengths
    ).astype(jnp.bfloat16)
    fresh_keys = rotate(
        keys_new.astype(jnp.float32).reshape(batch_rows, heads_here, key_width), lengths
    ) * key_width ** (-0.5)
    fresh_values = values_new.astype(jnp.float32).reshape(batch_rows, heads_here, value_width)
    filled = lengths % block_len
    slots = jnp.arange(block_len, dtype=jnp.int32)
    distance = (filled[:, None] - slots[None, :]).astype(jnp.float32)
    live_slots = (slots[None, :] < filled[:, None])[:, None, :]
    weighting = jnp.where(
        live_slots, jnp.exp(-decay_rate[None, :, None] * distance[:, None, :]), jnp.float32(0.0)
    )
    scores = jnp.einsum("shk,shjk->shj", rotated, key_block, preferred_element_type=jnp.float32)
    block_weights = (scores * weighting).astype(jnp.bfloat16)
    block_term = jnp.einsum(
        "shj,shjv->shv", block_weights, value_block, preferred_element_type=jnp.float32
    )
    rotated_wide = rotated.astype(jnp.float32)
    own_term = jnp.sum(rotated_wide * fresh_keys, axis=-1, keepdims=True) * fresh_values
    carried = jnp.exp(-decay_rate[None, :, None] * (filled[:, None, None] + 1).astype(jnp.float32))
    state_term = carried * jnp.einsum(
        "shk,shkv->shv", rotated_wide, prior_state, precision=lax.Precision.HIGHEST
    )
    retained = own_term + block_term + state_term
    centre = jnp.mean(retained, axis=-1, keepdims=True)
    spread = jnp.mean(jnp.square(retained - centre), axis=-1, keepdims=True)
    normed = (retained - centre) * lax.rsqrt(spread + epsilon)
    gated = (
        jax.nn.silu(gates.astype(jnp.float32)).reshape(batch_rows, heads_here, value_width)
        * normed
        * group_gain.reshape(heads_here, value_width)
    )
    return gated.astype(jnp.bfloat16).reshape(batch_rows, heads_here * value_width)


def local(
    hidden_in,
    mixer_gain,
    query_weight,
    key_weight,
    value_weight,
    gate_weight,
    decay_rate,
    prior_state,
    key_block,
    value_block,
    lengths,
    group_gain,
    output_weight,
    channel_gain,
    hidden_gate,
    hidden_up,
    hidden_down,
):
    local_seqs = lengths.shape[0]
    first_row = lax.axis_index("tp") * local_seqs
    stream = hidden_in.astype(jnp.float32)
    scaled_in = (stream * mixer_gain).astype(jnp.bfloat16)
    own_squares = jnp.sum(stream * stream, axis=1)
    own_squares = over_copies(own_squares, "tp")
    all_rows, all_squares = (
        gathered_copies(scaled_in, "kv", 0),
        gathered_copies(own_squares.astype(jnp.bfloat16), "kv", 0).astype(own_squares.dtype),
    )
    weights_in = (query_weight, key_weight, value_weight, gate_weight)
    terms = tuple(
        (jnp.dot(all_rows, matrix, preferred_element_type=jnp.float32) for matrix in weights_in)
    )
    summed = jax.tree.map(lambda part: summed_on_arrival(part, "tp", 0), as_sent(terms))
    row_squares = lax.dynamic_slice_in_dim(all_squares, first_row, local_seqs, 0)
    first_scale = lax.rsqrt(row_squares / D + epsilon)[:, None]
    queries = (first_scale * summed[0]).astype(jnp.bfloat16)
    keys_new = (first_scale * summed[1]).astype(jnp.bfloat16)
    values_new = (first_scale * summed[2]).astype(jnp.bfloat16)
    gates = (first_scale * summed[3]).astype(jnp.bfloat16)
    mixed = retain(
        queries,
        keys_new,
        values_new,
        gates,
        decay_rate,
        prior_state,
        key_block,
        value_block,
        lengths,
        group_gain,
    )
    head_terms = jnp.dot(
        gathered_copies(mixed, "tp", 0), output_weight, preferred_element_type=jnp.float32
    )
    mixer_out = summed_on_arrival(head_terms.astype(jnp.bfloat16), "kv", 0)
    middle = stream + mixer_out
    scaled_mid = (middle * channel_gain).astype(jnp.bfloat16)
    middle_squares = jnp.sum(middle * middle, axis=1)
    middle_squares = over_copies(middle_squares, "tp")
    middle_rows, middle_all = (
        gathered_copies(scaled_mid, "kv", 0),
        gathered_copies(middle_squares.astype(jnp.bfloat16), "kv", 0).astype(middle_squares.dtype),
    )
    channel_terms = (
        jnp.dot(middle_rows, hidden_gate, preferred_element_type=jnp.float32),
        jnp.dot(middle_rows, hidden_up, preferred_element_type=jnp.float32),
    )
    channel_summed = side_by_side(
        (channel_terms[0].astype(jnp.bfloat16), channel_terms[1].astype(jnp.bfloat16)), "tp", 0, 1
    )
    middle_row_squares = lax.dynamic_slice_in_dim(middle_all, first_row, local_seqs, 0)
    second_scale = lax.rsqrt(middle_row_squares / D + epsilon)[:, None]
    gate_part = second_scale * channel_summed[0]
    up_part = second_scale * channel_summed[1]
    activated = (jax.nn.silu(gate_part) * up_part).astype(jnp.bfloat16)
    unit_terms = jnp.dot(
        gathered_copies(activated, "tp", 0), hidden_down, preferred_element_type=jnp.float32
    )
    channel_out = summed_on_arrival(unit_terms.astype(jnp.bfloat16), "kv", 0)
    return (middle + channel_out).astype(jnp.bfloat16)


def solution(mesh):
    in_specs = (
        P("kv", "tp"),
        P("tp"),
        P("tp", "kv"),
        P("tp", "kv"),
        P("tp", "kv"),
        P("tp", "kv"),
        P("kv"),
        P("tp", "kv", None, None),
        P("tp", "kv", None, None),
        P("tp", "kv", None, None),
        P("tp"),
        P("kv"),
        P("kv", "tp"),
        P("tp"),
        P("tp", "kv"),
        P("tp", "kv"),
        P("kv", "tp"),
    )
    out_specs = P("kv", "tp")
    return jax.shard_map(local, mesh=mesh, in_specs=in_specs, out_specs=out_specs, check_vma=False)
```

profile of v0, /device:TPU:1, one launch (start us, length us, event | category | flops | bytes accessed | tf_op | source)
XLA Modules:
  0.0 247.6 jit_solution(4408424907867211999)
XLA Ops:
  0.0 0.9 fusion.12
  0.9 0.6 broadcast_in_dim.20
  1.5 16.7 %all-to-all-start = ((f32[32,1,4]{2,1,0:T(1,128)}), f32[32,1,4]{2,1,0:T(1,128)S(1)}, u32[]{:S(2)}, u32[]{:S(2)}) async-start(f32[32,1,4]{2,1,0:T(1,128)} %broadcast_in_dim.20), calls=%async_computation | async-start | bytes 32768 | tf_op jit(solution)/shard_map/all_to_all | solution.py:14
  18.9 0.6 copy-done.14
  19.6 10.4 %all-to-all-done = f32[32,1,4]{2,1,0:T(1,128)S(1)} async-done(((f32[32,1,4]{2,1,0:T(1,128)}), f32[32,1,4]{2,1,0:T(1,128)S(1)}, u32[]{:S(2)}, u32[]{:S(2)}) %all-to-all-start) | async-done | bytes 544 | tf_op jit(solution)/shard_map/all_to_all | solution.py:14
  30.1 0.6 broadcast_in_dim.21
  30.7 6.8 %all-to-all-start.1 = ((bf16[16,1,4]{2,1,0:T(2,128)(2,1)}), bf16[16,1,4]{2,1,0:T(2,128)(2,1)S(1)}, u32[]{:S(2)}, u32[]{:S(2)}) async-start(bf16[16,1,4]{2,1,0:T(2,128)(2,1)} %broadcast_in_dim.21), calls=%async_computation.1 | async-start | bytes 16384 | tf_op jit(solution)/shard_map/all_to_all | solution.py:14
  37.4 6.4 %all-to-all-done.1 = bf16[16,1,4]{2,1,0:T(2,128)(2,1)S(1)} async-done(((bf16[16,1,4]{2,1,0:T(2,128)(2,1)}), bf16[16,1,4]{2,1,0:T(2,128)(2,1)S(1)}, u32[]{:S(2)}, u32[]{:S(2)}) %all-to-all-start.1) | async-done | bytes 160 | tf_op jit(solution)/shard_map/all_to_all | solution.py:14
  43.9 0.6 broadcast_in_dim.22
  44.5 3.5 %all-to-all-start.2 = ((bf16[16,4,128]{2,1,0:T(4,128)(2,1)}), bf16[16,4,128]{2,1,0:T(4,128)(2,1)S(1)}, u32[]{:S(2)}, u32[]{:S(2)}) async-start(bf16[16,4,128]{2,1,0:T(4,128)(2,1)} %broadcast_in_dim.22), calls=%async_computation.2 | async-start | bytes 32768 | tf_op jit(solution)/shard_map/all_to_all | solution.py:14
  48.0 0.1 reshape.384
  48.1 0.1 add_rsqrt_fusion.2
  48.2 6.2 %all-to-all-done.2 = bf16[16,4,128]{2,1,0:T(4,128)(2,1)S(1)} async-done(((bf16[16,4,128]{2,1,0:T(4,128)(2,1)}), bf16[16,4,128]{2,1,0:T(4,128)(2,1)S(1)}, u32[]{:S(2)}, u32[]{:S(2)}) %all-to-all-start.2) | async-done | bytes 16416 | tf_op jit(solution)/shard_map/all_to_all | solution.py:14
  54.3 0.1 convolution_convert_fusion.4
  54.5 0.6 reshape.373
  55.1 7.0 %all-to-all-start.5 = ((bf16[32,2,256]{2,1,0:T(2,128)(2,1)}), bf16[32,2,256]{2,1,0:T(2,128)(2,1)S(1)}, u32[]{:S(2)}, u32[]{:S(2)}) async-start(bf16[32,2,256]{2,1,0:T(2,128)(2,1)} %reshape.373), calls=%async_computation.5 | async-start | bytes 65536 | tf_op jit(solution)/shard_map/all_to_all | solution.py:40
  62.1 0.1 convolution_convert_fusion.5
  62.2 0.6 reshape.372
  62.9 0.1 convolution_convert_fusion.2
  63.0 11.3 %all-to-all-done.5 = bf16[32,2,256]{2,1,0:T(2,128)(2,1)S(1)} async-done(((bf16[32,2,256]{2,1,0:T(2,128)(2,1)}), bf16[32,2,256]{2,1,0:T(2,128)(2,1)S(1)}, u32[]{:S(2)}, u32[]{:S(2)}) %all-to-all-start.5) | async-done | bytes 32800 | tf_op jit(solution)/shard_map/all_to_all | solution.py:40
  74.4 4.5 %all-to-all-start.4 = ((bf16[32,2,256]{2,1,0:T(2,128)(2,1)}), bf16[32,2,256]{2,1,0:T(2,128)(2,1)S(1)}, u32[]{:S(2)}, u32[]{:S(2)}) async-start(bf16[32,2,256]{2,1,0:T(2,128)(2,1)} %reshape.372), calls=%async_computation.4 | async-start | bytes 65536 | tf_op jit(solution)/shard_map/all_to_all | solution.py:40
  78.9 0.1 convolution_convert_fusion.3
  79.1 0.7 reshape.374
  79.7 0.6 reshape.371
  80.4 10.7 %all-to-all-done.4 = bf16[32,2,256]{2,1,0:T(2,128)(2,1)S(1)} async-done(((bf16[32,2,256]{2,1,0:T(2,128)(2,1)}), bf16[32,2,256]{2,1,0:T(2,128)(2,1)S(1)}, u32[]{:S(2)}, u32[]{:S(2)}) %all-to-all-start.4) | async-done | bytes 32800 | tf_op jit(solution)/shard_map/all_to_all | solution.py:40
  91.1 4.5 %all-to-all-start.6 = ((bf16[32,2,512]{2,1,0:T(2,128)(2,1)}), bf16[32,2,512]{2,1,0:T(2,128)(2,1)S(1)}, u32[]{:S(2)}, u32[]{:S(2)}) async-start(bf16[32,2,512]{2,1,0:T(2,128)(2,1)} %reshape.374), calls=%async_computation.6 | async-start | bytes 131072 | tf_op jit(solution)/shard_map/all_to_all | solution.py:40
  95.8 0.1 fusion.30
  95.9 0.1 fusion.4
  96.1 0.1 fusion.40
  96.2 0.2 fusion.2
  96.3 0.1 fusion.17
  96.5 0.4 fusion
  96.9 11.8 %all-to-all-done.6 = bf16[32,2,512]{2,1,0:T(2,128)(2,1)S(1)} async-done(((bf16[32,2,512]{2,1,0:T(2,128)(2,1)}), bf16[32,2,512]{2,1,0:T(2,128)(2,1)S(1)}, u32[]{:S(2)}, u32[]{:S(2)}) %all-to-all-start.6) | async-done | bytes 65568 | tf_op jit(solution)/shard_map/all_to_all | solution.py:40
  108.7 5.1 %all-to-all-start.3 = ((bf16[32,2,512]{2,1,0:T(2,128)(2,1)}), bf16[32,2,512]{2,1,0:T(2,128)(2,1)S(1)}, u32[]{:S(2)}, u32[]{:S(2)}) async-start(bf16[32,2,512]{2,1,0:T(2,128)(2,1)} %reshape.371), calls=%async_computation.3 | async-start | bytes 131072 | tf_op jit(solution)/shard_map/all_to_all | solution.py:40
  113.9 0.2 fusion.41
  114.1 0.2 multiply_reduce_fusion
  114.3 12.5 %all-to-all-done.3 = bf16[32,2,512]{2,1,0:T(2,128)(2,1)S(1)} async-done(((bf16[32,2,512]{2,1,0:T(2,128)(2,1)}), bf16[32,2,512]{2,1,0:T(2,128)(2,1)S(1)}, u32[]{:S(2)}, u32[]{:S(2)}) %all-to-all-start.3) | async-done | bytes 65568 | tf_op jit(solution)/shard_map/all_to_all | solution.py:40
  127.0 0.1 multiply_convert_fusion
  127.1 17.4 %all_to_all.79 = bf16[32,2,512]{2,1,0:T(2,128)(2,1)S(1)} all-to-all(bf16[32,2,512]{2,1,0:T(2,128)(2,1)S(1)} %broadcast_in_dim.24), channel_id=1, replica_groups=mesh['kv'=16,'tp'=32] {'tp'}, dimensions={0} | all-to-all | bytes 131072 | tf_op jit(solution)/shard_map/all_to_all | solution.py:14
  144.6 0.2 convolution_convert_fusion.7
  144.7 9.2 %all_to_all.80 = bf16[16,4,128]{2,1,0:T(4,128)(2,1)S(1)} all-to-all(bf16[16,4,128]{2,1,0:T(4,128)(2,1)S(1)} %bitcast.67), channel_id=1, replica_groups=mesh['kv'=16,'tp'=32] {'kv'}, dimensions={0} | all-to-all | bytes 32768 | tf_op jit(solution)/shard_map/all_to_all | solution.py:40
  154.0 0.6 copy-done.11
  154.6 0.1 multiply_reduce_fusion.1
  154.8 17.6 %all_to_all.81 = f32[32,1,4]{2,1,0:T(1,128)S(1)} all-to-all(f32[32,1,4]{2,1,0:T(1,128)S(1)} %broadcast_in_dim.25), channel_id=1, replica_groups=mesh['kv'=16,'tp'=32] {'tp'}, dimensions={0} | all-to-all | bytes 1024 | tf_op jit(solution)/shard_map/all_to_all | solution.py:14
  172.4 0.6 broadcast_in_dim.27
  173.0 3.6 %all-to-all-start.11 = ((bf16[16,4,128]{2,1,0:T(4,128)(2,1)}), bf16[16,4,128]{2,1,0:T(4,128)(2,1)S(1)}, u32[]{:S(2)}, u32[]{:S(2)}) async-start(bf16[16,4,128]{2,1,0:T(4,128)(2,1)} %broadcast_in_dim.27), calls=%async_computation.11 | async-start | bytes 32768 | tf_op jit(solution)/shard_map/all_to_all | solution.py:14
  176.7 6.3 %all-to-all-done.11 = bf16[16,4,128]{2,1,0:T(4,128)(2,1)S(1)} async-done(((bf16[16,4,128]{2,1,0:T(4,128)(2,1)}), bf16[16,4,128]{2,1,0:T(4,128)(2,1)S(1)}, u32[]{:S(2)}, u32[]{:S(2)}) %all-to-all-start.11) | async-done | bytes 16416 | tf_op jit(solution)/shard_map/all_to_all | solution.py:14
  183.0 0.6 broadcast_in_dim.26
  183.6 3.4 %all-to-all-start.10 = ((bf16[16,1,4]{2,1,0:T(2,128)(2,1)}), bf16[16,1,4]{2,1,0:T(2,128)(2,1)S(1)}, u32[]{:S(2)}, u32[]{:S(2)}) async-start(bf16[16,1,4]{2,1,0:T(2,128)(2,1)} %broadcast_in_dim.26), calls=%async_computation.10 | async-start | bytes 16384 | tf_op jit(solution)/shard_map/all_to_all | solution.py:14
  187.0 0.2 convolution_convert_fusion
  187.3 0.2 convolution_convert_fusion.1
  187.5 0.1 pad_maximum_fusion
  187.6 0.7 reshape.381
  188.3 5.0 %all-to-all-done.10 = bf16[16,1,4]{2,1,0:T(2,128)(2,1)S(1)} async-done(((bf16[16,1,4]{2,1,0:T(2,128)(2,1)}), bf16[16,1,4]{2,1,0:T(2,128)(2,1)S(1)}, u32[]{:S(2)}, u32[]{:S(2)}) %all-to-all-start.10) | async-done | bytes 160 | tf_op jit(solution)/shard_map/all_to_all | solution.py:14
  193.3 6.8 %all-to-all-start.12 = ((bf16[32,2,1408]{2,1,0:T(2,128)(2,1)}), bf16[32,2,1408]{2,1,0:T(2,128)(2,1)S(1)}, u32[]{:S(2)}, u32[]{:S(2)}) async-start(bf16[32,2,1408]{2,1,0:T(2,128)(2,1)} %reshape.381), calls=%async_computation.12 | async-start | bytes 360448 | tf_op jit(solution)/shard_map/all_to_all | solution.py:40
  200.1 0.1 reshape.385
  200.2 0.1 add_rsqrt_fusion
  200.3 17.8 %all-to-all-done.12 = bf16[32,2,1408]{2,1,0:T(2,128)(2,1)S(1)} async-done(((bf16[32,2,1408]{2,1,0:T(2,128)(2,1)}), bf16[32,2,1408]{2,1,0:T(2,128)(2,1)S(1)}, u32[]{:S(2)}, u32[]{:S(2)}) %all-to-all-start.12) | async-done | bytes 180256 | tf_op jit(solution)/shard_map/all_to_all | solution.py:40
  218.1 0.2 convert_reduce_fusion
  218.3 0.1 fusion.7
  218.4 19.1 %all_to_all.82 = bf16[32,2,704]{2,1,0:T(2,128)(2,1)S(1)} all-to-all(bf16[32,2,704]{2,1,0:T(2,128)(2,1)S(1)} %broadcast_in_dim.28), channel_id=1, replica_groups=mesh['kv'=16,'tp'=32] {'tp'}, dimensions={0} | all-to-all | bytes 180224 | tf_op jit(solution)/shard_map/all_to_all | solution.py:14
  237.6 0.2 convolution_convert_fusion.6
  237.8 9.2 %all_to_all.83 = bf16[16,4,128]{2,1,0:T(4,128)(2,1)S(1)} all-to-all(bf16[16,4,128]{2,1,0:T(4,128)(2,1)S(1)} %bitcast.66), channel_id=1, replica_groups=mesh['kv'=16,'tp'=32] {'kv'}, dimensions={0} | all-to-all | bytes 32768 | tf_op jit(solution)/shard_map/all_to_all | solution.py:40
  247.0 0.6 add_convert_fusion
  (50 shorter events, 0.9 us)
Async XLA Ops:
  0.0 96.4 %copy-start = (f32[2,1,256,512]{3,2,1,0:T(8,128)S(1)}, f32[2,1,256,512]{3,2,1,0:T(8,128)}, u32[]{:S(2)}) copy-start(f32[2,1,256,512]{3,2,1,0:T(8,128)} %param.24) | copy-start | bytes 3145732
  1.5 28.5 %all-to-all-start = ((f32[32,1,4]{2,1,0:T(1,128)}), f32[32,1,4]{2,1,0:T(1,128)S(1)}, u32[]{:S(2)}, u32[]{:S(2)}) async-start(f32[32,1,4]{2,1,0:T(1,128)} %broadcast_in_dim.20), calls=%async_computation | async-start | bytes 32768 | tf_op jit(solution)/shard_map/all_to_all | solution.py:14
  18.9 0.7 copy-start.14
  19.6 34.7 %copy-start.9 = (bf16[128,256]{1,0:T(8,128)(2,1)S(1)}, bf16[128,256]{1,0:T(8,128)(2,1)}, u32[]{:S(2)}) copy-start(bf16[128,256]{1,0:T(8,128)(2,1)} %param.20) | copy-start | bytes 196612
  30.7 13.2 %all-to-all-start.1 = ((bf16[16,1,4]{2,1,0:T(2,128)(2,1)}), bf16[16,1,4]{2,1,0:T(2,128)(2,1)S(1)}, u32[]{:S(2)}, u32[]{:S(2)}) async-start(bf16[16,1,4]{2,1,0:T(2,128)(2,1)} %broadcast_in_dim.21), calls=%async_computation.1 | async-start | bytes 16384 | tf_op jit(solution)/shard_map/all_to_all | solution.py:14
  44.5 9.9 %all-to-all-start.2 = ((bf16[16,4,128]{2,1,0:T(4,128)(2,1)}), bf16[16,4,128]{2,1,0:T(4,128)(2,1)S(1)}, u32[]{:S(2)}, u32[]{:S(2)}) async-start(bf16[16,4,128]{2,1,0:T(4,128)(2,1)} %broadcast_in_dim.22), calls=%async_computation.2 | async-start | bytes 32768 | tf_op jit(solution)/shard_map/all_to_all | solution.py:14
  54.5 7.6 %copy-start.10 = (bf16[128,256]{1,0:T(8,128)(2,1)S(1)}, bf16[128,256]{1,0:T(8,128)(2,1)}, u32[]{:S(2)}) copy-start(bf16[128,256]{1,0:T(8,128)(2,1)} %param.19) | copy-start | bytes 196612
  55.1 7.8 %copy-start.6 = (bf16[128,512]{1,0:T(8,128)(2,1)S(1)}, bf16[128,512]{1,0:T(8,128)(2,1)}, u32[]{:S(2)}) copy-start(bf16[128,512]{1,0:T(8,128)(2,1)} %param.21) | copy-start | bytes 393220
  55.1 19.3 %all-to-all-start.5 = ((bf16[32,2,256]{2,1,0:T(2,128)(2,1)}), bf16[32,2,256]{2,1,0:T(2,128)(2,1)S(1)}, u32[]{:S(2)}, u32[]{:S(2)}) async-start(bf16[32,2,256]{2,1,0:T(2,128)(2,1)} %reshape.373), calls=%async_computation.5 | async-start | bytes 65536 | tf_op jit(solution)/shard_map/all_to_all | solution.py:40
  62.9 16.0 %copy-start.7 = (bf16[128,512]{1,0:T(8,128)(2,1)S(1)}, bf16[128,512]{1,0:T(8,128)(2,1)}, u32[]{:S(2)}) copy-start(bf16[128,512]{1,0:T(8,128)(2,1)} %param.22) | copy-start | bytes 393220
  74.4 16.8 %all-to-all-start.4 = ((bf16[32,2,256]{2,1,0:T(2,128)(2,1)}), bf16[32,2,256]{2,1,0:T(2,128)(2,1)S(1)}, u32[]{:S(2)}, u32[]{:S(2)}) async-start(bf16[32,2,256]{2,1,0:T(2,128)(2,1)} %reshape.372), calls=%async_computation.4 | async-start | bytes 65536 | tf_op jit(solution)/shard_map/all_to_all | solution.py:40
  79.0 16.9 %copy-start.5 = (bf16[2,1,128,256]{3,2,1,0:T(8,128)(2,1)S(1)}, bf16[2,1,128,256]{3,2,1,0:T(8,128)(2,1)}, u32[]{:S(2)}) copy-start(bf16[2,1,128,256]{3,2,1,0:T(8,128)(2,1)} %param.25) | copy-start | bytes 393220
  79.7 16.5 %copy-start.1 = (bf16[2,1,128,512]{3,2,1,0:T(8,128)(2,1)S(1)}, bf16[2,1,128,512]{3,2,1,0:T(8,128)(2,1)}, u32[]{:S(2)}) copy-start(bf16[2,1,128,512]{3,2,1,0:T(8,128)(2,1)} %param.26) | copy-start | bytes 786436
  91.1 17.6 %all-to-all-start.6 = ((bf16[32,2,512]{2,1,0:T(2,128)(2,1)}), bf16[32,2,512]{2,1,0:T(2,128)(2,1)S(1)}, u32[]{:S(2)}, u32[]{:S(2)}) async-start(bf16[32,2,512]{2,1,0:T(2,128)(2,1)} %reshape.374), calls=%async_computation.6 | async-start | bytes 131072 | tf_op jit(solution)/shard_map/all_to_all | solution.py:40
  108.7 18.2 %all-to-all-start.3 = ((bf16[32,2,512]{2,1,0:T(2,128)(2,1)}), bf16[32,2,512]{2,1,0:T(2,128)(2,1)S(1)}, u32[]{:S(2)}, u32[]{:S(2)}) async-start(bf16[32,2,512]{2,1,0:T(2,128)(2,1)} %reshape.371), calls=%async_computation.3 | async-start | bytes 131072 | tf_op jit(solution)/shard_map/all_to_all | solution.py:40
  114.3 12.6 %copy-start.12 = (f32[512]{0:T(512)S(1)}, f32[512]{0:T(512)}, u32[]{:S(2)}) copy-start(f32[512]{0:T(512)} %param.28) | copy-start | bytes 6148
  127.1 17.5 %copy-start.8 = (bf16[512,128]{1,0:T(8,128)(2,1)S(1)}, bf16[512,128]{1,0:T(8,128)(2,1)}, u32[]{:S(2)}) copy-start(bf16[512,128]{1,0:T(8,128)(2,1)} %param.29) | copy-start | bytes 393220
  144.6 42.5 %copy-start.2 = (bf16[128,704]{0,1:T(8,128)(2,1)S(1)}, bf16[128,704]{0,1:T(8,128)(2,1)}, u32[]{:S(2)}) copy-start(bf16[128,704]{0,1:T(8,128)(2,1)} %param.32) | copy-start | bytes 540676
  154.0 0.7 copy-start.11
  154.0 0.7 copy-start.13
  173.0 14.3 %copy-start.3 = (bf16[128,704]{0,1:T(8,128)(2,1)S(1)}, bf16[128,704]{0,1:T(8,128)(2,1)}, u32[]{:S(2)}) copy-start(bf16[128,704]{0,1:T(8,128)(2,1)} %param.31) | copy-start | bytes 540676
  173.0 10.0 %all-to-all-start.11 = ((bf16[16,4,128]{2,1,0:T(4,128)(2,1)}), bf16[16,4,128]{2,1,0:T(4,128)(2,1)S(1)}, u32[]{:S(2)}, u32[]{:S(2)}) async-start(bf16[16,4,128]{2,1,0:T(4,128)(2,1)} %broadcast_in_dim.27), calls=%async_computation.11 | async-start | bytes 32768 | tf_op jit(solution)/shard_map/all_to_all | solution.py:14
  183.6 9.7 %all-to-all-start.10 = ((bf16[16,1,4]{2,1,0:T(2,128)(2,1)}), bf16[16,1,4]{2,1,0:T(2,128)(2,1)S(1)}, u32[]{:S(2)}, u32[]{:S(2)}) async-start(bf16[16,1,4]{2,1,0:T(2,128)(2,1)} %broadcast_in_dim.26), calls=%async_computation.10 | async-start | bytes 16384 | tf_op jit(solution)/shard_map/all_to_all | solution.py:14
  193.3 24.8 %all-to-all-start.12 = ((bf16[32,2,1408]{2,1,0:T(2,128)(2,1)}), bf16[32,2,1408]{2,1,0:T(2,128)(2,1)S(1)}, u32[]{:S(2)}, u32[]{:S(2)}) async-start(bf16[32,2,1408]{2,1,0:T(2,128)(2,1)} %reshape.381), calls=%async_computation.12 | async-start | bytes 360448 | tf_op jit(solution)/shard_map/all_to_all | solution.py:40
  218.4 19.2 %copy-start.4 = (bf16[704,128]{1,0:T(8,128)(2,1)S(1)}, bf16[704,128]{1,0:T(8,128)(2,1)}, u32[]{:S(2)}) copy-start(bf16[704,128]{1,0:T(8,128)(2,1)} %param.33) | copy-start | bytes 540676
where the time goes:
time: 249 us; the launch traced here: 248 us
  waiting for transfers between devices  98.5 us (40%)
  blocking collectives  72.5 us (29%)
  starting transfers between devices  62.1 us (25%)
  local copies, waits for them, and re-layouts  8.04 us (3%)
  other arithmetic  3.44 us (1%)
    all_to_all x5, waiting for transfers between devices, summed_on_arrival(): parts = lax.all_to_all(split_up(value, dim, count), axis, 0, 0, tiled=True)  64.2 us
    all_to_all x3, blocking collectives, from_everyone(): return lax.all_to_all(copies, axis, split_axis=0, concat_axis=0, tiled=True)  54.1 us
    all_to_all x5, waiting for transfers between devices, from_everyone(): return lax.all_to_all(copies, axis, split_axis=0, concat_axis=0, tiled=True)  34.3 us
    all_to_all x5, starting transfers between devices, from_everyone(): return lax.all_to_all(copies, axis, split_axis=0, concat_axis=0, tiled=True)  34 us
    all_to_all x5, starting transfers between devices, summed_on_arrival(): parts = lax.all_to_all(split_up(value, dim, count), axis, 0, 0, tiled=True)  28 us
    all_to_all x2, blocking collectives, summed_on_arrival(): parts = lax.all_to_all(split_up(value, dim, count), axis, 0, 0, tiled=True)  18.4 us
  transfers between devices with their start and end apart: 10, of which 10 were waited for; matrix products, arithmetic and copies ran while one was open for 2% of the time, Pallas kernels for 0%

commit v1 on v0

--- a/solution.py
+++ b/solution.py
@@ -4,6 +4,7 @@
 from jax.sharding import PartitionSpec as P
 
 D = 4096
+LANES = 128
 
 
 epsilon = 1e-06
@@ -12,10 +13,6 @@
 def from_everyone(value, axis):
     copies = jnp.broadcast_to(value, (lax.axis_size(axis), *value.shape))
     return lax.all_to_all(copies, axis, split_axis=0, concat_axis=0, tiled=True)
-
-
-def over_copies(value, axis):
-    return from_everyone(value, axis).sum(axis=0)
 
 
 def in_order(parts, dim):
@@ -39,10 +36,6 @@
     count = lax.axis_size(axis)
     parts = lax.all_to_all(split_up(value, dim, count), axis, 0, 0, tiled=True)
     return jnp.sum(parts.astype(jnp.float32), axis=0)
-
-
-def as_sent(value):
-    return jax.tree.map(lambda a: a.astype(jnp.bfloat16) if a.dtype == jnp.float32 else a, value)
 
 
 def side_by_side(arrays, axis, dim, along):
@@ -52,6 +45,10 @@
         ends.append(at)
     both = jnp.concatenate(arrays, axis=along)
     return tuple(jnp.split(summed_on_arrival(both, axis, dim), ends, axis=along))
+
+
+def as_column(value, width):
+    return jnp.pad(value, ((0, 0), (0, width - 1))).astype(jnp.bfloat16)
 
 
 def rotate(vectors, position):
@@ -144,27 +141,24 @@
     hidden_up,
     hidden_down,
 ):
-    local_seqs = lengths.shape[0]
-    first_row = lax.axis_index("tp") * local_seqs
-    stream = hidden_in.astype(jnp.float32)
+    own_rows = hidden_in.shape[0]
+    units = hidden_gate.shape[1]
+    pad = -units % LANES
+    stream = gathered_copies(hidden_in, "kv", 0).astype(jnp.float32)
     scaled_in = (stream * mixer_gain).astype(jnp.bfloat16)
-    own_squares = jnp.sum(stream * stream, axis=1)
-    own_squares = over_copies(own_squares, "tp")
-    all_rows, all_squares = (
-        gathered_copies(scaled_in, "kv", 0),
-        gathered_copies(own_squares.astype(jnp.bfloat16), "kv", 0).astype(own_squares.dtype),
-    )
-    weights_in = (query_weight, key_weight, value_weight, gate_weight)
-    terms = tuple(
-        (jnp.dot(all_rows, matrix, preferred_element_type=jnp.float32) for matrix in weights_in)
-    )
-    summed = jax.tree.map(lambda part: summed_on_arrival(part, "tp", 0), as_sent(terms))
-    row_squares = lax.dynamic_slice_in_dim(all_squares, first_row, local_seqs, 0)
-    first_scale = lax.rsqrt(row_squares / D + epsilon)[:, None]
-    queries = (first_scale * summed[0]).astype(jnp.bfloat16)
-    keys_new = (first_scale * summed[1]).astype(jnp.bfloat16)
-    values_new = (first_scale * summed[2]).astype(jnp.bfloat16)
-    gates = (first_scale * summed[3]).astype(jnp.bfloat16)
+    squares = as_column(jnp.sum(stream * stream, axis=1, keepdims=True), LANES)
+    terms = [
+        jnp.dot(scaled_in, matrix, preferred_element_type=jnp.float32).astype(jnp.bfloat16)
+        for matrix in (query_weight, key_weight, value_weight, gate_weight)
+    ]
+    queries, keys_new, values_new, gates, row_squares = side_by_side(
+        (*terms, squares), "tp", 0, 1
+    )
+    first_scale = lax.rsqrt(row_squares[:, :1] / D + epsilon)
+    queries = (first_scale * queries).astype(jnp.bfloat16)
+    keys_new = (first_scale * keys_new).astype(jnp.bfloat16)
+    values_new = (first_scale * values_new).astype(jnp.bfloat16)
+    gates = (first_scale * gates).astype(jnp.bfloat16)
     mixed = retain(
         queries,
         keys_new,
@@ -180,32 +174,27 @@
     head_terms = jnp.dot(
         gathered_copies(mixed, "tp", 0), output_weight, preferred_element_type=jnp.float32
     )
-    mixer_out = summed_on_arrival(head_terms.astype(jnp.bfloat16), "kv", 0)
-    middle = stream + mixer_out
+    head_parts = from_everyone(head_terms.astype(jnp.bfloat16), "kv")
+    middle = stream + jnp.sum(head_parts.astype(jnp.float32), axis=0)
     scaled_mid = (middle * channel_gain).astype(jnp.bfloat16)
-    middle_squares = jnp.sum(middle * middle, axis=1)
-    middle_squares = over_copies(middle_squares, "tp")
-    middle_rows, middle_all = (
-        gathered_copies(scaled_mid, "kv", 0),
-        gathered_copies(middle_squares.astype(jnp.bfloat16), "kv", 0).astype(middle_squares.dtype),
-    )
-    channel_terms = (
-        jnp.dot(middle_rows, hidden_gate, preferred_element_type=jnp.float32),
-        jnp.dot(middle_rows, hidden_up, preferred_element_type=jnp.float32),
-    )
-    channel_summed = side_by_side(
-        (channel_terms[0].astype(jnp.bfloat16), channel_terms[1].astype(jnp.bfloat16)), "tp", 0, 1
-    )
-    middle_row_squares = lax.dynamic_slice_in_dim(middle_all, first_row, local_seqs, 0)
-    second_scale = lax.rsqrt(middle_row_squares / D + epsilon)[:, None]
-    gate_part = second_scale * channel_summed[0]
-    up_part = second_scale * channel_summed[1]
+    middle_squares = as_column(jnp.sum(middle * middle, axis=1, keepdims=True), pad)
+    gate_terms, up_terms = (
+        jnp.dot(scaled_mid, matrix, preferred_element_type=jnp.float32).astype(jnp.bfloat16)
+        for matrix in (hidden_gate, hidden_up)
+    )
+    channel_summed = summed_on_arrival(
+        jnp.concatenate([gate_terms, middle_squares, up_terms], axis=1), "tp", 0
+    )
+    second_scale = lax.rsqrt(channel_summed[:, units : units + 1] / D + epsilon)
+    gate_part = second_scale * channel_summed[:, :units]
+    up_part = second_scale * channel_summed[:, units + pad :]
     activated = (jax.nn.silu(gate_part) * up_part).astype(jnp.bfloat16)
     unit_terms = jnp.dot(
         gathered_copies(activated, "tp", 0), hidden_down, preferred_element_type=jnp.float32
     )
     channel_out = summed_on_arrival(unit_terms.astype(jnp.bfloat16), "kv", 0)
-    return (middle + channel_out).astype(jnp.bfloat16)
+    own_middle = lax.dynamic_slice_in_dim(middle, lax.axis_index("kv") * own_rows, own_rows, 0)
+    return (own_middle + channel_out).astype(jnp.bfloat16)
 
 
 def solution(mesh):

time: 249 us -> 143 us (0.57)
  waiting for transfers between devices: 98.5 us -> 25.2 us
  starting transfers between devices: 62.1 us -> 21 us
  blocking collectives: 72.5 us -> 84.9 us
  local copies, waits for them, and re-layouts: 8.04 us -> 4.79 us
    all_to_all x5 -> x2, waiting for transfers between devices: 64.2 us -> 25.2 us  [summed_on_arrival(): parts = lax.all_to_all(split_up(value, dim, count), axis, 0, 0, tiled=True)]
    all_to_all x5 -> x0, waiting for transfers between devices: 34.3 us -> none  [from_everyone(): return lax.all_to_all(copies, axis, split_axis=0, concat_axis=0, tiled=True)]
    all_to_all x5 -> x0, starting transfers between devices: 34 us -> none  [from_everyone(): return lax.all_to_all(copies, axis, split_axis=0, concat_axis=0, tiled=True)]
    all_to_all x5 -> x2, starting transfers between devices: 28 us -> 21 us  [summed_on_arrival(): parts = lax.all_to_all(split_up(value, dim, count), axis, 0, 0, tiled=True)]
    all_to_all x2 -> x1, blocking collectives: 18.4 us -> 24.7 us  [summed_on_arrival(): parts = lax.all_to_all(split_up(value, dim, count), axis, 0, 0, tiled=True)]
    all_to_all x3 -> x4, blocking collectives: 54.1 us -> 60.2 us  [from_everyone(): return lax.all_to_all(copies, axis, split_axis=0, concat_axis=0, tiled=True)]
  transfers between devices with their start and end apart: 10 -> 2, of which waited for: 10 -> 2; matrix products, arithmetic and copies ran while one was open for 2% -> 0% of each run, Pallas kernels for 0% -> 0%
where the time goes in v1:
time: 143 us; the launch traced here: 142 us
  blocking collectives  84.9 us (59%)
  waiting for transfers between devices  25.2 us (18%)
  starting transfers between devices  21 us (15%)
  local copies, waits for them, and re-layouts  4.79 us (3%)
  matrix products  2.58 us (2%)
  other arithmetic  2.5 us (2%)
    all_to_all x4, blocking collectives, from_everyone(): return lax.all_to_all(copies, axis, split_axis=0, concat_axis=0, tiled=True)  60.2 us
    all_to_all x2, waiting for transfers between devices, summed_on_arrival(): parts = lax.all_to_all(split_up(value, dim, count), axis, 0, 0, tiled=True)  25.2 us
    all_to_all x1, blocking collectives, summed_on_arrival(): parts = lax.all_to_all(split_up(value, dim, count), axis, 0, 0, tiled=True)  24.7 us
    all_to_all x2, starting transfers between devices, summed_on_arrival(): parts = lax.all_to_all(split_up(value, dim, count), axis, 0, 0, tiled=True)  21 us
  transfers between devices with their start and end apart: 2, of which 2 were waited for; matrix products, arithmetic and copies ran while one was open for 0% of the time, Pallas kernels for 0%

profile of v1, /device:TPU:1, one launch (start us, length us, event | category | flops | bytes accessed | tf_op | source)
XLA Modules:
  0.0 141.9 jit_solution(369580406044176203)
XLA Ops:
  0.0 0.0 copy-start
  0.0 0.8 broadcast_in_dim.18
  0.8 13.9 %all_to_all.35 = bf16[16,4,128]{2,1,0:T(4,128)(2,1)S(1)} all-to-all(bf16[16,4,128]{2,1,0:T(4,128)(2,1)S(1)} %broadcast_in_dim.18), channel_id=1, replica_groups=mesh['kv'=16,'tp'=32] {'kv'}, dimensions={0} | all-to-all | bytes 32768 | tf_op jit(solution)/shard_map/all_to_all | solution.py:15
  14.7 0.1 multiply_reduce_fusion.1
  14.8 0.0 copy-start.6
  14.8 0.1 broadcast_in_dim.25
  14.9 0.0 copy-done.9
  14.9 0.0 copy-done.11
  14.9 0.1 fusion.3
  15.0 0.5 copy-done.10
  15.6 0.1 fusion.2
  15.7 0.0 copy-done.6
  15.7 0.1 fusion.1
  15.9 0.8 copy-done.7
  16.6 0.1 fusion
  16.8 0.8 reshape.286
  17.6 17.5 %all-to-all-start.1 = ((bf16[32,2,1664]{2,1,0:T(2,128)(2,1)}), bf16[32,2,1664]{2,1,0:T(2,128)(2,1)S(1)}, u32[]{:S(2)}, u32[]{:S(2)}) async-start(bf16[32,2,1664]{2,1,0:T(2,128)(2,1)} %reshape.286), calls=%async_computation.1 | async-start | bytes 425984 | tf_op jit(solution)/shard_map/all_to_all | solution.py:37
  35.1 0.0 copy-done.14
  35.7 0.0 copy-start.5
  35.8 18.9 %all-to-all-done.1 = bf16[32,2,1664]{2,1,0:T(2,128)(2,1)S(1)} async-done(((bf16[32,2,1664]{2,1,0:T(2,128)(2,1)}), bf16[32,2,1664]{2,1,0:T(2,128)(2,1)S(1)}, u32[]{:S(2)}, u32[]{:S(2)}) %all-to-all-start.1) | async-done | bytes 213024 | tf_op jit(solution)/shard_map/all_to_all | solution.py:37
  54.6 0.2 convert_reduce_fusion.1
  54.8 0.1 fusion.43
  54.9 0.1 bitcast_convert_fusion
  55.0 0.1 fusion.34
  55.2 0.0 copy-done.5
  55.2 0.1 fusion.8
  55.3 0.0 copy-done
  55.3 0.5 fusion.4
  55.8 0.1 fusion.21
  55.9 0.1 fusion.48
  56.0 0.3 copy-done.1
  56.3 0.1 fusion.6
  56.4 0.2 fusion.49
  56.6 0.2 multiply_reduce_fusion.2
  56.8 0.1 copy-done.13
  57.0 0.1 multiply_convert_fusion.4
  57.1 0.0 copy-start.8
  57.1 17.1 %all_to_all.36 = bf16[32,2,512]{2,1,0:T(2,128)(2,1)S(1)} all-to-all(bf16[32,2,512]{2,1,0:T(2,128)(2,1)S(1)} %broadcast_in_dim.21), channel_id=1, replica_groups=mesh['kv'=16,'tp'=32] {'tp'}, dimensions={0} | all-to-all | bytes 131072 | tf_op jit(solution)/shard_map/all_to_all | solution.py:15
  74.3 0.0 copy-done.8
  74.3 0.2 convolution_convert_fusion.7
  74.4 0.1 broadcast_in_dim.22
  74.5 10.3 %all_to_all.37 = bf16[16,64,128]{2,1,0:T(8,128)(2,1)S(1)} all-to-all(bf16[16,64,128]{2,1,0:T(8,128)(2,1)S(1)} %broadcast_in_dim.22), channel_id=1, replica_groups=mesh['kv'=16,'tp'=32] {'kv'}, dimensions={0} | all-to-all | bytes 524288 | tf_op jit(solution)/shard_map/all_to_all | solution.py:15
  84.8 0.0 copy-start.3
  84.8 0.8 copy-done.2
  85.7 0.0 copy-done.12
  85.7 0.2 convolution_convert_fusion
  85.9 0.2 convolution_convert_fusion.1
  86.1 0.1 multiply_reduce_fusion
  86.2 0.1 broadcast_in_dim.50
  86.3 0.1 concatenate.45
  86.4 0.1 reshape.295
  86.5 24.7 %all_to_all.38 = bf16[32,2,1472]{2,1,0:T(2,128)(2,1)S(1)} all-to-all(bf16[32,2,1472]{2,1,0:T(2,128)(2,1)S(1)} %reshape.295), channel_id=1, replica_groups=mesh['kv'=16,'tp'=32] {'tp'}, dimensions={0} | all-to-all | bytes 376832 | tf_op jit(solution)/shard_map/all_to_all | solution.py:37
  111.2 0.2 convert_reduce_fusion.2
  111.3 0.2 fusion.44
  111.5 0.1 fusion.11
  111.6 0.1 broadcast_in_dim.24
  111.7 0.0 copy-start.4
  111.7 18.8 %all_to_all.39 = bf16[32,2,704]{2,1,0:T(2,128)(2,1)S(1)} all-to-all(bf16[32,2,704]{2,1,0:T(2,128)(2,1)S(1)} %broadcast_in_dim.24), channel_id=1, replica_groups=mesh['kv'=16,'tp'=32] {'tp'}, dimensions={0} | all-to-all | bytes 180224 | tf_op jit(solution)/shard_map/all_to_all | solution.py:15
  130.5 0.1 reshape.296
  130.6 0.0 copy-done.4
  130.6 0.8 convolution_convert_fusion.6
  131.4 3.5 %all-to-all-start.6 = ((bf16[16,4,128]{2,1,0:T(4,128)(2,1)}), bf16[16,4,128]{2,1,0:T(4,128)(2,1)S(1)}, u32[]{:S(2)}, u32[]{:S(2)}) async-start(bf16[16,4,128]{2,1,0:T(4,128)(2,1)} %bitcast.18), calls=%async_computation.6 | async-start | bytes 32768 | tf_op jit(solution)/shard_map/all_to_all | solution.py:37
  134.9 6.4 %all-to-all-done.6 = bf16[16,4,128]{2,1,0:T(4,128)(2,1)S(1)} async-done(((bf16[16,4,128]{2,1,0:T(4,128)(2,1)}), bf16[16,4,128]{2,1,0:T(4,128)(2,1)S(1)}, u32[]{:S(2)}, u32[]{:S(2)}) %all-to-all-start.6) | async-done | bytes 16416 | tf_op jit(solution)/shard_map/all_to_all | solution.py:37
  141.3 0.6 add_convert_fusion
  (23 shorter events, 0.2 us)
Async XLA Ops:
  0.0 55.3 %copy-start = (f32[2,1,256,512]{3,2,1,0:T(8,128)S(1)}, f32[2,1,256,512]{3,2,1,0:T(8,128)}, u32[]{:S(2)}) copy-start(f32[2,1,256,512]{3,2,1,0:T(8,128)} %param.24) | copy-start | bytes 3145732
  0.0 14.9 %copy-start.9 = (bf16[128,256]{1,0:T(8,128)(2,1)S(1)}, bf16[128,256]{1,0:T(8,128)(2,1)}, u32[]{:S(2)}) copy-start(bf16[128,256]{1,0:T(8,128)(2,1)} %param.19) | copy-start | bytes 196612
  0.8 14.1 %copy-start.11 = (f32[128]{0:T(128)S(1)}, f32[128]{0:T(128)}, u32[]{:S(2)}) copy-start(f32[128]{0:T(128)} %param.18) | copy-start | bytes 1540
  14.7 0.8 copy-start.10
  14.8 0.9 copy-start.6
  15.7 0.9 copy-start.7
  17.6 17.5 %copy-start.14 = (s32[2]{0:T(128)S(1)}, s32[2]{0:T(128)}, u32[]{:S(2)}) copy-start(s32[2]{0:T(128)} %param.27) | copy-start | bytes 28
  17.6 37.1 %all-to-all-start.1 = ((bf16[32,2,1664]{2,1,0:T(2,128)(2,1)}), bf16[32,2,1664]{2,1,0:T(2,128)(2,1)S(1)}, u32[]{:S(2)}, u32[]{:S(2)}) async-start(bf16[32,2,1664]{2,1,0:T(2,128)(2,1)} %reshape.286), calls=%async_computation.1 | async-start | bytes 425984 | tf_op jit(solution)/shard_map/all_to_all | solution.py:37
  35.7 19.4 %copy-start.5 = (bf16[2,1,128,256]{3,2,1,0:T(8,128)(2,1)S(1)}, bf16[2,1,128,256]{3,2,1,0:T(8,128)(2,1)}, u32[]{:S(2)}) copy-start(bf16[2,1,128,256]{3,2,1,0:T(8,128)(2,1)} %param.25) | copy-start | bytes 393220
  55.3 1.0 copy-start.1
  56.3 0.7 copy-start.13
  57.1 17.2 %copy-start.8 = (bf16[512,128]{1,0:T(8,128)(2,1)S(1)}, bf16[512,128]{1,0:T(8,128)(2,1)}, u32[]{:S(2)}) copy-start(bf16[512,128]{1,0:T(8,128)(2,1)} %param.29) | copy-start | bytes 393220
  84.8 0.9 copy-start.2
  84.8 0.9 copy-start.12
  84.8 1.1 copy-start.3
  111.7 18.9 %copy-start.4 = (bf16[704,128]{1,0:T(8,128)(2,1)S(1)}, bf16[704,128]{1,0:T(8,128)(2,1)}, u32[]{:S(2)}) copy-start(bf16[704,128]{1,0:T(8,128)(2,1)} %param.33) | copy-start | bytes 540676
  131.4 9.9 %all-to-all-start.6 = ((bf16[16,4,128]{2,1,0:T(4,128)(2,1)}), bf16[16,4,128]{2,1,0:T(4,128)(2,1)S(1)}, u32[]{:S(2)}, u32[]{:S(2)}) async-start(bf16[16,4,128]{2,1,0:T(4,128)(2,1)} %bitcast.18), calls=%async_computation.6 | async-start | bytes 32768 | tf_op jit(solution)/shard_map/all_to_all | solution.py:37

commit v2 on v1

v2 whole, which is shorter than its diff:
```python
import jax
import jax.numpy as jnp
from jax import lax
from jax.sharding import Mesh
from jax.sharding import PartitionSpec as P

D = 4096
LANES = 128


epsilon = 1e-06


def exchange(parts, axes):
    return lax.all_to_all(parts, axes, split_axis=0, concat_axis=0, tiled=True)


def copies(value, count):
    return jnp.broadcast_to(value, (count, *value.shape))


def from_partner(value):
    return lax.ppermute(value, "core", [(0, 1), (1, 0)])


def wide_dot(left, right):
    return jnp.dot(left, right, preferred_element_type=jnp.float32)


def as_column(value, width):
    return jnp.pad(value, ((0, 0), (0, width - 1))).astype(jnp.bfloat16)


def thirds(value):
    high = lax.reduce_precision(value, 8, 7)
    rest = value - high
    middle = lax.reduce_precision(rest, 8, 7)
    return [part.astype(jnp.bfloat16) for part in (high, middle, rest - middle)]


def rotate(vectors, position):
    half_dim = vectors.shape[-1] // 2
    inverse = 10000.0 ** (-jnp.arange(half_dim, dtype=jnp.float32) / half_dim)
    angles = position.astype(jnp.float32)[:, None, None] * inverse
    cosine_part = jnp.cos(angles)
    sine_part = jnp.sin(angles)
    front_half = vectors[..., :half_dim]
    back_half = vectors[..., half_dim:]
    return jnp.concatenate(
        [
            front_half * cosine_part - back_half * sine_part,
            front_half * sine_part + back_half * cosine_part,
        ],
        axis=-1,
    )


def retain(
    queries,
    keys_new,
    values_new,
    gates,
    decay_rate,
    prior_state,
    key_block,
    value_block,
    lengths,
    group_gain,
):
    batch_rows = queries.shape[0]
    heads_here = decay_rate.shape[0]
    key_width = prior_state.shape[2]
    value_width = prior_state.shape[3]
    block_len = key_block.shape[2]
    rotated = rotate(
        queries.astype(jnp.float32).reshape(batch_rows, heads_here, key_width), lengths
    ).astype(jnp.bfloat16)
    fresh_keys = rotate(
        keys_new.astype(jnp.float32).reshape(batch_rows, heads_here, key_width), lengths
    ) * key_width ** (-0.5)
    fresh_values = values_new.astype(jnp.float32).reshape(batch_rows, heads_here, value_width)
    filled = lengths % block_len
    slots = jnp.arange(block_len, dtype=jnp.int32)
    distance = (filled[:, None] - slots[None, :]).astype(jnp.float32)
    live_slots = (slots[None, :] < filled[:, None])[:, None, :]
    weighting = jnp.where(
        live_slots, jnp.exp(-decay_rate[None, :, None] * distance[:, None, :]), jnp.float32(0.0)
    )
    scores = jnp.einsum("shk,shjk->shj", rotated, key_block, preferred_element_type=jnp.float32)
    block_weights = (scores * weighting).astype(jnp.bfloat16)
    block_term = jnp.einsum(
        "shj,shjv->shv", block_weights, value_block, preferred_element_type=jnp.float32
    )
    rotated_wide = rotated.astype(jnp.float32)
    own_term = jnp.sum(rotated_wide * fresh_keys, axis=-1, keepdims=True) * fresh_values
    carried = jnp.exp(-decay_rate[None, :, None] * (filled[:, None, None] + 1).astype(jnp.float32))
    state_term = carried * jnp.einsum(
        "shk,shkv->shv", rotated_wide, prior_state, precision=lax.Precision.HIGHEST
    )
    retained = own_term + block_term + state_term
    centre = jnp.mean(retained, axis=-1, keepdims=True)
    spread = jnp.mean(jnp.square(retained - centre), axis=-1, keepdims=True)
    normed = (retained - centre) * lax.rsqrt(spread + epsilon)
    gated = (
        jax.nn.silu(gates.astype(jnp.float32)).reshape(batch_rows, heads_here, value_width)
        * normed
        * group_gain.reshape(heads_here, value_width)
    )
    return gated.astype(jnp.bfloat16).reshape(batch_rows, heads_here * value_width)


def local(
    hidden_in,
    mixer_gain,
    query_weight,
    key_weight,
    value_weight,
    gate_weight,
    decay_rate,
    prior_state,
    key_block,
    value_block,
    lengths,
    group_gain,
    output_weight,
    channel_gain,
    hidden_gate,
    hidden_up,
    hidden_down,
):
    kv, z = lax.axis_size("kv"), lax.axis_size("z")
    core = lax.axis_index("core")
    own_rows, features = hidden_in.shape
    half = own_rows // 2
    rows = kv * half
    key_width, value_width = query_weight.shape[1], value_weight.shape[1]
    head_width, units = output_weight.shape[0], hidden_gate.shape[1]
    pad = -units % LANES

    def own_and_partner(pair):
        swapped = core == 1
        return (
            jnp.where(swapped, pair[1], pair[0]),
            jnp.where(swapped, pair[0], pair[1]),
        )

    with jax.named_scope("rows"):
        scaled = (hidden_in.astype(jnp.float32) * mixer_gain).astype(jnp.bfloat16)
        by_core = jnp.concatenate(
            [hidden_in.reshape(2, half, features), scaled.reshape(2, half, features)], axis=1
        )
        sent = jnp.broadcast_to(by_core[:, None], (2, kv, 2 * half, features))
        arrived = exchange(sent.reshape(2 * kv, 2 * half, features), ("core", "kv"))
        arrived = arrived.reshape(2, kv, 2 * half, features)
    with jax.named_scope("swap_first"):
        first_own = jnp.concatenate([query_weight, key_weight, value_weight, gate_weight], axis=1)
        first_partner = from_partner(first_own)
    with jax.named_scope("swap_second"):
        second_partner = from_partner(
            jnp.concatenate(
                [
                    output_weight,
                    hidden_gate.T,
                    hidden_up.T,
                    hidden_down,
                    jnp.pad(jnp.stack(thirds(channel_gain)), ((0, 13), (0, 0))),
                ],
                axis=0,
            )
        )
        at = head_width + 3 * units
        partner_output = second_partner[:head_width]
        partner_gate = second_partner[head_width : head_width + units]
        partner_up = second_partner[head_width + units : head_width + 2 * units]
        partner_down = second_partner[head_width + 2 * units : at]
        partner_gain = jnp.sum(second_partner[at : at + 3].astype(jnp.float32), axis=0)

    with jax.named_scope("project"):
        stream = own_and_partner(
            arrived[:, :, :half].reshape(2, rows, features).astype(jnp.float32)
        )
        scaled_in = own_and_partner(arrived[:, :, half:].reshape(2, rows, features))
        squares = sum(jnp.sum(part * part, axis=1, keepdims=True) for part in stream)
        terms = wide_dot(scaled_in[0], first_own) + wide_dot(scaled_in[1], first_partner)
        terms = jnp.concatenate([terms.astype(jnp.bfloat16), as_column(squares, LANES)], axis=1)
        arrived = exchange(terms.reshape(z, half, -1), "z")
        summed = jnp.sum(arrived.astype(jnp.float32), axis=0)
    with jax.named_scope("retain"):
        ends = [key_width, 2 * key_width, 2 * key_width + value_width]
        ends.append(ends[-1] + value_width)
        *projected, row_squares = jnp.split(summed, ends, axis=1)
        first_scale = lax.rsqrt(row_squares[:, :1] / D + epsilon)
        projected = [(first_scale * part).astype(jnp.bfloat16) for part in projected]
        mixed = retain(
            *projected,
            decay_rate,
            prior_state,
            key_block,
            value_block,
            lengths,
            group_gain,
        )
    with jax.named_scope("mix"):
        all_mixed = exchange(copies(mixed, z), "z").reshape(rows, head_width)
        head_terms = jnp.concatenate(
            [wide_dot(all_mixed, output_weight), wide_dot(all_mixed, partner_output)], axis=1
        ).astype(jnp.bfloat16)
        head_parts = exchange(copies(head_terms, kv), "kv")
        mixer_out = jnp.sum(head_parts.astype(jnp.float32), axis=0)
    with jax.named_scope("channel"):
        middle = [
            part + out for part, out in zip(stream, jnp.split(mixer_out, 2, axis=1))
        ]
        scaled_own = (middle[0] * channel_gain).astype(jnp.bfloat16)
        scaled_partner = (middle[1] * partner_gain).astype(jnp.bfloat16)
        middle_squares = sum(jnp.sum(part * part, axis=1, keepdims=True) for part in middle)
        gate_terms = wide_dot(scaled_own, hidden_gate) + wide_dot(scaled_partner, partner_gate.T)
        up_terms = wide_dot(scaled_own, hidden_up) + wide_dot(scaled_partner, partner_up.T)
        channel_terms = jnp.concatenate(
            [
                gate_terms.astype(jnp.bfloat16),
                as_column(middle_squares, pad),
                up_terms.astype(jnp.bfloat16),
            ],
            axis=1,
        )
        arrived = exchange(channel_terms.reshape(z, half, -1), "z")
        channel_summed = jnp.sum(arrived.astype(jnp.float32), axis=0)
        second_scale = lax.rsqrt(channel_summed[:, units : units + 1] / D + epsilon)
        gate_part = second_scale * channel_summed[:, :units]
        up_part = second_scale * channel_summed[:, units + pad :]
        activated = (jax.nn.silu(gate_part) * up_part).astype(jnp.bfloat16)
    with jax.named_scope("finish"):
        all_activated = exchange(copies(activated, z), "z").reshape(rows, units)
        here = (jnp.arange(rows) // half == lax.axis_index("kv"))[:, None]
        unit_terms = [
            wide_dot(all_activated, matrix) + jnp.where(here, part, 0.0)
            for matrix, part in zip((hidden_down, partner_down), middle)
        ]
        sent = jnp.stack(own_and_partner(unit_terms)).reshape(2 * kv, half, features)
        arrived = exchange(sent, ("core", "kv")).reshape(2, kv, half, features)
        return jnp.sum(arrived, axis=1).reshape(own_rows, features).astype(jnp.bfloat16)


def solution(mesh):
    kv, tp = mesh.shape["kv"], mesh.shape["tp"]
    chips = Mesh(mesh.devices.reshape(kv, tp // 2, 2), ("kv", "z", "core"))
    tp = ("z", "core")
    in_specs = (
        P("kv", tp),
        P(tp),
        P(tp, "kv"),
        P(tp, "kv"),
        P(tp, "kv"),
        P(tp, "kv"),
        P("kv"),
        P(tp, "kv", None, None),
        P(tp, "kv", None, None),
        P(tp, "kv", None, None),
        P(tp),
        P("kv"),
        P("kv", tp),
        P(tp),
        P(tp, "kv"),
        P(tp, "kv"),
        P("kv", tp),
    )
    return jax.shard_map(
        local, mesh=chips, in_specs=in_specs, out_specs=P("kv", tp), check_vma=False
    )
```

time: 143 us -> 129 us (0.902)
  blocking collectives: 84.9 us -> 46.4 us
  starting transfers between devices: 21 us -> 39 us
  waiting for transfers between devices: 25.2 us -> 28.1 us
  local copies, waits for them, and re-layouts: 4.79 us -> 7.21 us
  other arithmetic: 2.5 us -> 3.96 us
    all_to_all x5 -> x3, blocking collectives: 84.9 us -> 46.4 us  [exchange(): return lax.all_to_all(parts, axes, split_axis=0, concat_axis=0, tiled=True)]
    all_to_all x2 -> x4, starting transfers between devices: 21 us -> 33.8 us  [exchange(): return lax.all_to_all(parts, axes, split_axis=0, concat_axis=0, tiled=True)]
    ppermute x0 -> x2, starting transfers between devices: none -> 5.25 us  [from_partner(): return lax.ppermute(value, 'core', [(0, 1), (1, 0)])]
    all_to_all x2 -> x4, waiting for transfers between devices: 25.2 us -> 28.1 us  [exchange(): return lax.all_to_all(parts, axes, split_axis=0, concat_axis=0, tiled=True)]
    unnamed x30 -> x35, local copies, waits for them, and re-layouts: 2.66 us -> 4.12 us
  transfers between devices with their start and end apart: 2 -> 6, of which waited for: 2 -> 4; matrix products, arithmetic and copies ran while one was open for 0% -> 2% of each run, Pallas kernels for 0% -> 0%
where the time goes in v2:
time: 129 us; the launch traced here: 128 us
  blocking collectives  46.4 us (36%)
  starting transfers between devices  39 us (30%)
  waiting for transfers between devices  28.1 us (22%)
  local copies, waits for them, and re-layouts  7.21 us (6%)
  other arithmetic  3.96 us (3%)
  matrix products  2.4 us (2%)
    all_to_all x3, blocking collectives, exchange(): return lax.all_to_all(parts, axes, split_axis=0, concat_axis=0, tiled=True)  46.4 us
    all_to_all x4, starting transfers between devices, exchange(): return lax.all_to_all(parts, axes, split_axis=0, concat_axis=0, tiled=True)  33.8 us
    all_to_all x4, waiting for transfers between devices, exchange(): return lax.all_to_all(parts, axes, split_axis=0, concat_axis=0, tiled=True)  28.1 us
    ppermute x2, starting transfers between devices, from_partner(): return lax.ppermute(value, 'core', [(0, 1), (1, 0)])  5.25 us
    unnamed x35, local copies, waits for them, and re-layouts  4.12 us
  transfers between devices with their start and end apart: 6, of which 4 were waited for; matrix products, arithmetic and copies ran while one was open for 2% of the time, Pallas kernels for 0%

profile of v2, /device:TPU:1, one launch (start us, length us, event | category | flops | bytes accessed | tf_op | source)
XLA Modules:
  0.0 128.1 jit_solution(12801317835496346997)
XLA Ops:
  0.0 0.8 multiply_convert_fusion.7
  0.8 0.7 pad_maximum_fusion.2
  1.5 0.6 broadcast_in_dim.24
  2.1 10.6 %all-to-all-start = ((bf16[32,4,128]{2,1,0:T(4,128)(2,1)}), bf16[32,4,128]{2,1,0:T(4,128)(2,1)S(1)}, u32[]{:S(2)}, u32[]{:S(2)}) async-start(bf16[32,4,128]{2,1,0:T(4,128)(2,1)} %bitcast.2), calls=%async_computation | async-start | bytes 65536 | tf_op jit(solution)/shard_map/rows/all_to_all | solution.py:15
  12.7 0.0 copy-start.6
  12.7 0.9 copy-done.6
  13.6 0.9 copy-done.7
  14.5 0.0 copy-start.2
  14.5 2.3 %collective-permute-start = (bf16[128,1536]{1,0:T(8,128)(2,1)S(1)}, bf16[128,1536]{1,0:T(8,128)(2,1)S(1)}, u32[]{:S(2)}, u32[]{:S(2)}) collective-permute-start(bf16[128,1536]{1,0:T(8,128)(2,1)S(1)} %constant_dynamic-update-slice_fusion), channel_id=1, source_target_pairs={{0,1},{1,0},{2,3},{3,2},{4,5},{5,4},{6,7},{7,6},{8,9},{9,8},{10,11... | collective-permute-start | bytes 1179656 | tf_op jit(solution)/shard_map/swap_first/ppermute | solution.py:23
  16.8 0.0 copy-done.4
  16.9 0.0 copy-done.2
  16.9 0.0 copy-start.1
  16.9 0.9 copy-done.1
  17.8 0.9 copy-done.3
  18.8 0.9 all-to-all-done
  19.7 0.1 multiply_reduce_fusion.2
  19.8 0.1 copy.26
  20.0 0.2 fusion.70
  20.1 0.0 collective-permute-done
  20.1 0.2 fusion
  20.4 0.7 reshape.367
  21.0 13.2 %all-to-all-start.1 = ((bf16[16,2,1664]{2,1,0:T(2,128)(2,1)}), bf16[16,2,1664]{2,1,0:T(2,128)(2,1)S(1)}, u32[]{:S(2)}, u32[]{:S(2)}) async-start(bf16[16,2,1664]{2,1,0:T(2,128)(2,1)} %reshape.367), calls=%async_computation.1 | async-start | bytes 212992 | tf_op jit(solution)/shard_map/project/all_to_all | solution.py:15
  34.2 0.0 copy-start.8
  34.3 3.0 %collective-permute-start.1 = (bf16[2640,128]{1,0:T(8,128)(2,1)S(1)}, bf16[2640,128]{1,0:T(8,128)(2,1)S(1)}, u32[]{:S(2)}, u32[]{:S(2)}) collective-permute-start(bf16[2640,128]{1,0:T(8,128)(2,1)S(1)} %constant_dynamic-update-slice_fusion.4), channel_id=1, source_target_pairs={{0,1},{1,0},{2,3},{3,2},{4,5},{5,4},{6,7},{7,6},{8,9},{9,8},{10,11... | collective-permute-start | bytes 2027528 | tf_op jit(solution)/shard_map/swap_second/ppermute | solution.py:23
  38.0 8.1 %all-to-all-done.1 = bf16[16,2,1664]{2,1,0:T(2,128)(2,1)S(1)} async-done(((bf16[16,2,1664]{2,1,0:T(2,128)(2,1)}), bf16[16,2,1664]{2,1,0:T(2,128)(2,1)S(1)}, u32[]{:S(2)}, u32[]{:S(2)}) %all-to-all-start.1) | async-done | bytes 106528 | tf_op jit(solution)/shard_map/project/all_to_all | solution.py:15
  46.1 0.1 convert_reduce_fusion.1
  46.2 0.1 fusion.55
  46.3 0.1 bitcast_convert_fusion
  46.4 0.1 fusion.46
  46.5 0.1 fusion.12
  46.7 0.5 fusion.3
  47.1 0.1 fusion.33
  47.3 0.1 fusion.65
  47.3 0.3 copy-done.5
  47.6 0.1 fusion.5
  47.8 0.2 fusion.66
  48.0 0.2 multiply_reduce_fusion.4
  48.2 0.1 copy-done.12
  48.3 0.1 multiply_convert_fusion.2
  48.4 16.3 %all_to_all.35 = bf16[16,2,512]{2,1,0:T(2,128)(2,1)S(1)} all-to-all(bf16[16,2,512]{2,1,0:T(2,128)(2,1)S(1)} %broadcast_in_dim.26), channel_id=1, replica_groups=mesh['kv'=16,'z'=16,'core'=2] {'z'}, dimensions={0} | all-to-all | bytes 65536 | tf_op jit(solution)/shard_map/mix/all_to_all | solution.py:15
  64.8 0.1 convolution_convert_fusion.1
  64.9 0.0 collective-permute-done.1
  64.9 0.1 convolution_convert_fusion
  65.1 0.7 broadcast_in_dim.27
  65.8 6.5 %all-to-all-start.3 = ((bf16[16,32,256]{2,1,0:T(8,128)(2,1)}), bf16[16,32,256]{2,1,0:T(8,128)(2,1)S(1)}, u32[]{:S(2)}, u32[]{:S(2)}) async-start(bf16[16,32,256]{2,1,0:T(8,128)(2,1)} %broadcast_in_dim.27), calls=%async_computation.3 | async-start | bytes 524288 | tf_op jit(solution)/shard_map/mix/all_to_all | solution.py:15
  72.3 7.5 %all-to-all-done.3 = bf16[16,32,256]{2,1,0:T(8,128)(2,1)S(1)} async-done(((bf16[16,32,256]{2,1,0:T(8,128)(2,1)}), bf16[16,32,256]{2,1,0:T(8,128)(2,1)S(1)}, u32[]{:S(2)}, u32[]{:S(2)}) %all-to-all-start.3) | async-done | bytes 262176 | tf_op jit(solution)/shard_map/mix/all_to_all | solution.py:15
  79.9 0.1 multiply_reduce_fusion
  80.0 0.2 fusion.28
  80.2 0.2 fusion.29
  80.4 0.1 copy.27
  80.5 0.2 fusion.2
  80.7 0.2 fusion.1
  80.9 0.1 concatenate.62
  81.0 14.3 %all_to_all.36 = bf16[16,2,1472]{2,1,0:T(2,128)(2,1)S(1)} all-to-all(bf16[16,2,1472]{2,1,0:T(2,128)(2,1)S(1)} %reshape.376), channel_id=1, replica_groups=mesh['kv'=16,'z'=16,'core'=2] {'z'}, dimensions={0} | all-to-all | bytes 188416 | tf_op jit(solution)/shard_map/channel/all_to_all | solution.py:15
  95.3 0.1 convert_reduce_fusion.2
  95.4 0.2 fusion.56
  95.6 0.1 fusion.19
  95.7 0.6 broadcast_in_dim.28
  96.4 3.5 %all-to-all-start.5 = ((bf16[16,2,704]{2,1,0:T(2,128)(2,1)}), bf16[16,2,704]{2,1,0:T(2,128)(2,1)S(1)}, u32[]{:S(2)}, u32[]{:S(2)}) async-start(bf16[16,2,704]{2,1,0:T(2,128)(2,1)} %broadcast_in_dim.28), calls=%async_computation.5 | async-start | bytes 98304 | tf_op jit(solution)/shard_map/finish/all_to_all | solution.py:15
  99.9 11.5 %all-to-all-done.5 = bf16[16,2,704]{2,1,0:T(2,128)(2,1)S(1)} async-done(((bf16[16,2,704]{2,1,0:T(2,128)(2,1)}), bf16[16,2,704]{2,1,0:T(2,128)(2,1)S(1)}, u32[]{:S(2)}, u32[]{:S(2)}) %all-to-all-start.5) | async-done | bytes 45088 | tf_op jit(solution)/shard_map/finish/all_to_all | solution.py:15
  111.5 0.2 convolution_add_fusion.3
  111.6 0.2 select_bitcast_fusion.1
  111.8 15.7 %all_to_all.37 = f32[32,2,128]{2,1,0:T(2,128)S(1)} all-to-all(f32[32,2,128]{2,1,0:T(2,128)S(1)} %bitcast.82), channel_id=1, replica_groups=mesh['kv'=16,'z'=16,'core'=2] {'core','kv'}, dimensions={0} | all-to-all | bytes 65536 | tf_op jit(solution)/shard_map/finish/all_to_all | solution.py:15
  127.5 0.6 bitcast_reduce_fusion
  (48 shorter events, 0.5 us)
Async XLA Ops:
  0.0 46.7 %copy-start = (f32[2,1,256,512]{3,2,1,0:T(8,128)S(1)}, f32[2,1,256,512]{3,2,1,0:T(8,128)}, u32[]{:S(2)}) copy-start(f32[2,1,256,512]{3,2,1,0:T(8,128)} %param.24) | copy-start | bytes 3145732
  0.0 12.7 %copy-start.9 = (bf16[128,256]{1,0:T(8,128)(2,1)S(1)}, bf16[128,256]{1,0:T(8,128)(2,1)}, u32[]{:S(2)}) copy-start(bf16[128,256]{1,0:T(8,128)(2,1)} %param.19) | copy-start | bytes 196612
  2.1 10.6 %copy-start.10 = (bf16[128,256]{1,0:T(8,128)(2,1)S(1)}, bf16[128,256]{1,0:T(8,128)(2,1)}, u32[]{:S(2)}) copy-start(bf16[128,256]{1,0:T(8,128)(2,1)} %param.20) | copy-start | bytes 196612
  2.1 17.6 %all-to-all-start = ((bf16[32,4,128]{2,1,0:T(4,128)(2,1)}), bf16[32,4,128]{2,1,0:T(4,128)(2,1)S(1)}, u32[]{:S(2)}, u32[]{:S(2)}) async-start(bf16[32,4,128]{2,1,0:T(4,128)(2,1)} %bitcast.2), calls=%async_computation | async-start | bytes 65536 | tf_op jit(solution)/shard_map/rows/all_to_all | solution.py:15
  12.7 0.9 copy-start.6
  13.6 0.9 copy-start.7
  14.5 2.3 %copy-start.11 = (f32[128]{0:T(128)S(1)}, f32[128]{0:T(128)}, u32[]{:S(2)}) copy-start(f32[128]{0:T(128)} %param.30) | copy-start | bytes 1540
  14.5 2.3 %copy-start.4 = (bf16[512,128]{1,0:T(8,128)(2,1)S(1)}, bf16[512,128]{1,0:T(8,128)(2,1)}, u32[]{:S(2)}) copy-start(bf16[512,128]{1,0:T(8,128)(2,1)} %param.29) | copy-start | bytes 393220
  14.5 2.4 %copy-start.2 = (bf16[128,704]{0,1:T(8,128)(2,1)S(1)}, bf16[128,704]{0,1:T(8,128)(2,1)}, u32[]{:S(2)}) copy-start(bf16[128,704]{0,1:T(8,128)(2,1)} %param.31) | copy-start | bytes 540676
  14.5 5.6 %collective-permute-start = (bf16[128,1536]{1,0:T(8,128)(2,1)S(1)}, bf16[128,1536]{1,0:T(8,128)(2,1)S(1)}, u32[]{:S(2)}, u32[]{:S(2)}) collective-permute-start(bf16[128,1536]{1,0:T(8,128)(2,1)S(1)} %constant_dynamic-update-slice_fusion), channel_id=1, source_target_pairs={{0,1},{1,0},{2,3},{3,2},{4,5},{5,4},{6,7},{7,6},{8,9},{9,8},{10,11... | collective-permute-start | bytes 1179656 | tf_op jit(solution)/shard_map/swap_first/ppermute | solution.py:23
  16.9 0.9 copy-start.1
  17.8 0.9 copy-start.3
  21.0 16.2 %copy-start.13 = (s32[2]{0:T(128)S(1)}, s32[2]{0:T(128)}, u32[]{:S(2)}) copy-start(s32[2]{0:T(128)} %param.27) | copy-start | bytes 28
  21.0 25.1 %all-to-all-start.1 = ((bf16[16,2,1664]{2,1,0:T(2,128)(2,1)}), bf16[16,2,1664]{2,1,0:T(2,128)(2,1)S(1)}, u32[]{:S(2)}, u32[]{:S(2)}) async-start(bf16[16,2,1664]{2,1,0:T(2,128)(2,1)} %reshape.367), calls=%async_computation.1 | async-start | bytes 212992 | tf_op jit(solution)/shard_map/project/all_to_all | solution.py:15
  34.2 12.3 %copy-start.8 = (bf16[2,1,128,256]{3,2,1,0:T(8,128)(2,1)S(1)}, bf16[2,1,128,256]{3,2,1,0:T(8,128)(2,1)}, u32[]{:S(2)}) copy-start(bf16[2,1,128,256]{3,2,1,0:T(8,128)(2,1)} %param.25) | copy-start | bytes 393220
  34.3 30.6 %collective-permute-start.1 = (bf16[2640,128]{1,0:T(8,128)(2,1)S(1)}, bf16[2640,128]{1,0:T(8,128)(2,1)S(1)}, u32[]{:S(2)}, u32[]{:S(2)}) collective-permute-start(bf16[2640,128]{1,0:T(8,128)(2,1)S(1)} %constant_dynamic-update-slice_fusion.4), channel_id=1, source_target_pairs={{0,1},{1,0},{2,3},{3,2},{4,5},{5,4},{6,7},{7,6},{8,9},{9,8},{10,11... | collective-permute-start | bytes 2027528 | tf_op jit(solution)/shard_map/swap_second/ppermute | solution.py:23
  46.7 1.0 copy-start.5
  47.6 0.7 copy-start.12
  65.8 14.0 %all-to-all-start.3 = ((bf16[16,32,256]{2,1,0:T(8,128)(2,1)}), bf16[16,32,256]{2,1,0:T(8,128)(2,1)S(1)}, u32[]{:S(2)}, u32[]{:S(2)}) async-start(bf16[16,32,256]{2,1,0:T(8,128)(2,1)} %broadcast_in_dim.27), calls=%async_computation.3 | async-start | bytes 524288 | tf_op jit(solution)/shard_map/mix/all_to_all | solution.py:15
  96.4 15.1 %all-to-all-start.5 = ((bf16[16,2,704]{2,1,0:T(2,128)(2,1)}), bf16[16,2,704]{2,1,0:T(2,128)(2,1)S(1)}, u32[]{:S(2)}, u32[]{:S(2)}) async-start(bf16[16,2,704]{2,1,0:T(2,128)(2,1)} %broadcast_in_dim.28), calls=%async_computation.5 | async-start | bytes 98304 | tf_op jit(solution)/shard_map/finish/all_to_all | solution.py:15

commit v3 on v2

--- a/solution.py
+++ b/solution.py
@@ -1,6 +1,10 @@
+import functools
+
 import jax
 import jax.numpy as jnp
 from jax import lax
+from jax.experimental import pallas as pl
+from jax.experimental.pallas import tpu as pltpu
 from jax.sharding import Mesh
 from jax.sharding import PartitionSpec as P
 
@@ -31,11 +35,155 @@
     return jnp.pad(value, ((0, 0), (0, width - 1))).astype(jnp.bfloat16)
 
 
+IN_VMEM = pl.BlockSpec(memory_space=pltpu.VMEM)
+IN_HBM = pl.BlockSpec(memory_space=pltpu.HBM)
+GAIN_ROWS = 16
+
+
 def thirds(value):
-    high = lax.reduce_precision(value, 8, 7)
-    rest = value - high
-    middle = lax.reduce_precision(rest, 8, 7)
-    return [part.astype(jnp.bfloat16) for part in (high, middle, rest - middle)]
+    high = value.astype(jnp.bfloat16)
+    rest = value - high.astype(jnp.float32)
+    middle = rest.astype(jnp.bfloat16)
+    return high, middle, (rest - middle.astype(jnp.float32)).astype(jnp.bfloat16)
+
+
+def gain_block(gain, width):
+    row = lax.broadcasted_iota(jnp.int32, (GAIN_ROWS, width), 0)
+    high, middle, low = (part.astype(jnp.float32) for part in thirds(gain))
+    block = jnp.where(row == 0, high, jnp.where(row == 1, middle, jnp.where(row == 2, low, 0.0)))
+    return block.astype(jnp.bfloat16)
+
+
+def from_thirds(block):
+    wide = block.astype(jnp.float32)
+    return wide[0:1] + wide[1:2] + wide[2:3]
+
+
+def join_kernel(places, *refs):
+    *sources, gain, out, arrived = refs
+    moves = [
+        pltpu.make_async_copy(source, out.at[place], arrived.at[i])
+        for i, (source, place) in enumerate(zip(sources, places))
+    ]
+    for move in moves:
+        move.start()
+    rows = out.shape[0] - GAIN_ROWS
+    out[rows:, :LANES] = gain_block(gain[...], LANES)
+    for move in moves:
+        move.wait()
+
+
+def joined(arrays, gain, axis):
+    places, at = [], 0
+    for array in arrays:
+        span = slice(at, at + array.shape[axis])
+        at += array.shape[axis]
+        places.append((slice(0, array.shape[0]), span) if axis == 1 else (span,))
+    shape = (arrays[0].shape[0] + GAIN_ROWS, at) if axis == 1 else (at + GAIN_ROWS, LANES)
+    return pl.pallas_call(
+        functools.partial(join_kernel, places),
+        out_shape=pltpu.VMEM(shape, jnp.bfloat16),
+        in_specs=[IN_HBM] * len(arrays) + [IN_VMEM],
+        out_specs=IN_VMEM,
+        scratch_shapes=[pltpu.SemaphoreType.DMA((len(arrays),))],
+        compiler_params=pltpu.CompilerParams(vmem_limit_bytes=8 << 20),
+        cost_estimate=pl.CostEstimate(flops=2_000_000, bytes_accessed=1_000_000, transcendentals=0),
+        name="join",
+    )(*(pltpu.with_memory_space_constraint(array, pltpu.HBM) for array in arrays), gain[None])
+
+
+def transposed_dot(left, right):
+    return lax.dot_general(
+        left, right, (((1,), (1,)), ((), ())), preferred_element_type=jnp.float32
+    )
+
+
+def store_by_peer(terms, wide):
+    half = terms.shape[1]
+    for i in range(terms.shape[0]):
+        terms[i] = wide[half * i : half * (i + 1)].astype(jnp.bfloat16)
+
+
+def project_kernel(stream, own, partner, terms, wide):
+    _, rows, features = stream.shape
+    width = own.shape[1]
+    parts = [stream[i].astype(jnp.float32) for i in range(2)]
+    total = None
+    for part, weights in zip(parts, (own, partner)):
+        gain = from_thirds(weights[features : features + GAIN_ROWS, :features])
+        scaled = (part * gain).astype(jnp.bfloat16)
+        term = jnp.dot(scaled, weights[:features], preferred_element_type=jnp.float32)
+        total = term if total is None else total + term
+    wide[:, :width] = total
+    squares = jnp.sum(parts[0] * parts[0] + parts[1] * parts[1], axis=1, keepdims=True)
+    lane = lax.broadcasted_iota(jnp.int32, (rows, LANES), 1)
+    wide[:, width:] = jnp.where(lane == 0, squares, 0.0)
+    store_by_peer(terms, wide)
+
+
+def project(stream, own, partner, z):
+    rows = stream.shape[1]
+    width = own.shape[1] + LANES
+    return pl.pallas_call(
+        project_kernel,
+        out_shape=jax.ShapeDtypeStruct((z, rows // z, width), jnp.bfloat16),
+        in_specs=[IN_VMEM] * 3,
+        out_specs=IN_VMEM,
+        scratch_shapes=[pltpu.VMEM((rows, width), jnp.float32)],
+        compiler_params=pltpu.CompilerParams(vmem_limit_bytes=8 << 20),
+        cost_estimate=pl.CostEstimate(flops=8_000_000, bytes_accessed=1_000_000, transcendentals=0),
+        name="project",
+    )(stream, own, partner)
+
+
+def channel_kernel(
+    head, units, pad, parts, stream, gain, gate, up, partner, terms, residual, wide
+):
+    rows, features = stream.shape[1:]
+    half = terms.shape[1]
+    mixer_out = parts[0].astype(jnp.float32)
+    for i in range(1, parts.shape[0]):
+        mixer_out = mixer_out + parts[i].astype(jnp.float32)
+    own = stream[0].astype(jnp.float32) + mixer_out[:, :features]
+    other = stream[1].astype(jnp.float32) + mixer_out[:, features:]
+    at = head + 3 * units
+    other_gain = from_thirds(partner[at : at + GAIN_ROWS])
+    scaled_own = (own * gain[...]).astype(jnp.bfloat16)
+    scaled_other = (other * other_gain).astype(jnp.bfloat16)
+    squares = jnp.sum(own * own + other * other, axis=1, keepdims=True)
+    wide[:, :units] = transposed_dot(scaled_own, gate[...]) + transposed_dot(
+        scaled_other, partner[head : head + units]
+    )
+    lane = lax.broadcasted_iota(jnp.int32, (rows, pad), 1)
+    wide[:, units : units + pad] = jnp.where(lane == 0, squares, 0.0)
+    wide[:, units + pad :] = transposed_dot(scaled_own, up[...]) + transposed_dot(
+        scaled_other, partner[head + units : head + 2 * units]
+    )
+    store_by_peer(terms, wide)
+    row = lax.broadcasted_iota(jnp.int32, (rows, features), 0)
+    here = row // half == lax.axis_index("kv")
+    residual[0] = jnp.where(here, own, 0.0)
+    residual[1] = jnp.where(here, other, 0.0)
+
+
+def channel(parts, stream, gain, gate, up, partner, head, z):
+    units = gate.shape[0]
+    pad = -units % LANES
+    _, rows, features = stream.shape
+    width = 2 * units + pad
+    return pl.pallas_call(
+        functools.partial(channel_kernel, head, units, pad),
+        out_shape=(
+            jax.ShapeDtypeStruct((z, rows // z, width), jnp.bfloat16),
+            jax.ShapeDtypeStruct((2, rows, features), jnp.float32),
+        ),
+        in_specs=[IN_VMEM] * 6,
+        out_specs=(IN_VMEM, IN_VMEM),
+        scratch_shapes=[pltpu.VMEM((rows, width), jnp.float32)],
+        compiler_params=pltpu.CompilerParams(vmem_limit_bytes=8 << 20),
+        cost_estimate=pl.CostEstimate(flops=8_000_000, bytes_accessed=1_000_000, transcendentals=0),
+        name="channel",
+    )(parts, stream, gain[None], gate, up, partner)
 
 
 def rotate(vectors, position):
@@ -145,45 +293,22 @@
         )
 
     with jax.named_scope("rows"):
-        scaled = (hidden_in.astype(jnp.float32) * mixer_gain).astype(jnp.bfloat16)
-        by_core = jnp.concatenate(
-            [hidden_in.reshape(2, half, features), scaled.reshape(2, half, features)], axis=1
-        )
-        sent = jnp.broadcast_to(by_core[:, None], (2, kv, 2 * half, features))
-        arrived = exchange(sent.reshape(2 * kv, 2 * half, features), ("core", "kv"))
-        arrived = arrived.reshape(2, kv, 2 * half, features)
+        sent = copies(hidden_in, 2 * kv)
+        arrived = exchange(sent, ("core", "kv")).reshape(2, kv, 2, half, features)
+        mine = jnp.where(core == 1, arrived[:, :, 1], arrived[:, :, 0])
+        stream = jnp.stack(own_and_partner(mine.reshape(2, rows, features)))
     with jax.named_scope("swap_first"):
-        first_own = jnp.concatenate([query_weight, key_weight, value_weight, gate_weight], axis=1)
+        first_own = joined((query_weight, key_weight, value_weight, gate_weight), mixer_gain, 1)
         first_partner = from_partner(first_own)
     with jax.named_scope("swap_second"):
-        second_partner = from_partner(
-            jnp.concatenate(
-                [
-                    output_weight,
-                    hidden_gate.T,
-                    hidden_up.T,
-                    hidden_down,
-                    jnp.pad(jnp.stack(thirds(channel_gain)), ((0, 13), (0, 0))),
-                ],
-                axis=0,
-            )
-        )
-        at = head_width + 3 * units
+        later = (output_weight, hidden_gate.T, hidden_up.T, hidden_down)
+        later, stream = lax.optimization_barrier((later, stream))
+        second_partner = from_partner(joined(later, channel_gain, 0))
         partner_output = second_partner[:head_width]
-        partner_gate = second_partner[head_width : head_width + units]
-        partner_up = second_partner[head_width + units : head_width + 2 * units]
-        partner_down = second_partner[head_width + 2 * units : at]
-        partner_gain = jnp.sum(second_partner[at : at + 3].astype(jnp.float32), axis=0)
+        partner_down = second_partner[head_width + 2 * units : head_width + 3 * units]
 
     with jax.named_scope("project"):
-        stream = own_and_partner(
-            arrived[:, :, :half].reshape(2, rows, features).astype(jnp.float32)
-        )
-        scaled_in = own_and_partner(arrived[:, :, half:].reshape(2, rows, features))
-        squares = sum(jnp.sum(part * part, axis=1, keepdims=True) for part in stream)
-        terms = wide_dot(scaled_in[0], first_own) + wide_dot(scaled_in[1], first_partner)
-        terms = jnp.concatenate([terms.astype(jnp.bfloat16), as_column(squares, LANES)], axis=1)
-        arrived = exchange(terms.reshape(z, half, -1), "z")
+        arrived = exchange(project(stream, first_own, first_partner, z), "z")
         summed = jnp.sum(arrived.astype(jnp.float32), axis=0)
     with jax.named_scope("retain"):
         ends = [key_width, 2 * key_width, 2 * key_width + value_width]
@@ -206,25 +331,18 @@
             [wide_dot(all_mixed, output_weight), wide_dot(all_mixed, partner_output)], axis=1
         ).astype(jnp.bfloat16)
         head_parts = exchange(copies(head_terms, kv), "kv")
-        mixer_out = jnp.sum(head_parts.astype(jnp.float32), axis=0)
     with jax.named_scope("channel"):
-        middle = [
-            part + out for part, out in zip(stream, jnp.split(mixer_out, 2, axis=1))
-        ]
-        scaled_own = (middle[0] * channel_gain).astype(jnp.bfloat16)
-        scaled_partner = (middle[1] * partner_gain).astype(jnp.bfloat16)
-        middle_squares = sum(jnp.sum(part * part, axis=1, keepdims=True) for part in middle)
-        gate_terms = wide_dot(scaled_own, hidden_gate) + wide_dot(scaled_partner, partner_gate.T)
-        up_terms = wide_dot(scaled_own, hidden_up) + wide_dot(scaled_partner, partner_up.T)
-        channel_terms = jnp.concatenate(
-            [
-                gate_terms.astype(jnp.bfloat16),
-                as_column(middle_squares, pad),
-                up_terms.astype(jnp.bfloat16),
-            ],
-            axis=1,
+        channel_terms, residual = channel(
+            head_parts,
+            stream,
+            channel_gain,
+            hidden_gate.T,
+            hidden_up.T,
+            second_partner,
+            head_width,
+            z,
         )
-        arrived = exchange(channel_terms.reshape(z, half, -1), "z")
+        arrived = exchange(channel_terms, "z")
         channel_summed = jnp.sum(arrived.astype(jnp.float32), axis=0)
         second_scale = lax.rsqrt(channel_summed[:, units : units + 1] / D + epsilon)
         gate_part = second_scale * channel_summed[:, :units]
@@ -232,10 +350,9 @@
         activated = (jax.nn.silu(gate_part) * up_part).astype(jnp.bfloat16)
     with jax.named_scope("finish"):
         all_activated = exchange(copies(activated, z), "z").reshape(rows, units)
-        here = (jnp.arange(rows) // half == lax.axis_index("kv"))[:, None]
         unit_terms = [
-            wide_dot(all_activated, matrix) + jnp.where(here, part, 0.0)
-            for matrix, part in zip((hidden_down, partner_down), middle)
+            wide_dot(all_activated, matrix) + part
+            for matrix, part in zip((hidden_down, partner_down), residual)
         ]
         sent = jnp.stack(own_and_partner(unit_terms)).reshape(2 * kv, half, features)
         arrived = exchange(sent, ("core", "kv")).reshape(2, kv, half, features)

time: 129 us -> 124 us (0.961)
  blocking collectives: 46.4 us -> 74.5 us
  waiting for transfers between devices: 28.1 us -> 9.38 us
  starting transfers between devices: 39 us -> 28.8 us
  local copies, waits for them, and re-layouts: 7.21 us -> 3.32 us
  Pallas kernels: 0 us -> 3.58 us
  other arithmetic: 3.96 us -> 2.11 us
    all_to_all x3 -> x5, blocking collectives: 46.4 us -> 74.5 us  [exchange(): return lax.all_to_all(parts, axes, split_axis=0, concat_axis=0, tiled=True)]
    all_to_all x4 -> x2, waiting for transfers between devices: 28.1 us -> 9.37 us  [exchange(): return lax.all_to_all(parts, axes, split_axis=0, concat_axis=0, tiled=True)]
    all_to_all x4 -> x2, starting transfers between devices: 33.8 us -> 23.6 us  [exchange(): return lax.all_to_all(parts, axes, split_axis=0, concat_axis=0, tiled=True)]
    pallas_call x0 -> x4, Pallas kernels: none -> 3.58 us  [the longest x2 2.27 us: joined(): pl.pallas_call(functools.partial(join_kernel, places), out_shape=pltpu.VM...]
    unnamed x35 -> x22, local copies, waits for them, and re-layouts: 4.12 us -> 1.78 us
  transfers between devices with their start and end apart: 6 -> 4, of which waited for: 4 -> 2; matrix products, arithmetic and copies ran while one was open for 2% -> 2% of each run, Pallas kernels for 0% -> 2%
where the time goes in v3:
time: 124 us
  blocking collectives  74.5 us (60%)
  starting transfers between devices  28.8 us (23%)
  waiting for transfers between devices  9.38 us (8%)
  Pallas kernels  3.58 us (3%)
  local copies, waits for them, and re-layouts  3.32 us (3%)
  other arithmetic  2.11 us (2%)
  matrix products  1.31 us (1%)
    all_to_all x5, blocking collectives, exchange(): return lax.all_to_all(parts, axes, split_axis=0, concat_axis=0, tiled=True)  74.5 us
    all_to_all x2, starting transfers between devices, exchange(): return lax.all_to_all(parts, axes, split_axis=0, concat_axis=0, tiled=True)  23.6 us
    all_to_all x2, waiting for transfers between devices, exchange(): return lax.all_to_all(parts, axes, split_axis=0, concat_axis=0, tiled=True)  9.37 us
    ppermute x2, starting transfers between devices, from_partner(): return lax.ppermute(value, 'core', [(0, 1), (1, 0)])  5.12 us
  transfers between devices with their start and end apart: 4, of which 2 were waited for; matrix products, arithmetic and copies ran while one was open for 2% of the time, Pallas kernels for 2%

profile of v3, /device:TPU:1, one launch (start us, length us, event | category | flops | bytes accessed | tf_op | source)
XLA Modules:
  0.0 123.9 jit_solution(411435148927369657)
XLA Ops:
  0.0 0.0 copy-start
  0.0 1.4 %broadcast_in_dim.16 = bf16[32,4,128]{2,1,0:T(4,128)(2,1)} broadcast(bf16[4,128]{1,0:T(4,128)(2,1)} %param.17), dimensions={1,2} | broadcast | bytes 33792 | tf_op jit(solution)/shard_map/rows/broadcast_in_dim | solution.py:23
  1.4 10.4 %all-to-all-start = ((bf16[32,4,128]{2,1,0:T(4,128)(2,1)}), bf16[32,4,128]{2,1,0:T(4,128)(2,1)S(1)}, u32[]{:S(2)}, u32[]{:S(2)}) async-start(bf16[32,4,128]{2,1,0:T(4,128)(2,1)} %broadcast_in_dim.16), calls=%async_computation | async-start | bytes 65536 | tf_op jit(solution)/shard_map/rows/all_to_all | solution.py:19
  11.8 0.0 copy-start.4
  11.8 0.6 copy-done.4
  12.5 1.1 join.2.own
  13.6 2.2 %collective-permute-start = (bf16[144,1536]{1,0:T(8,128)(2,1)S(1)}, bf16[144,1536]{1,0:T(8,128)(2,1)S(1)}, u32[]{:S(2)}, u32[]{:S(2)}) collective-permute-start(bf16[144,1536]{1,0:T(8,128)(2,1)S(1)} %join.2.own), channel_id=1, source_target_pairs={{0,1},{1,0},{2,3},{3,2},{4,5},{5,4},{6,7},{7,6},{8,9},{9,8},{10,11... | collective-permute-start | bytes 1327112 | tf_op jit(solution)/shard_map/swap_first/ppermute | solution.py:27
  15.7 3.1 %all-to-all-done = bf16[32,4,128]{2,1,0:T(4,128)(2,1)S(1)} async-done(((bf16[32,4,128]{2,1,0:T(4,128)(2,1)}), bf16[32,4,128]{2,1,0:T(4,128)(2,1)S(1)}, u32[]{:S(2)}, u32[]{:S(2)}) %all-to-all-start) | async-done | bytes 32800 | tf_op jit(solution)/shard_map/rows/all_to_all | solution.py:19
  18.9 0.0 collective-permute-done.partner
  18.9 0.9 project.1
  19.8 0.0 copy-start.10
  19.8 13.2 %all-to-all-start.1 = ((bf16[16,2,1664]{2,1,0:T(2,128)(2,1)}), bf16[16,2,1664]{2,1,0:T(2,128)(2,1)S(1)}, u32[]{:S(2)}, u32[]{:S(2)}) async-start(bf16[16,2,1664]{2,1,0:T(2,128)(2,1)} %project.1), calls=%async_computation.1 | async-start | bytes 212992 | tf_op jit(solution)/shard_map/project/all_to_all | solution.py:19
  33.0 0.0 copy-done.10
  33.7 0.0 copy-start.3
  33.7 0.6 copy-done.3
  34.4 1.2 join.3
  35.6 0.0 copy-start.8
  35.6 3.0 %collective-permute-start.1 = (bf16[2640,128]{1,0:T(8,128)(2,1)S(1)}, bf16[2640,128]{1,0:T(8,128)(2,1)S(1)}, u32[]{:S(2)}, u32[]{:S(2)}) collective-permute-start(bf16[2640,128]{1,0:T(8,128)(2,1)S(1)} %join.3), channel_id=1, source_target_pairs={{0,1},{1,0},{2,3},{3,2},{4,5},{5,4},{6,7},{7,6},{8,9},{9,8},{10,11... | collective-permute-start | bytes 2027528 | tf_op jit(solution)/shard_map/swap_second/ppermute | solution.py:27
  38.6 6.3 %all-to-all-done.1 = bf16[16,2,1664]{2,1,0:T(2,128)(2,1)S(1)} async-done(((bf16[16,2,1664]{2,1,0:T(2,128)(2,1)}), bf16[16,2,1664]{2,1,0:T(2,128)(2,1)S(1)}, u32[]{:S(2)}, u32[]{:S(2)}) %all-to-all-start.1) | async-done | bytes 106528 | tf_op jit(solution)/shard_map/project/all_to_all | solution.py:19
  44.9 0.1 convert_reduce_fusion
  45.0 0.1 fusion.41
  45.1 0.1 bitcast_convert_fusion
  45.2 0.1 fusion.32
  45.3 0.0 copy-done.8
  45.3 0.1 fusion.6
  45.4 0.0 copy-done
  45.4 0.0 copy-start.7
  45.5 0.5 fusion
  45.9 0.1 fusion.19
  46.0 0.1 fusion.46
  46.1 0.3 copy-done.7
  46.4 0.0 copy-start.9
  46.4 0.1 fusion.2
  46.6 0.0 copy-start.6
  46.6 0.2 fusion.47
  46.8 0.2 multiply_reduce_fusion
  47.0 0.1 copy-done.9
  47.1 0.1 multiply_convert_fusion
  47.2 16.7 %all_to_all.35 = bf16[16,2,512]{2,1,0:T(2,128)(2,1)S(1)} all-to-all(bf16[16,2,512]{2,1,0:T(2,128)(2,1)S(1)} %broadcast_in_dim.19), channel_id=1, replica_groups=mesh['kv'=16,'z'=16,'core'=2] {'z'}, dimensions={0} | all-to-all | bytes 65536 | tf_op jit(solution)/shard_map/mix/all_to_all | solution.py:19
  64.0 0.0 copy-done.6
  64.0 0.1 convolution_convert_fusion.1
  64.1 0.0 collective-permute-done.1.partner
  64.1 0.1 convolution_convert_fusion
  64.3 0.0 copy-start.1
  64.3 0.0 copy-start.2
  64.3 12.5 %all_to_all.36.parts = bf16[16,32,256]{2,1,0:T(8,128)(2,1)S(1)} all-to-all(bf16[16,32,256]{2,1,0:T(8,128)(2,1)S(1)} %broadcast_in_dim.21), channel_id=1, replica_groups=mesh['kv'=16,'z'=16,'core'=2] {'kv'}, dimensions={0} | all-to-all | bytes 524288 | tf_op jit(solution)/shard_map/mix/all_to_all | solution.py:19
  76.9 0.0 copy-done.1
  76.9 0.0 copy-done.2
  76.9 0.4 channel.1
  77.3 14.3 %all_to_all.37 = bf16[16,2,1472]{2,1,0:T(2,128)(2,1)S(1)} all-to-all(bf16[16,2,1472]{2,1,0:T(2,128)(2,1)S(1)} %get-tuple-element.17), channel_id=1, replica_groups=mesh['kv'=16,'z'=16,'core'=2] {'z'}, dimensions={0} | all-to-all | bytes 188416 | tf_op jit(solution)/shard_map/channel/all_to_all | solution.py:19
  91.6 0.0 copy-start.5
  91.6 0.1 convert_reduce_fusion.1
  91.7 0.2 fusion.42
  91.9 0.1 fusion.9
  92.1 14.9 %all_to_all.38 = bf16[16,2,704]{2,1,0:T(2,128)(2,1)S(1)} all-to-all(bf16[16,2,704]{2,1,0:T(2,128)(2,1)S(1)} %broadcast_in_dim.22), channel_id=1, replica_groups=mesh['kv'=16,'z'=16,'core'=2] {'z'}, dimensions={0} | all-to-all | bytes 90112 | tf_op jit(solution)/shard_map/finish/all_to_all | solution.py:19
  107.0 0.0 copy-done.5
  107.0 0.1 fusion.51
  107.1 0.2 select_bitcast_fusion.1
  107.3 16.0 %all_to_all.39 = f32[32,2,128]{2,1,0:T(2,128)S(1)} all-to-all(f32[32,2,128]{2,1,0:T(2,128)S(1)} %bitcast.72), channel_id=1, replica_groups=mesh['kv'=16,'z'=16,'core'=2] {'core','kv'}, dimensions={0} | all-to-all | bytes 65536 | tf_op jit(solution)/shard_map/finish/all_to_all | solution.py:19
  123.3 0.6 bitcast_reduce_fusion
  (19 shorter events, 0.2 us)
Async XLA Ops:
  0.0 45.4 %copy-start = (f32[2,1,256,512]{3,2,1,0:T(8,128)S(1)}, f32[2,1,256,512]{3,2,1,0:T(8,128)}, u32[]{:S(2)}) copy-start(f32[2,1,256,512]{3,2,1,0:T(8,128)} %param.24) | copy-start | bytes 3145732
  1.4 17.4 %all-to-all-start = ((bf16[32,4,128]{2,1,0:T(4,128)(2,1)}), bf16[32,4,128]{2,1,0:T(4,128)(2,1)S(1)}, u32[]{:S(2)}, u32[]{:S(2)}) async-start(bf16[32,4,128]{2,1,0:T(4,128)(2,1)} %broadcast_in_dim.16), calls=%async_computation | async-start | bytes 65536 | tf_op jit(solution)/shard_map/rows/all_to_all | solution.py:19
  11.8 0.7 copy-start.4
  13.6 5.3 %collective-permute-start = (bf16[144,1536]{1,0:T(8,128)(2,1)S(1)}, bf16[144,1536]{1,0:T(8,128)(2,1)S(1)}, u32[]{:S(2)}, u32[]{:S(2)}) collective-permute-start(bf16[144,1536]{1,0:T(8,128)(2,1)S(1)} %join.2.own), channel_id=1, source_target_pairs={{0,1},{1,0},{2,3},{3,2},{4,5},{5,4},{6,7},{7,6},{8,9},{9,8},{10,11... | collective-permute-start | bytes 1327112 | tf_op jit(solution)/shard_map/swap_first/ppermute | solution.py:27
  19.8 13.2 %copy-start.10 = (s32[2]{0:T(128)S(1)}, s32[2]{0:T(128)}, u32[]{:S(2)}) copy-start(s32[2]{0:T(128)} %param.27) | copy-start | bytes 28
  19.8 25.1 %all-to-all-start.1 = ((bf16[16,2,1664]{2,1,0:T(2,128)(2,1)}), bf16[16,2,1664]{2,1,0:T(2,128)(2,1)S(1)}, u32[]{:S(2)}, u32[]{:S(2)}) async-start(bf16[16,2,1664]{2,1,0:T(2,128)(2,1)} %project.1), calls=%async_computation.1 | async-start | bytes 212992 | tf_op jit(solution)/shard_map/project/all_to_all | solution.py:19
  33.7 0.7 copy-start.3
  35.6 9.7 %copy-start.8 = (bf16[2,1,128,256]{3,2,1,0:T(8,128)(2,1)S(1)}, bf16[2,1,128,256]{3,2,1,0:T(8,128)(2,1)}, u32[]{:S(2)}) copy-start(bf16[2,1,128,256]{3,2,1,0:T(8,128)(2,1)} %param.25) | copy-start | bytes 393220
  35.6 28.5 %collective-permute-start.1 = (bf16[2640,128]{1,0:T(8,128)(2,1)S(1)}, bf16[2640,128]{1,0:T(8,128)(2,1)S(1)}, u32[]{:S(2)}, u32[]{:S(2)}) collective-permute-start(bf16[2640,128]{1,0:T(8,128)(2,1)S(1)} %join.3), channel_id=1, source_target_pairs={{0,1},{1,0},{2,3},{3,2},{4,5},{5,4},{6,7},{7,6},{8,9},{9,8},{10,11... | collective-permute-start | bytes 2027528 | tf_op jit(solution)/shard_map/swap_second/ppermute | solution.py:27
  45.4 1.0 copy-start.7
  46.4 0.7 copy-start.9
  46.6 17.4 %copy-start.6 = (bf16[512,128]{1,0:T(8,128)(2,1)S(1)}, bf16[512,128]{1,0:T(8,128)(2,1)}, u32[]{:S(2)}) copy-start(bf16[512,128]{1,0:T(8,128)(2,1)} %refs_0_.2) | copy-start | bytes 393220
  64.3 12.6 %copy-start.1 = (bf16[128,704]{0,1:T(8,128)(2,1)S(1)}, bf16[128,704]{0,1:T(8,128)(2,1)}, u32[]{:S(2)}) copy-start(bf16[128,704]{0,1:T(8,128)(2,1)} %param.31) | copy-start | bytes 540676
  64.3 12.6 %copy-start.2 = (bf16[128,704]{0,1:T(8,128)(2,1)S(1)}, bf16[128,704]{0,1:T(8,128)(2,1)}, u32[]{:S(2)}) copy-start(bf16[128,704]{0,1:T(8,128)(2,1)} %param.32) | copy-start | bytes 540676
  91.6 15.3 %copy-start.5 = (bf16[704,128]{1,0:T(8,128)(2,1)S(1)}, bf16[704,128]{1,0:T(8,128)(2,1)}, u32[]{:S(2)}) copy-start(bf16[704,128]{1,0:T(8,128)(2,1)} %refs_3_.2) | copy-start | bytes 540676

commit v4 on v3

v4 whole, which is shorter than its diff:
```python
import functools

import jax
import jax.numpy as jnp
from jax import lax
from jax.experimental import pallas as pl
from jax.experimental.pallas import tpu as pltpu
from jax.sharding import Mesh
from jax.sharding import PartitionSpec as P

D = 4096
LANES = 128
BLOCK = 128


epsilon = 1e-06


def exchange(parts, axes):
    return lax.all_to_all(parts, axes, split_axis=0, concat_axis=0, tiled=True)


def copies(value, count):
    return jnp.broadcast_to(value, (count, *value.shape))


def from_partner(value):
    return lax.ppermute(value, "core", [(0, 1), (1, 0)])


def wide_dot(left, right):
    return jnp.dot(left, right, preferred_element_type=jnp.float32)


IN_VMEM = pl.BlockSpec(memory_space=pltpu.VMEM)
IN_HBM = pl.BlockSpec(memory_space=pltpu.HBM)
GAIN_ROWS = 16


def thirds(value):
    high = value.astype(jnp.bfloat16)
    rest = value - high.astype(jnp.float32)
    middle = rest.astype(jnp.bfloat16)
    return high, middle, (rest - middle.astype(jnp.float32)).astype(jnp.bfloat16)


def from_thirds(block):
    wide = block.astype(jnp.float32)
    return wide[0:1] + wide[1:2] + wide[2:3]


def open_kernel(
    first_at,
    second_at,
    hidden,
    lengths,
    mixer_gain,
    channel_gain,
    inverse,
    *refs,
):
    count = len(first_at) + len(second_at)
    sources = refs[:count]
    sent, first, second, table, rows, many, gains, place, arrived = refs[count:]
    moves = [
        pltpu.make_async_copy(source, target, arrived.at[i])
        for i, (source, target) in enumerate(
            [
                (hidden, rows),
                (lengths, place),
                (mixer_gain, gains.at[0:1]),
                (channel_gain, gains.at[1:2]),
                *((source, first.at[at]) for source, at in zip(sources, first_at)),
                *((source, second.at[at]) for source, at in zip(sources[len(first_at) :], second_at)),
            ]
        )
    ]
    for move in moves:
        move.start()
    lane = lax.broadcasted_iota(jnp.int32, (1, LANES), 1)
    moves[0].wait()
    many[...] = jnp.broadcast_to(rows[...][None], many.shape)
    out = pltpu.make_async_copy(many, sent, arrived.at[len(moves)])
    out.start()
    moves[1].wait()
    seqs = place.shape[0]
    for i in range(seqs):
        angle = place[i].astype(jnp.float32) * inverse[...]
        filled = lax.rem(place[i], BLOCK)
        table[i : i + 1] = jnp.cos(angle)
        table[seqs + i : seqs + i + 1] = jnp.sin(angle)
        table[2 * seqs + i : 2 * seqs + i + 1] = (filled - lane).astype(jnp.float32)
        table[3 * seqs + i : 3 * seqs + i + 1] = (filled + 1 + 0 * lane).astype(jnp.float32)
    moves[2].wait()
    moves[3].wait()
    for target, gain in zip((first, second), (gains[0:1], gains[1:2])):
        high, middle, low = (part.astype(jnp.float32) for part in thirds(gain))
        row = lax.broadcasted_iota(jnp.int32, (GAIN_ROWS, LANES), 0)
        block = jnp.where(row == 0, high, jnp.where(row == 1, middle, jnp.where(row == 2, low, 0.0)))
        target[target.shape[0] - GAIN_ROWS :, :LANES] = block.astype(jnp.bfloat16)
    for move in moves[4:]:
        move.wait()
    out.wait()


def opening(hidden, lengths, mixer_gain, channel_gain, first, second, peers):
    half = LANES
    inverse = 10000.0 ** (-jnp.arange(half, dtype=jnp.float32) / half)
    first_at, at = [], 0
    for array in first:
        first_at.append((slice(0, array.shape[0]), slice(at, at + array.shape[1])))
        at += array.shape[1]
    first_shape = (first[0].shape[0] + GAIN_ROWS, at)
    second_at, at = [], 0
    for array in second:
        second_at.append((slice(at, at + array.shape[0]),))
        at += array.shape[0]
    second_shape = (at + GAIN_ROWS, LANES)
    in_hbm = [hidden, lengths, mixer_gain[None], channel_gain[None]]
    in_hbm = [pltpu.with_memory_space_constraint(array, pltpu.HBM) for array in in_hbm]
    weights = [
        pltpu.with_memory_space_constraint(array, pltpu.HBM) for array in (*first, *second)
    ]
    many = (peers, *hidden.shape)
    return pl.pallas_call(
        functools.partial(open_kernel, first_at, second_at),
        out_shape=(
            jax.ShapeDtypeStruct(many, jnp.bfloat16),
            pltpu.VMEM(first_shape, jnp.bfloat16),
            pltpu.VMEM(second_shape, jnp.bfloat16),
            pltpu.VMEM((4 * lengths.shape[0], LANES), jnp.float32),
        ),
        in_specs=[IN_HBM] * 4 + [IN_VMEM] + [IN_HBM] * len(weights),
        out_specs=(IN_HBM, IN_VMEM, IN_VMEM, IN_VMEM),
        scratch_shapes=[
            pltpu.VMEM(hidden.shape, jnp.bfloat16),
            pltpu.VMEM(many, jnp.bfloat16),
            pltpu.VMEM((2, LANES), jnp.float32),
            pltpu.SMEM(lengths.shape, jnp.int32),
            pltpu.SemaphoreType.DMA((5 + len(weights),)),
        ],
        compiler_params=pltpu.CompilerParams(vmem_limit_bytes=8 << 20),
        cost_estimate=pl.CostEstimate(flops=2_000_000, bytes_accessed=1_000_000, transcendentals=0),
        name="opening",
    )(*in_hbm, inverse[None], *weights)


def rotated_by(vectors, cosine, sine):
    half = cosine.shape[1]
    front, back = vectors[:, :half], vectors[:, half:]
    return jnp.concatenate([front * cosine - back * sine, front * sine + back * cosine], axis=1)


def of_each(row, products):
    result = products[0]
    for i, product in enumerate(products[1:], 1):
        result = jnp.where(row == i, product, result)
    return result


def retain_kernel(decay, arrived, table, state, keys, values, group_gain, mixed):
    seqs, _, key_width, value_width = state.shape
    total = arrived[0].astype(jnp.float32)
    for i in range(1, arrived.shape[0]):
        total = total + arrived[i].astype(jnp.float32)
    ends = 2 * (key_width + value_width)
    scale = lax.rsqrt(total[:, ends : ends + 1] / D + epsilon)
    ready = (scale * total[:, :ends]).astype(jnp.bfloat16).astype(jnp.float32)
    cosine, sine = table[:seqs], table[seqs : 2 * seqs]
    distance = table[2 * seqs : 3 * seqs]
    weighting = jnp.where(distance > 0.0, jnp.exp(-decay[0] * distance), 0.0)
    carried = jnp.exp(-decay[0] * table[3 * seqs :, :1])
    query = rotated_by(ready[:, :key_width], cosine, sine).astype(jnp.bfloat16)
    fresh = rotated_by(ready[:, key_width : 2 * key_width], cosine, sine) * key_width ** (-0.5)
    value = ready[:, 2 * key_width : 2 * key_width + value_width]
    gate = ready[:, 2 * key_width + value_width :]
    own = jnp.sum(query.astype(jnp.float32) * fresh, axis=1, keepdims=True) * value
    row_k = lax.broadcasted_iota(jnp.int32, (seqs, keys.shape[2]), 0)
    row_v = lax.broadcasted_iota(jnp.int32, (seqs, value_width), 0)
    scores = of_each(row_k, [transposed_dot(query, keys[i, 0]) for i in range(seqs)])
    block_weights = (scores * weighting).astype(jnp.bfloat16)
    block = of_each(row_v, [wide_dot(block_weights, values[i, 0]) for i in range(seqs)])
    remembered = []
    for i in range(seqs):
        high = state[i, 0].astype(jnp.bfloat16)
        low = (state[i, 0] - high.astype(jnp.float32)).astype(jnp.bfloat16)
        remembered.append(wide_dot(query, high) + wide_dot(query, low))
    retained = own + block + carried * of_each(row_v, remembered)
    centre = jnp.mean(retained, axis=1, keepdims=True)
    away = retained - centre
    spread = jnp.mean(away * away, axis=1, keepdims=True)
    normed = away * lax.rsqrt(spread + epsilon)
    result = (jax.nn.silu(gate) * normed * group_gain[...]).astype(jnp.bfloat16)
    for i in range(mixed.shape[0]):
        mixed[i] = result


def retain(decay, arrived, table, state, keys, values, group_gain):
    z = arrived.shape[0]
    seqs, _, _, value_width = state.shape
    return pl.pallas_call(
        retain_kernel,
        out_shape=jax.ShapeDtypeStruct((z, seqs, value_width), jnp.bfloat16),
        in_specs=[pl.BlockSpec(memory_space=pltpu.SMEM)] + [IN_VMEM] * 6,
        out_specs=IN_VMEM,
        compiler_params=pltpu.CompilerParams(vmem_limit_bytes=8 << 20),
        cost_estimate=pl.CostEstimate(flops=8_000_000, bytes_accessed=2_000_000, transcendentals=0),
        name="retain",
    )(decay, arrived, table, state, keys, values, group_gain[None])


def activate_kernel(units, pad, arrived, activated):
    total = arrived[0].astype(jnp.float32)
    for i in range(1, arrived.shape[0]):
        total = total + arrived[i].astype(jnp.float32)
    scale = lax.rsqrt(total[:, units : units + 1] / D + epsilon)
    gate, up = scale * total[:, :units], scale * total[:, units + pad :]
    result = (jax.nn.silu(gate) * up).astype(jnp.bfloat16)
    for i in range(activated.shape[0]):
        activated[i] = result


def activate(arrived, units, pad):
    z, half, _ = arrived.shape
    return pl.pallas_call(
        functools.partial(activate_kernel, units, pad),
        out_shape=jax.ShapeDtypeStruct((z, half, units), jnp.bfloat16),
        in_specs=[IN_VMEM],
        out_specs=IN_VMEM,
        compiler_params=pltpu.CompilerParams(vmem_limit_bytes=8 << 20),
        cost_estimate=pl.CostEstimate(flops=1_000_000, bytes_accessed=200_000, transcendentals=0),
        name="activate",
    )(arrived)


def transposed_dot(left, right):
    return lax.dot_general(
        left, right, (((1,), (1,)), ((), ())), preferred_element_type=jnp.float32
    )


def store_by_peer(terms, wide):
    half = terms.shape[1]
    for i in range(terms.shape[0]):
        terms[i] = wide[half * i : half * (i + 1)].astype(jnp.bfloat16)


def project_kernel(stream, own, partner, terms, wide):
    _, rows, features = stream.shape
    width = own.shape[1]
    parts = [stream[i].astype(jnp.float32) for i in range(2)]
    total = None
    for part, weights in zip(parts, (own, partner)):
        gain = from_thirds(weights[features : features + GAIN_ROWS, :features])
        scaled = (part * gain).astype(jnp.bfloat16)
        term = jnp.dot(scaled, weights[:features], preferred_element_type=jnp.float32)
        total = term if total is None else total + term
    wide[:, :width] = total
    squares = jnp.sum(parts[0] * parts[0] + parts[1] * parts[1], axis=1, keepdims=True)
    lane = lax.broadcasted_iota(jnp.int32, (rows, LANES), 1)
    wide[:, width:] = jnp.where(lane == 0, squares, 0.0)
    store_by_peer(terms, wide)


def project(stream, own, partner, z):
    rows = stream.shape[1]
    width = own.shape[1] + LANES
    return pl.pallas_call(
        project_kernel,
        out_shape=jax.ShapeDtypeStruct((z, rows // z, width), jnp.bfloat16),
        in_specs=[IN_VMEM] * 3,
        out_specs=IN_VMEM,
        scratch_shapes=[pltpu.VMEM((rows, width), jnp.float32)],
        compiler_params=pltpu.CompilerParams(vmem_limit_bytes=8 << 20),
        cost_estimate=pl.CostEstimate(flops=8_000_000, bytes_accessed=1_000_000, transcendentals=0),
        name="project",
    )(stream, own, partner)


def channel_kernel(
    head, units, pad, parts, stream, own_weights, partner, terms, residual, wide
):
    rows, features = stream.shape[1:]
    half = terms.shape[1]
    mixer_out = parts[0].astype(jnp.float32)
    for i in range(1, parts.shape[0]):
        mixer_out = mixer_out + parts[i].astype(jnp.float32)
    own = stream[0].astype(jnp.float32) + mixer_out[:, :features]
    other = stream[1].astype(jnp.float32) + mixer_out[:, features:]
    at = head + 3 * units
    scaled_own, scaled_other = (
        (part * from_thirds(weights[at : at + GAIN_ROWS])).astype(jnp.bfloat16)
        for part, weights in ((own, own_weights), (other, partner))
    )
    squares = jnp.sum(own * own + other * other, axis=1, keepdims=True)
    wide[:, :units] = transposed_dot(
        scaled_own, own_weights[head : head + units]
    ) + transposed_dot(
        scaled_other, partner[head : head + units]
    )
    lane = lax.broadcasted_iota(jnp.int32, (rows, pad), 1)
    wide[:, units : units + pad] = jnp.where(lane == 0, squares, 0.0)
    wide[:, units + pad :] = transposed_dot(
        scaled_own, own_weights[head + units : head + 2 * units]
    ) + transposed_dot(
        scaled_other, partner[head + units : head + 2 * units]
    )
    store_by_peer(terms, wide)
    row = lax.broadcasted_iota(jnp.int32, (rows, features), 0)
    here = row // half == lax.axis_index("kv")
    residual[0] = jnp.where(here, own, 0.0)
    residual[1] = jnp.where(here, other, 0.0)


def channel(parts, stream, own_weights, partner, head, units, z):
    pad = -units % LANES
    _, rows, features = stream.shape
    width = 2 * units + pad
    return pl.pallas_call(
        functools.partial(channel_kernel, head, units, pad),
        out_shape=(
            jax.ShapeDtypeStruct((z, rows // z, width), jnp.bfloat16),
            jax.ShapeDtypeStruct((2, rows, features), jnp.float32),
        ),
        in_specs=[IN_VMEM] * 4,
        out_specs=(IN_VMEM, IN_VMEM),
        scratch_shapes=[pltpu.VMEM((rows, width), jnp.float32)],
        compiler_params=pltpu.CompilerParams(vmem_limit_bytes=8 << 20),
        cost_estimate=pl.CostEstimate(flops=8_000_000, bytes_accessed=1_000_000, transcendentals=0),
        name="channel",
    )(parts, stream, own_weights, partner)


def local(
    hidden_in,
    mixer_gain,
    query_weight,
    key_weight,
    value_weight,
    gate_weight,
    decay_rate,
    prior_state,
    key_block,
    value_block,
    lengths,
    group_gain,
    output_weight,
    channel_gain,
    hidden_gate,
    hidden_up,
    hidden_down,
):
    kv, z = lax.axis_size("kv"), lax.axis_size("z")
    core = lax.axis_index("core")
    own_rows, features = hidden_in.shape
    half = own_rows // 2
    rows = kv * half
    head_width, units = output_weight.shape[0], hidden_gate.shape[1]
    pad = -units % LANES

    def own_and_partner(pair):
        swapped = core == 1
        return (
            jnp.where(swapped, pair[1], pair[0]),
            jnp.where(swapped, pair[0], pair[1]),
        )

    with jax.named_scope("rows"):
        sent, first_own, second_own, table = opening(
            hidden_in,
            lengths,
            mixer_gain,
            channel_gain,
            (query_weight, key_weight, value_weight, gate_weight),
            (output_weight, hidden_gate.T, hidden_up.T, hidden_down),
            2 * kv,
        )
        arrived = exchange(sent, ("core", "kv")).reshape(2, kv, 2, half, features)
        mine = jnp.where(core == 1, arrived[:, :, 1], arrived[:, :, 0])
        stream = jnp.stack(own_and_partner(mine.reshape(2, rows, features)))
    with jax.named_scope("swap"):
        first_partner = from_partner(first_own)
        second_own, stream = lax.optimization_barrier((second_own, stream))
        second_partner = from_partner(second_own)
        own_output, partner_output = (
            weights[:head_width] for weights in (second_own, second_partner)
        )
        own_down, partner_down = (
            weights[head_width + 2 * units : head_width + 3 * units]
            for weights in (second_own, second_partner)
        )
    with jax.named_scope("project"):
        arrived = exchange(project(stream, first_own, first_partner, z), "z")
    with jax.named_scope("retain"):
        mixed = retain(
            decay_rate, arrived, table, prior_state, key_block, value_block, group_gain
        )
    with jax.named_scope("mix"):
        all_mixed = exchange(mixed, "z").reshape(rows, head_width)
        head_terms = jnp.concatenate(
            [wide_dot(all_mixed, own_output), wide_dot(all_mixed, partner_output)], axis=1
        ).astype(jnp.bfloat16)
        head_parts = exchange(copies(head_terms, kv), "kv")
    with jax.named_scope("channel"):
        channel_terms, residual = channel(
            head_parts, stream, second_own, second_partner, head_width, units, z
        )
        activated = activate(exchange(channel_terms, "z"), units, pad)
    with jax.named_scope("finish"):
        all_activated = exchange(activated, "z").reshape(rows, units)
        unit_terms = [
            wide_dot(all_activated, matrix) + part
            for matrix, part in zip((own_down, partner_down), residual)
        ]
        sent = jnp.stack(own_and_partner(unit_terms)).reshape(2 * kv, half, features)
        arrived = exchange(sent, ("core", "kv")).reshape(2, kv, half, features)
        return jnp.sum(arrived, axis=1).reshape(own_rows, features).astype(jnp.bfloat16)


def solution(mesh):
    kv, tp = mesh.shape["kv"], mesh.shape["tp"]
    chips = Mesh(mesh.devices.reshape(kv, tp // 2, 2), ("kv", "z", "core"))
    tp = ("z", "core")
    in_specs = (
        P("kv", tp),
        P(tp),
        P(tp, "kv"),
        P(tp, "kv"),
        P(tp, "kv"),
        P(tp, "kv"),
        P("kv"),
        P(tp, "kv", None, None),
        P(tp, "kv", None, None),
        P(tp, "kv", None, None),
        P(tp),
        P("kv"),
        P("kv", tp),
        P(tp),
        P(tp, "kv"),
        P(tp, "kv"),
        P("kv", tp),
    )
    return jax.shard_map(
        local, mesh=chips, in_specs=in_specs, out_specs=P("kv", tp), check_vma=False
    )
```

time: 124 us -> 121 us (0.976)
  waiting for transfers between devices: 9.38 us -> 13.2 us
  local copies, waits for them, and re-layouts: 3.32 us -> 0.1 us
  blocking collectives: 74.5 us -> 72.6 us
  other arithmetic: 2.11 us -> 0.65 us
    all_to_all x2, waiting for transfers between devices: 9.37 us -> 13.2 us  [exchange(): return lax.all_to_all(parts, axes, split_axis=0, concat_axis=0, tiled=True)]
    all_to_all x5, blocking collectives: 74.5 us -> 72.6 us  [exchange(): return lax.all_to_all(parts, axes, split_axis=0, concat_axis=0, tiled=True)]
    unnamed x22 -> x8, local copies, waits for them, and re-layouts: 1.78 us -> 0.02 us
    broadcast_in_dim x4 -> x1, local copies, waits for them, and re-layouts: 1.46 us -> 0.02 us  [copies(): return jnp.broadcast_to(value, (count, *value.shape))]
  transfers between devices with their start and end apart: 4 -> 4, of which waited for: 2 -> 2; matrix products, arithmetic and copies ran while one was open for 2% -> 0% of each run, Pallas kernels for 2% -> 1%
where the time goes in v4:
time: 121 us; the launch traced here: 120 us
  blocking collectives  72.6 us (60%)
  starting transfers between devices  28.6 us (24%)
  waiting for transfers between devices  13.2 us (11%)
  Pallas kernels  3.73 us (3%)
    all_to_all x5, blocking collectives, exchange(): return lax.all_to_all(parts, axes, split_axis=0, concat_axis=0, tiled=True)  72.6 us
    all_to_all x2, starting transfers between devices, exchange(): return lax.all_to_all(parts, axes, split_axis=0, concat_axis=0, tiled=True)  23.7 us
    all_to_all x2, waiting for transfers between devices, exchange(): return lax.all_to_all(parts, axes, split_axis=0, concat_axis=0, tiled=True)  13.2 us
    ppermute x2, starting transfers between devices, from_partner(): return lax.ppermute(value, 'core', [(0, 1), (1, 0)])  4.98 us
  transfers between devices with their start and end apart: 4, of which 2 were waited for; matrix products, arithmetic and copies ran while one was open for 0% of the time, Pallas kernels for 1%

profile of v4, /device:TPU:1, one launch (start us, length us, event | category | flops | bytes accessed | tf_op | source)
XLA Modules:
  0.0 120.3 jit_solution(17981496627310355501)
XLA Ops:
  0.0 0.0 copy-start
  0.0 1.5 %opening.1 = (bf16[32,4,128]{2,1,0:T(4,128)(2,1)}, bf16[144,1536]{1,0:T(8,128)(2,1)S(1)}, bf16[2640,128]{1,0:T(8,128)(2,1)S(1)}, f32[8,128]{1,0:T(8,128)S(1)}) custom-call(bf16[4,128]{1,0:T(4,128)(2,1)} %hidden.1, s32[2]{0:T(128)} %lengths.1, f32[1,128]{1,0:T(1,128)} %bitcast.45, f32[1,128]{1,0:T(1,128)} %bitcast.46, ...), custom_call_target="tpu_custom_call" | custom-call | flops 2000000 | bytes 1000000 | tf_op jit(solution)/shard_map/rows/opening/pallas_call | solution.py:125
  1.6 10.4 %all-to-all-start = ((bf16[32,4,128]{2,1,0:T(4,128)(2,1)}), bf16[32,4,128]{2,1,0:T(4,128)(2,1)S(1)}, u32[]{:S(2)}, u32[]{:S(2)}) async-start(bf16[32,4,128]{2,1,0:T(4,128)(2,1)} %get-tuple-element.14), calls=%async_computation | async-start | bytes 65536 | tf_op jit(solution)/shard_map/rows/all_to_all | solution.py:20
  12.0 2.2 %collective-permute-start = (bf16[144,1536]{1,0:T(8,128)(2,1)S(1)}, bf16[144,1536]{1,0:T(8,128)(2,1)S(1)}, u32[]{:S(2)}, u32[]{:S(2)}) collective-permute-start(bf16[144,1536]{1,0:T(8,128)(2,1)S(1)} %get-tuple-element.16.own), channel_id=1, source_target_pairs={{0,1},{1,0},{2,3},{3,2},{4,5},{5,4},{6,7},{7,6},{8,9},{9,8},{10,11... | collective-permute-start | bytes 1327112 | tf_op jit(solution)/shard_map/swap/ppermute | solution.py:28
  14.2 4.8 %all-to-all-done = bf16[32,4,128]{2,1,0:T(4,128)(2,1)S(1)} async-done(((bf16[32,4,128]{2,1,0:T(4,128)(2,1)}), bf16[32,4,128]{2,1,0:T(4,128)(2,1)S(1)}, u32[]{:S(2)}, u32[]{:S(2)}) %all-to-all-start) | async-done | bytes 32800 | tf_op jit(solution)/shard_map/rows/all_to_all | solution.py:20
  19.1 0.0 collective-permute-done.partner
  19.1 0.0 copy-start.1
  19.1 0.9 project.1
  20.0 0.0 copy-start.2
  20.0 13.2 %all-to-all-start.1 = ((bf16[16,2,1664]{2,1,0:T(2,128)(2,1)}), bf16[16,2,1664]{2,1,0:T(2,128)(2,1)S(1)}, u32[]{:S(2)}, u32[]{:S(2)}) async-start(bf16[16,2,1664]{2,1,0:T(2,128)(2,1)} %project.1), calls=%async_computation.1 | async-start | bytes 212992 | tf_op jit(solution)/shard_map/project/all_to_all | solution.py:20
  33.2 2.8 %collective-permute-start.1 = (bf16[2640,128]{1,0:T(8,128)(2,1)S(1)}, bf16[2640,128]{1,0:T(8,128)(2,1)S(1)}, u32[]{:S(2)}, u32[]{:S(2)}) collective-permute-start(bf16[2640,128]{1,0:T(8,128)(2,1)S(1)} %get-tuple-element.18.own_weights), channel_id=1, source_target_pairs={{0,1},{1,0},{2,3},{3,2},{4,5},{5,4},{6,7},{7,6},{8,9},{9,8},{10,11... | collective-permute-start | bytes 2027528 | tf_op jit(solution)/shard_map/swap/ppermute | solution.py:28
  36.7 0.0 copy-start.3
  36.7 8.4 %all-to-all-done.1.arrived = bf16[16,2,1664]{2,1,0:T(2,128)(2,1)S(1)} async-done(((bf16[16,2,1664]{2,1,0:T(2,128)(2,1)}), bf16[16,2,1664]{2,1,0:T(2,128)(2,1)S(1)}, u32[]{:S(2)}, u32[]{:S(2)}) %all-to-all-start.1) | async-done | bytes 106528 | tf_op jit(solution)/shard_map/project/all_to_all | solution.py:20
  45.1 0.0 copy-done
  45.1 0.0 copy-done.1
  45.1 0.0 copy-done.2
  45.1 0.0 copy-done.3
  45.1 0.7 retain.1
  45.8 16.3 %all_to_all.35 = bf16[16,2,512]{2,1,0:T(2,128)(2,1)S(1)} all-to-all(bf16[16,2,512]{2,1,0:T(2,128)(2,1)S(1)} %retain.1), channel_id=1, replica_groups=mesh['kv'=16,'z'=16,'core'=2] {'z'}, dimensions={0} | all-to-all | bytes 65536 | tf_op jit(solution)/shard_map/mix/all_to_all | solution.py:20
  62.1 0.1 convolution_convert_fusion.1
  62.3 0.0 collective-permute-done.1.partner
  62.3 0.1 convolution_convert_fusion
  62.4 11.1 %all_to_all.36.parts = bf16[16,32,256]{2,1,0:T(8,128)(2,1)S(1)} all-to-all(bf16[16,32,256]{2,1,0:T(8,128)(2,1)S(1)} %broadcast_in_dim.16), channel_id=1, replica_groups=mesh['kv'=16,'z'=16,'core'=2] {'kv'}, dimensions={0} | all-to-all | bytes 524288 | tf_op jit(solution)/shard_map/mix/all_to_all | solution.py:20
  73.5 0.4 channel.1
  73.9 14.3 %all_to_all.37.arrived = bf16[16,2,1472]{2,1,0:T(2,128)(2,1)S(1)} all-to-all(bf16[16,2,1472]{2,1,0:T(2,128)(2,1)S(1)} %get-tuple-element.19), channel_id=1, replica_groups=mesh['kv'=16,'z'=16,'core'=2] {'z'}, dimensions={0} | all-to-all | bytes 188416 | tf_op jit(solution)/shard_map/channel/all_to_all | solution.py:20
  88.3 0.2 activate.1
  88.5 14.9 %all_to_all.38 = bf16[16,2,704]{2,1,0:T(2,128)(2,1)S(1)} all-to-all(bf16[16,2,704]{2,1,0:T(2,128)(2,1)S(1)} %activate.1), channel_id=1, replica_groups=mesh['kv'=16,'z'=16,'core'=2] {'z'}, dimensions={0} | all-to-all | bytes 90112 | tf_op jit(solution)/shard_map/finish/all_to_all | solution.py:20
  103.4 0.2 fusion.1
  103.5 0.2 select_bitcast_fusion.1
  103.7 16.0 %all_to_all.39 = f32[32,2,128]{2,1,0:T(2,128)S(1)} all-to-all(f32[32,2,128]{2,1,0:T(2,128)S(1)} %bitcast.42), channel_id=1, replica_groups=mesh['kv'=16,'z'=16,'core'=2] {'core','kv'}, dimensions={0} | all-to-all | bytes 65536 | tf_op jit(solution)/shard_map/finish/all_to_all | solution.py:20
  119.7 0.6 bitcast_reduce_fusion
  (9 shorter events, 0.1 us)
Async XLA Ops:
  0.0 45.1 %copy-start = (f32[2,1,256,512]{3,2,1,0:T(8,128)S(1)}, f32[2,1,256,512]{3,2,1,0:T(8,128)}, u32[]{:S(2)}) copy-start(f32[2,1,256,512]{3,2,1,0:T(8,128)} %state.1) | copy-start | bytes 3145732
  1.6 17.4 %all-to-all-start = ((bf16[32,4,128]{2,1,0:T(4,128)(2,1)}), bf16[32,4,128]{2,1,0:T(4,128)(2,1)S(1)}, u32[]{:S(2)}, u32[]{:S(2)}) async-start(bf16[32,4,128]{2,1,0:T(4,128)(2,1)} %get-tuple-element.14), calls=%async_computation | async-start | bytes 65536 | tf_op jit(solution)/shard_map/rows/all_to_all | solution.py:20
  12.0 7.0 %collective-permute-start = (bf16[144,1536]{1,0:T(8,128)(2,1)S(1)}, bf16[144,1536]{1,0:T(8,128)(2,1)S(1)}, u32[]{:S(2)}, u32[]{:S(2)}) collective-permute-start(bf16[144,1536]{1,0:T(8,128)(2,1)S(1)} %get-tuple-element.16.own), channel_id=1, source_target_pairs={{0,1},{1,0},{2,3},{3,2},{4,5},{5,4},{6,7},{7,6},{8,9},{9,8},{10,11... | collective-permute-start | bytes 1327112 | tf_op jit(solution)/shard_map/swap/ppermute | solution.py:28
  19.1 26.0 %copy-start.1 = (bf16[2,1,128,512]{3,2,1,0:T(8,128)(2,1)S(1)}, bf16[2,1,128,512]{3,2,1,0:T(8,128)(2,1)}, u32[]{:S(2)}) copy-start(bf16[2,1,128,512]{3,2,1,0:T(8,128)(2,1)} %values.1) | copy-start | bytes 786436
  20.0 25.1 %copy-start.2 = (bf16[2,1,128,256]{3,2,1,0:T(8,128)(2,1)S(1)}, bf16[2,1,128,256]{3,2,1,0:T(8,128)(2,1)}, u32[]{:S(2)}) copy-start(bf16[2,1,128,256]{3,2,1,0:T(8,128)(2,1)} %keys.1) | copy-start | bytes 393220
  20.0 25.1 %all-to-all-start.1 = ((bf16[16,2,1664]{2,1,0:T(2,128)(2,1)}), bf16[16,2,1664]{2,1,0:T(2,128)(2,1)S(1)}, u32[]{:S(2)}, u32[]{:S(2)}) async-start(bf16[16,2,1664]{2,1,0:T(2,128)(2,1)} %project.1), calls=%async_computation.1 | async-start | bytes 212992 | tf_op jit(solution)/shard_map/project/all_to_all | solution.py:20
  33.2 29.0 %collective-permute-start.1 = (bf16[2640,128]{1,0:T(8,128)(2,1)S(1)}, bf16[2640,128]{1,0:T(8,128)(2,1)S(1)}, u32[]{:S(2)}, u32[]{:S(2)}) collective-permute-start(bf16[2640,128]{1,0:T(8,128)(2,1)S(1)} %get-tuple-element.18.own_weights), channel_id=1, source_target_pairs={{0,1},{1,0},{2,3},{3,2},{4,5},{5,4},{6,7},{7,6},{8,9},{9,8},{10,11... | collective-permute-start | bytes 2027528 | tf_op jit(solution)/shard_map/swap/ppermute | solution.py:28
  36.7 8.4 %copy-start.3 = (f32[512]{0:T(512)S(1)}, f32[512]{0:T(512)}, u32[]{:S(2)}) copy-start(f32[512]{0:T(512)} %param.28) | copy-start | bytes 6148

commit v5 on v4

v5 whole, which is shorter than its diff:
```python
import functools

import jax
import jax.numpy as jnp
from jax import lax
from jax.experimental import pallas as pl
from jax.experimental.pallas import tpu as pltpu
from jax.sharding import Mesh
from jax.sharding import PartitionSpec as P

D = 4096
LANES = 128
BLOCK = 128


epsilon = 1e-06


def exchange(parts, axes):
    return lax.all_to_all(parts, axes, split_axis=0, concat_axis=0, tiled=True)


def wide_dot(left, right):
    return jnp.dot(left, right, preferred_element_type=jnp.float32)


IN_VMEM = pl.BlockSpec(memory_space=pltpu.VMEM)
IN_HBM = pl.BlockSpec(memory_space=pltpu.HBM)
IN_SMEM = pl.BlockSpec(memory_space=pltpu.SMEM)
GAIN_ROWS = 16


def thirds(value):
    high = value.astype(jnp.bfloat16)
    rest = value - high.astype(jnp.float32)
    middle = rest.astype(jnp.bfloat16)
    return high, middle, (rest - middle.astype(jnp.float32)).astype(jnp.bfloat16)


def from_thirds(block):
    wide = block.astype(jnp.float32)
    return wide[0:1] + wide[1:2] + wide[2:3]


def open_kernel(at, decay, hidden, lengths, mixer_gain, channel_gain, inverse, *refs):
    sources = refs[: len(at)]
    sent, joined, table, rows, gains, place, arrived = refs[len(at) :]
    pairs = [
        (hidden, rows),
        (lengths, place),
        (mixer_gain, gains.at[0:1]),
        (channel_gain, gains.at[1:2]),
    ]
    for source, first in zip(sources, at):
        for lanes in range(0, source.shape[1], LANES):
            span = slice(first + lanes // LANES * source.shape[0], None)
            span = slice(span.start, span.start + source.shape[0])
            pairs.append((source.at[:, lanes : lanes + LANES], joined.at[span]))
    moves = [
        pltpu.make_async_copy(source, target, arrived.at[i])
        for i, (source, target) in enumerate(pairs)
    ]
    for move in moves:
        move.start()
    lane = lax.broadcasted_iota(jnp.int32, (1, LANES), 1)
    for move in moves[:4]:
        move.wait()
    peers, half, _ = sent.shape
    wide = rows[...].astype(jnp.float32)
    for i in range(peers):
        first = half * (2 * i // peers)
        sent[i] = wide[first : first + half].astype(jnp.bfloat16)
    seqs = place.shape[0]
    for i in range(seqs):
        angle = place[i].astype(jnp.float32) * inverse[...]
        filled = lax.rem(place[i], BLOCK)
        distance = (filled - lane).astype(jnp.float32)
        table[i : i + 1] = jnp.cos(angle)
        table[seqs + i : seqs + i + 1] = jnp.sin(angle)
        table[2 * seqs + i : 2 * seqs + i + 1] = jnp.where(
            lane < filled, jnp.exp(-decay[0] * distance), 0.0
        )
        reach = (filled + 1 + 0 * lane).astype(jnp.float32)
        table[3 * seqs + i : 3 * seqs + i + 1] = jnp.exp(-decay[0] * reach)
    row = lax.broadcasted_iota(jnp.int32, (GAIN_ROWS, LANES), 0)
    end = joined.shape[0]
    for i in range(2):
        high, middle, low = (part.astype(jnp.float32) for part in thirds(gains[i : i + 1]))
        block = jnp.where(row == 0, high, jnp.where(row == 1, middle, jnp.where(row == 2, low, 0.0)))
        first = end - (2 - i) * GAIN_ROWS
        joined[first : first + GAIN_ROWS] = block.astype(jnp.bfloat16)
    for move in moves[4:]:
        move.wait()


def opening(hidden, lengths, decay, mixer_gain, channel_gain, weights, peers):
    inverse = 10000.0 ** (-jnp.arange(LANES, dtype=jnp.float32) / LANES)
    at, end = [], 0
    for array in weights:
        at.append(end)
        end += array.size // LANES
    in_hbm = [
        pltpu.with_memory_space_constraint(array, pltpu.HBM)
        for array in (hidden, lengths, mixer_gain[None], channel_gain[None], *weights)
    ]
    pieces = sum(array.shape[1] // LANES for array in weights)
    return pl.pallas_call(
        functools.partial(open_kernel, at),
        out_shape=(
            jax.ShapeDtypeStruct((peers, hidden.shape[0] // 2, LANES), jnp.bfloat16),
            pltpu.VMEM((end + 2 * GAIN_ROWS, LANES), jnp.bfloat16),
            pltpu.VMEM((4 * lengths.shape[0], LANES), jnp.float32),
        ),
        in_specs=[IN_SMEM] + [IN_HBM] * 4 + [IN_VMEM] + [IN_HBM] * len(weights),
        out_specs=(IN_VMEM, IN_VMEM, IN_VMEM),
        scratch_shapes=[
            pltpu.VMEM(hidden.shape, jnp.bfloat16),
            pltpu.VMEM((2, LANES), jnp.float32),
            pltpu.SMEM(lengths.shape, jnp.int32),
            pltpu.SemaphoreType.DMA((4 + pieces,)),
        ],
        compiler_params=pltpu.CompilerParams(vmem_limit_bytes=8 << 20),
        cost_estimate=pl.CostEstimate(flops=2_000_000, bytes_accessed=1_000_000, transcendentals=0),
        name="opening",
    )(decay, *in_hbm[:4], inverse[None], *in_hbm[4:])


def rotated_by(vectors, cosine, sine):
    half = cosine.shape[1]
    front, back = vectors[:, :half], vectors[:, half:]
    return jnp.concatenate([front * cosine - back * sine, front * sine + back * cosine], axis=1)


def of_each(row, products):
    result = products[0]
    for i, product in enumerate(products[1:], 1):
        result = jnp.where(row == i, product, result)
    return result


def retain_kernel(arrived, table, state, keys, values, group_gain, mixed):
    seqs, _, key_width, value_width = state.shape
    total = arrived[0].astype(jnp.float32)
    for i in range(1, arrived.shape[0]):
        total = total + arrived[i].astype(jnp.float32)
    ends = 2 * (key_width + value_width)
    scale = lax.rsqrt(total[:, ends : ends + 1] / D + epsilon)
    ready = (scale * total[:, :ends]).astype(jnp.bfloat16).astype(jnp.float32)
    cosine, sine = table[:seqs], table[seqs : 2 * seqs]
    weighting = table[2 * seqs : 3 * seqs]
    carried = table[3 * seqs :, :1]
    query = rotated_by(ready[:, :key_width], cosine, sine).astype(jnp.bfloat16)
    fresh = rotated_by(ready[:, key_width : 2 * key_width], cosine, sine) * key_width ** (-0.5)
    value = ready[:, 2 * key_width : 2 * key_width + value_width]
    gate = ready[:, 2 * key_width + value_width :]
    own = jnp.sum(query.astype(jnp.float32) * fresh, axis=1, keepdims=True) * value
    row_k = lax.broadcasted_iota(jnp.int32, (seqs, keys.shape[2]), 0)
    row_v = lax.broadcasted_iota(jnp.int32, (seqs, value_width), 0)
    scores = of_each(row_k, [transposed_dot(query, keys[i, 0]) for i in range(seqs)])
    block_weights = (scores * weighting).astype(jnp.bfloat16)
    block = of_each(row_v, [wide_dot(block_weights, values[i, 0]) for i in range(seqs)])
    remembered = []
    for i in range(seqs):
        high = state[i, 0].astype(jnp.bfloat16)
        low = (state[i, 0] - high.astype(jnp.float32)).astype(jnp.bfloat16)
        remembered.append(wide_dot(query, high) + wide_dot(query, low))
    retained = own + block + carried * of_each(row_v, remembered)
    centre = jnp.mean(retained, axis=1, keepdims=True)
    away = retained - centre
    spread = jnp.mean(away * away, axis=1, keepdims=True)
    normed = away * lax.rsqrt(spread + epsilon)
    result = (jax.nn.silu(gate) * normed * group_gain[...]).astype(jnp.bfloat16)
    for i in range(mixed.shape[0]):
        mixed[i] = result


def retain(arrived, table, state, keys, values, group_gain):
    seqs, _, _, value_width = state.shape
    out_shape = jax.ShapeDtypeStruct((arrived.shape[0], seqs, value_width), jnp.bfloat16)
    operands = (arrived, table, state, keys, values, group_gain[None])
    return call(retain_kernel, out_shape, operands, [], "retain")


def activate_kernel(units, pad, arrived, activated):
    total = arrived[0].astype(jnp.float32)
    for i in range(1, arrived.shape[0]):
        total = total + arrived[i].astype(jnp.float32)
    scale = lax.rsqrt(total[:, units : units + 1] / D + epsilon)
    gate, up = scale * total[:, :units], scale * total[:, units + pad :]
    result = (jax.nn.silu(gate) * up).astype(jnp.bfloat16)
    for i in range(activated.shape[0]):
        activated[i] = result


def activate(arrived, units, pad):
    out_shape = jax.ShapeDtypeStruct((*arrived.shape[:2], units), jnp.bfloat16)
    kernel = functools.partial(activate_kernel, units, pad)
    return call(kernel, out_shape, (arrived,), [], "activate")


def transposed_dot(left, right):
    return lax.dot_general(
        left, right, (((1,), (1,)), ((), ())), preferred_element_type=jnp.float32
    )


def store_by_peer(terms, wide):
    half = terms.shape[1]
    for i in range(terms.shape[0]):
        terms[i] = wide[half * i : half * (i + 1)].astype(jnp.bfloat16)


def gathered_rows(arrived, wide):
    half = arrived.shape[1]
    for i in range(arrived.shape[0]):
        wide[half * i : half * (i + 1)] = arrived[i].astype(jnp.float32)


def project_kernel(arrived, own, partner, terms, stream, wide):
    _, rows, features = stream.shape
    half = terms.shape[1]
    width = wide.shape[1] - LANES
    side = lax.axis_index("core")
    for i in range(rows // half):
        span = slice(half * i, half * (i + 1))
        stream[0, span] = arrived[side, i].astype(jnp.float32)
        stream[1, span] = arrived[1 - side, i].astype(jnp.float32)
    parts = [stream[i] for i in range(2)]
    end = own.shape[0]
    scaled = jnp.concatenate(
        [
            (part * from_thirds(weights[end - 2 * GAIN_ROWS : end - GAIN_ROWS])).astype(
                jnp.bfloat16
            )
            for part, weights in zip(parts, (own, partner))
        ],
        axis=1,
    )
    for i in range(width // LANES):
        span = slice(features * i, features * (i + 1))
        columns = jnp.concatenate([own[span], partner[span]], axis=0)
        wide[:, LANES * i : LANES * (i + 1)] = wide_dot(scaled, columns)
    squares = jnp.sum(parts[0] * parts[0] + parts[1] * parts[1], axis=1, keepdims=True)
    lane = lax.broadcasted_iota(jnp.int32, (rows, LANES), 1)
    wide[:, width:] = jnp.where(lane == 0, squares, 0.0)
    store_by_peer(terms, wide)


def call(kernel, out_shape, operands, scratch, name):
    return pl.pallas_call(
        kernel,
        out_shape=out_shape,
        in_specs=[IN_VMEM] * len(operands),
        out_specs=jax.tree.map(lambda _: IN_VMEM, out_shape),
        scratch_shapes=scratch,
        compiler_params=pltpu.CompilerParams(vmem_limit_bytes=8 << 20),
        cost_estimate=pl.CostEstimate(flops=8_000_000, bytes_accessed=1_000_000, transcendentals=0),
        name=name,
    )(*operands)


def project(arrived, own, partner, width, z):
    _, kv, half, features = arrived.shape
    rows = kv * half
    width = width + LANES
    out_shape = (
        jax.ShapeDtypeStruct((z, rows // z, width), jnp.bfloat16),
        jax.ShapeDtypeStruct((2, rows, features), jnp.float32),
    )
    scratch = [pltpu.VMEM((rows, width), jnp.float32)]
    return call(project_kernel, out_shape, (arrived, own, partner), scratch, "project")


def mix_kernel(head, arrived, own, partner, terms, wide):
    gathered_rows(arrived, wide)
    every = wide[...].astype(jnp.bfloat16)
    span = slice(head, head + wide.shape[1])
    both = jnp.concatenate([wide_dot(every, own[span]), wide_dot(every, partner[span])], axis=1)
    both = both.astype(jnp.bfloat16)
    for i in range(terms.shape[0]):
        terms[i] = both


def mix(arrived, own, partner, head, kv):
    z, half, width = arrived.shape
    rows = z * half
    out_shape = jax.ShapeDtypeStruct((kv, rows, 2 * LANES), jnp.bfloat16)
    scratch = [pltpu.VMEM((rows, width), jnp.float32)]
    return call(
        functools.partial(mix_kernel, head), out_shape, (arrived, own, partner), scratch, "mix"
    )


def finish_kernel(down, arrived, own, partner, residual, sent, wide):
    gathered_rows(arrived, wide)
    every = wide[...].astype(jnp.bfloat16)
    span = slice(down, down + wide.shape[1])
    side = lax.axis_index("core")
    peers, half, _ = sent.shape
    for i, weights in enumerate((own, partner)):
        total = wide_dot(every, weights[span]) + residual[i]
        to = side if i == 0 else 1 - side
        for peer in range(peers // 2):
            sent[to * (peers // 2) + peer] = total[half * peer : half * (peer + 1)]


def finish(arrived, own, partner, residual, down, kv):
    z, half, width = arrived.shape
    rows = z * half
    out_shape = jax.ShapeDtypeStruct((2 * kv, rows // kv, LANES), jnp.float32)
    scratch = [pltpu.VMEM((rows, width), jnp.float32)]
    return call(
        functools.partial(finish_kernel, down),
        out_shape,
        (arrived, own, partner, residual),
        scratch,
        "finish",
    )


def channel_kernel(
    head, units, pad, parts, stream, own_weights, partner, terms, residual, wide
):
    rows, features = stream.shape[1:]
    half = terms.shape[1]
    mixer_out = parts[0].astype(jnp.float32)
    for i in range(1, parts.shape[0]):
        mixer_out = mixer_out + parts[i].astype(jnp.float32)
    own = stream[0] + mixer_out[:, :features]
    other = stream[1] + mixer_out[:, features:]
    end = partner.shape[0]
    scaled_own, scaled_other = (
        (part * from_thirds(weights[end - GAIN_ROWS :])).astype(jnp.bfloat16)
        for part, weights in ((own, own_weights), (other, partner))
    )
    squares = jnp.sum(own * own + other * other, axis=1, keepdims=True)
    wide[:, :units] = transposed_dot(
        scaled_own, own_weights[head : head + units]
    ) + transposed_dot(
        scaled_other, partner[head : head + units]
    )
    lane = lax.broadcasted_iota(jnp.int32, (rows, pad), 1)
    wide[:, units : units + pad] = jnp.where(lane == 0, squares, 0.0)
    wide[:, units + pad :] = transposed_dot(
        scaled_own, own_weights[head + units : head + 2 * units]
    ) + transposed_dot(
        scaled_other, partner[head + units : head + 2 * units]
    )
    store_by_peer(terms, wide)
    row = lax.broadcasted_iota(jnp.int32, (rows, features), 0)
    here = row // half == lax.axis_index("kv")
    residual[0] = jnp.where(here, own, 0.0)
    residual[1] = jnp.where(here, other, 0.0)


def channel(parts, stream, own_weights, partner, head, units, z):
    pad = -units % LANES
    _, rows, features = stream.shape
    width = 2 * units + pad
    out_shape = (
        jax.ShapeDtypeStruct((z, rows // z, width), jnp.bfloat16),
        jax.ShapeDtypeStruct((2, rows, features), jnp.float32),
    )
    return call(
        functools.partial(channel_kernel, head, units, pad),
        out_shape,
        (parts, stream, own_weights, partner),
        [pltpu.VMEM((rows, width), jnp.float32)],
        "channel",
    )


def local(
    hidden_in,
    mixer_gain,
    query_weight,
    key_weight,
    value_weight,
    gate_weight,
    decay_rate,
    prior_state,
    key_block,
    value_block,
    lengths,
    group_gain,
    output_weight,
    channel_gain,
    hidden_gate,
    hidden_up,
    hidden_down,
):
    kv, z = lax.axis_size("kv"), lax.axis_size("z")
    own_rows, features = hidden_in.shape
    half = own_rows // 2
    head_width, units = output_weight.shape[0], hidden_gate.shape[1]
    weights = (
        query_weight,
        key_weight,
        value_weight,
        gate_weight,
        output_weight,
        hidden_gate.T,
        hidden_up.T,
        hidden_down,
    )
    width = sum(array.shape[1] for array in weights[:4])
    inner = width + head_width
    sent, own, table = opening(
        hidden_in, lengths, decay_rate, mixer_gain, channel_gain, weights, 2 * kv
    )
    partner = lax.ppermute(own, "core", [(0, 1), (1, 0)])
    rows = exchange(sent, ("core", "kv")).reshape(2, kv, half, features)
    terms, stream = project(rows, own, partner, width, z)
    mixed = retain(exchange(terms, "z"), table, prior_state, key_block, value_block, group_gain)
    parts = exchange(mix(exchange(mixed, "z"), own, partner, width, kv), "kv")
    terms, residual = channel(parts, stream, own, partner, inner, units, z)
    activated = activate(exchange(terms, "z"), units, -units % LANES)
    total = finish(
        exchange(activated, "z"), own, partner, residual, inner + 2 * units, kv
    )
    total = exchange(total, ("core", "kv")).reshape(2, kv, half, features)
    return jnp.sum(total, axis=1).reshape(own_rows, features).astype(jnp.bfloat16)


def solution(mesh):
    kv, tp = mesh.shape["kv"], mesh.shape["tp"]
    chips = Mesh(mesh.devices.reshape(kv, tp // 2, 2), ("kv", "z", "core"))
    tp = ("z", "core")
    in_specs = (
        P("kv", tp),
        P(tp),
        P(tp, "kv"),
        P(tp, "kv"),
        P(tp, "kv"),
        P(tp, "kv"),
        P("kv"),
        P(tp, "kv", None, None),
        P(tp, "kv", None, None),
        P(tp, "kv", None, None),
        P(tp),
        P("kv"),
        P("kv", tp),
        P(tp),
        P(tp, "kv"),
        P(tp, "kv"),
        P("kv", tp),
    )
    return jax.shard_map(
        local, mesh=chips, in_specs=in_specs, out_specs=P("kv", tp), check_vma=False
    )
```

time: 121 us -> 121 us (level)
  blocking collectives: 72.6 us -> 107 us
  starting transfers between devices: 28.6 us -> 8.75 us
  waiting for transfers between devices: 13.2 us -> 0.01 us
    all_to_all x5 -> x7, blocking collectives: 72.6 us -> 107 us  [exchange(): return lax.all_to_all(parts, axes, split_axis=0, concat_axis=0, tiled=True)]
    all_to_all x2 -> x0, starting transfers between devices: 23.7 us -> none  [exchange(): return lax.all_to_all(parts, axes, split_axis=0, concat_axis=0, tiled=True)]
    all_to_all x2 -> x0, waiting for transfers between devices: 13.2 us -> none  [exchange(): return lax.all_to_all(parts, axes, split_axis=0, concat_axis=0, tiled=True)]
    ppermute x2 -> x1, starting transfers between devices: 4.98 us -> 8.75 us  [local(): partner = lax.ppermute(own, 'core', [(0, 1), (1, 0)])]
    pallas_call x5 -> x7, Pallas kernels: 3.73 us -> 3.46 us  [the longest x6 1.91 us: call(): pl.pallas_call(kernel, out_shape=out_shape, in_specs=[IN_VMEM] * len(oper...]
  transfers between devices with their start and end apart: 4 -> 1, of which waited for: 2 -> 0; matrix products, arithmetic and copies ran while one was open for 0% -> 0% of each run, Pallas kernels for 1% -> 0%
where the time goes in v5:
time: 121 us
  blocking collectives  107 us (88%)
  starting transfers between devices  8.75 us (7%)
  Pallas kernels  3.46 us (3%)
    all_to_all x7, blocking collectives, exchange(): return lax.all_to_all(parts, axes, split_axis=0, concat_axis=0, tiled=True)  107 us
    ppermute x1, starting transfers between devices, local(): partner = lax.ppermute(own, 'core', [(0, 1), (1, 0)])  8.75 us
  transfers between devices with their start and end apart: 1, of which 0 were waited for; matrix products, arithmetic and copies ran while one was open for 0% of the time, Pallas kernels for 0%

profile of v5, /device:TPU:1, one launch (start us, length us, event | category | flops | bytes accessed | tf_op | source)
XLA Modules:
  0.0 121.0 jit_solution(7913046523237786236)
XLA Ops:
  0.7 1.5 %opening.1 = (bf16[32,2,128]{2,1,0:T(2,128)(2,1)S(1)}, bf16[4192,128]{1,0:T(8,128)(2,1)S(1)}, f32[8,128]{1,0:T(8,128)S(1)}) custom-call(f32[1]{0:T(128)S(6)} %copy.18.decay, bf16[4,128]{1,0:T(4,128)(2,1)} %hidden.1, s32[2]{0:T(128)} %lengths.1, f32[1,128]{1,0:T(1,128)} %bitcast.13, f32[1,128]{1,0:T(1,128)} %bitcast.14, ...), custom_call_target="tpu_custom_call" | custom-call | flops 2000000 | bytes 1000000 | tf_op jit(solution)/shard_map/opening/pallas_call | solution.py:107
  2.2 8.7 %collective-permute-start = (bf16[4192,128]{1,0:T(8,128)(2,1)S(1)}, bf16[4192,128]{1,0:T(8,128)(2,1)S(1)}, u32[]{:S(2)}, u32[]{:S(2)}) collective-permute-start(bf16[4192,128]{1,0:T(8,128)(2,1)S(1)} %get-tuple-element.13.own.own_weights), channel_id=1, source_target_pairs={{0,1},{1,0},{2,3},{3,2},{4,5},{5,4},{6,7},{7,6},{8,9},{9,8},{10,11... | collective-permute-start | bytes 3219464 | tf_op jit(solution)/shard_map/ppermute | solution.py:411
  11.0 9.6 %all_to_all.35 = bf16[32,2,128]{2,1,0:T(2,128)(2,1)S(1)} all-to-all(bf16[32,2,128]{2,1,0:T(2,128)(2,1)S(1)} %get-tuple-element.12), channel_id=1, replica_groups=mesh['kv'=16,'z'=16,'core'=2] {'core','kv'}, dimensions={0} | all-to-all | bytes 32768 | tf_op jit(solution)/shard_map/all_to_all | solution.py:20
  20.6 0.0 collective-permute-done.partner
  20.6 0.0 copy-start
  20.6 0.0 copy-start.1
  20.6 0.0 copy-start.2
  20.6 0.0 copy-start.3
  20.6 0.3 project.1
  20.9 25.7 %all_to_all.36.arrived = bf16[16,2,1664]{2,1,0:T(2,128)(2,1)S(1)} all-to-all(bf16[16,2,1664]{2,1,0:T(2,128)(2,1)S(1)} %get-tuple-element.14), channel_id=1, replica_groups=mesh['kv'=16,'z'=16,'core'=2] {'z'}, dimensions={0} | all-to-all | bytes 212992 | tf_op jit(solution)/shard_map/all_to_all | solution.py:20
  46.5 0.0 copy-done
  46.5 0.0 copy-done.1
  46.5 0.0 copy-done.2
  46.5 0.0 copy-done.3
  46.5 0.7 retain.1
  47.2 16.2 %all_to_all.37.arrived = bf16[16,2,512]{2,1,0:T(2,128)(2,1)S(1)} all-to-all(bf16[16,2,512]{2,1,0:T(2,128)(2,1)S(1)} %retain.1), channel_id=1, replica_groups=mesh['kv'=16,'z'=16,'core'=2] {'z'}, dimensions={0} | all-to-all | bytes 65536 | tf_op jit(solution)/shard_map/all_to_all | solution.py:20
  63.4 0.2 mix.1
  63.6 10.4 %all_to_all.38.parts = bf16[16,32,256]{2,1,0:T(8,128)(2,1)S(1)} all-to-all(bf16[16,32,256]{2,1,0:T(8,128)(2,1)S(1)} %mix.1), channel_id=1, replica_groups=mesh['kv'=16,'z'=16,'core'=2] {'kv'}, dimensions={0} | all-to-all | bytes 524288 | tf_op jit(solution)/shard_map/all_to_all | solution.py:20
  74.0 0.4 channel.1
  74.4 14.3 %all_to_all.39.arrived = bf16[16,2,1472]{2,1,0:T(2,128)(2,1)S(1)} all-to-all(bf16[16,2,1472]{2,1,0:T(2,128)(2,1)S(1)} %get-tuple-element.17), channel_id=1, replica_groups=mesh['kv'=16,'z'=16,'core'=2] {'z'}, dimensions={0} | all-to-all | bytes 188416 | tf_op jit(solution)/shard_map/all_to_all | solution.py:20
  88.8 0.2 activate.1
  89.0 14.9 %all_to_all.40.arrived = bf16[16,2,704]{2,1,0:T(2,128)(2,1)S(1)} all-to-all(bf16[16,2,704]{2,1,0:T(2,128)(2,1)S(1)} %activate.1), channel_id=1, replica_groups=mesh['kv'=16,'z'=16,'core'=2] {'z'}, dimensions={0} | all-to-all | bytes 90112 | tf_op jit(solution)/shard_map/all_to_all | solution.py:20
  103.9 0.2 finish.1
  104.1 16.3 %all_to_all.41 = f32[32,2,128]{2,1,0:T(2,128)S(1)} all-to-all(f32[32,2,128]{2,1,0:T(2,128)S(1)} %finish.1), channel_id=1, replica_groups=mesh['kv'=16,'z'=16,'core'=2] {'core','kv'}, dimensions={0} | all-to-all | bytes 65536 | tf_op jit(solution)/shard_map/all_to_all | solution.py:20
  120.4 0.6 bitcast_reduce_fusion
  (1 shorter events, 0.0 us)
Async XLA Ops:
  2.2 18.3 %collective-permute-start = (bf16[4192,128]{1,0:T(8,128)(2,1)S(1)}, bf16[4192,128]{1,0:T(8,128)(2,1)S(1)}, u32[]{:S(2)}, u32[]{:S(2)}) collective-permute-start(bf16[4192,128]{1,0:T(8,128)(2,1)S(1)} %get-tuple-element.13.own.own_weights), channel_id=1, source_target_pairs={{0,1},{1,0},{2,3},{3,2},{4,5},{5,4},{6,7},{7,6},{8,9},{9,8},{10,11... | collective-permute-start | bytes 3219464 | tf_op jit(solution)/shard_map/ppermute | solution.py:411
  20.6 26.0 %copy-start = (f32[2,1,256,512]{3,2,1,0:T(8,128)S(1)}, f32[2,1,256,512]{3,2,1,0:T(8,128)}, u32[]{:S(2)}) copy-start(f32[2,1,256,512]{3,2,1,0:T(8,128)} %state.1) | copy-start | bytes 3145732
  20.6 26.0 %copy-start.1 = (bf16[2,1,128,512]{3,2,1,0:T(8,128)(2,1)S(1)}, bf16[2,1,128,512]{3,2,1,0:T(8,128)(2,1)}, u32[]{:S(2)}) copy-start(bf16[2,1,128,512]{3,2,1,0:T(8,128)(2,1)} %values.1) | copy-start | bytes 786436
  20.6 26.0 %copy-start.2 = (bf16[2,1,128,256]{3,2,1,0:T(8,128)(2,1)S(1)}, bf16[2,1,128,256]{3,2,1,0:T(8,128)(2,1)}, u32[]{:S(2)}) copy-start(bf16[2,1,128,256]{3,2,1,0:T(8,128)(2,1)} %keys.1) | copy-start | bytes 393220
  20.6 26.0 %copy-start.3 = (f32[512]{0:T(512)S(1)}, f32[512]{0:T(512)}, u32[]{:S(2)}) copy-start(f32[512]{0:T(512)} %param.28) | copy-start | bytes 6148

commit v6 on v5

--- a/solution.py
+++ b/solution.py
@@ -20,6 +20,10 @@
     return lax.all_to_all(parts, axes, split_axis=0, concat_axis=0, tiled=True)
 
 
+def from_partner(value):
+    return lax.ppermute(value, "core", [(0, 1), (1, 0)])
+
+
 def wide_dot(left, right):
     return jnp.dot(left, right, preferred_element_type=jnp.float32)
 
@@ -42,34 +46,85 @@
     return wide[0:1] + wide[1:2] + wide[2:3]
 
 
-def open_kernel(at, decay, hidden, lengths, mixer_gain, channel_gain, inverse, *refs):
-    sources = refs[: len(at)]
-    sent, joined, table, rows, gains, place, arrived = refs[len(at) :]
-    pairs = [
-        (hidden, rows),
-        (lengths, place),
-        (mixer_gain, gains.at[0:1]),
-        (channel_gain, gains.at[1:2]),
-    ]
-    for source, first in zip(sources, at):
-        for lanes in range(0, source.shape[1], LANES):
-            span = slice(first + lanes // LANES * source.shape[0], None)
-            span = slice(span.start, span.start + source.shape[0])
-            pairs.append((source.at[:, lanes : lanes + LANES], joined.at[span]))
+def store_gain(target, gain):
+    high, middle, low = (part.astype(jnp.float32) for part in thirds(gain))
+    row = lax.broadcasted_iota(jnp.int32, (GAIN_ROWS, LANES), 0)
+    block = jnp.where(row == 0, high, jnp.where(row == 1, middle, jnp.where(row == 2, low, 0.0)))
+    target[target.shape[0] - GAIN_ROWS :, :LANES] = block.astype(jnp.bfloat16)
+
+
+def started(pairs, arrived):
     moves = [
         pltpu.make_async_copy(source, target, arrived.at[i])
         for i, (source, target) in enumerate(pairs)
     ]
     for move in moves:
         move.start()
-    lane = lax.broadcasted_iota(jnp.int32, (1, LANES), 1)
-    for move in moves[:4]:
-        move.wait()
-    peers, half, _ = sent.shape
+    return moves
+
+
+def open_kernel(hidden, gain, *refs):
+    *sources, sent, joined, rows, own_gain, many, arrived = refs
+    pairs, at = [(hidden, rows), (gain, own_gain)], 0
+    for source in sources:
+        depth, columns = source.shape
+        pairs.append((source, joined.at[:depth, at : at + columns]))
+        at += columns
+    moves = started(pairs, arrived)
+    moves[0].wait()
+    peers, half, _ = many.shape
     wide = rows[...].astype(jnp.float32)
     for i in range(peers):
         first = half * (2 * i // peers)
-        sent[i] = wide[first : first + half].astype(jnp.bfloat16)
+        many[i] = wide[first : first + half].astype(jnp.bfloat16)
+    out = pltpu.make_async_copy(many, sent, arrived.at[len(moves)])
+    out.start()
+    moves[1].wait()
+    store_gain(joined, own_gain[...])
+    for move in moves[2:]:
+        move.wait()
+    out.wait()
+
+
+def held_in_hbm(*arrays):
+    return [pltpu.with_memory_space_constraint(array, pltpu.HBM) for array in arrays]
+
+
+def opening(hidden, gain, weights, peers):
+    many = (peers, hidden.shape[0] // 2, LANES)
+    joined = (LANES + GAIN_ROWS, sum(array.shape[1] for array in weights))
+    operands = held_in_hbm(hidden, gain[None], *weights)
+    return pl.pallas_call(
+        open_kernel,
+        out_shape=(
+            jax.ShapeDtypeStruct(many, jnp.bfloat16),
+            pltpu.VMEM(joined, jnp.bfloat16),
+        ),
+        in_specs=[IN_HBM] * len(operands),
+        out_specs=(IN_HBM, IN_VMEM),
+        scratch_shapes=[
+            pltpu.VMEM(hidden.shape, jnp.bfloat16),
+            pltpu.VMEM((1, LANES), jnp.float32),
+            pltpu.VMEM(many, jnp.bfloat16),
+            pltpu.SemaphoreType.DMA((len(operands) + 1,)),
+        ],
+        compiler_params=pltpu.CompilerParams(vmem_limit_bytes=8 << 20),
+        cost_estimate=pl.CostEstimate(flops=2_000_000, bytes_accessed=1_000_000, transcendentals=0),
+        name="opening",
+    )(*operands)
+
+
+def later_kernel(decay, inverse, lengths, gain, *refs):
+    *sources, joined, table, place, own_gain, arrived = refs
+    pairs, at = [(lengths, place), (gain, own_gain)], 0
+    for source in sources:
+        pairs.append((source, joined.at[at : at + source.shape[0]]))
+        at += source.shape[0]
+    moves = started(pairs, arrived)
+    lane = lax.broadcasted_iota(jnp.int32, (1, LANES), 1)
+    moves[0].wait()
+    moves[1].wait()
+    store_gain(joined, own_gain[...])
     seqs = place.shape[0]
     for i in range(seqs):
         angle = place[i].astype(jnp.float32) * inverse[...]
@@ -82,47 +137,31 @@
         )
         reach = (filled + 1 + 0 * lane).astype(jnp.float32)
         table[3 * seqs + i : 3 * seqs + i + 1] = jnp.exp(-decay[0] * reach)
-    row = lax.broadcasted_iota(jnp.int32, (GAIN_ROWS, LANES), 0)
-    end = joined.shape[0]
-    for i in range(2):
-        high, middle, low = (part.astype(jnp.float32) for part in thirds(gains[i : i + 1]))
-        block = jnp.where(row == 0, high, jnp.where(row == 1, middle, jnp.where(row == 2, low, 0.0)))
-        first = end - (2 - i) * GAIN_ROWS
-        joined[first : first + GAIN_ROWS] = block.astype(jnp.bfloat16)
-    for move in moves[4:]:
+    for move in moves[2:]:
         move.wait()
 
 
-def opening(hidden, lengths, decay, mixer_gain, channel_gain, weights, peers):
+def join_later(decay, lengths, gain, weights):
     inverse = 10000.0 ** (-jnp.arange(LANES, dtype=jnp.float32) / LANES)
-    at, end = [], 0
-    for array in weights:
-        at.append(end)
-        end += array.size // LANES
-    in_hbm = [
-        pltpu.with_memory_space_constraint(array, pltpu.HBM)
-        for array in (hidden, lengths, mixer_gain[None], channel_gain[None], *weights)
-    ]
-    pieces = sum(array.shape[1] // LANES for array in weights)
+    operands = held_in_hbm(lengths, gain[None], *weights)
+    depth = sum(array.shape[0] for array in weights) + GAIN_ROWS
     return pl.pallas_call(
-        functools.partial(open_kernel, at),
+        later_kernel,
         out_shape=(
-            jax.ShapeDtypeStruct((peers, hidden.shape[0] // 2, LANES), jnp.bfloat16),
-            pltpu.VMEM((end + 2 * GAIN_ROWS, LANES), jnp.bfloat16),
+            pltpu.VMEM((depth, LANES), jnp.bfloat16),
             pltpu.VMEM((4 * lengths.shape[0], LANES), jnp.float32),
         ),
-        in_specs=[IN_SMEM] + [IN_HBM] * 4 + [IN_VMEM] + [IN_HBM] * len(weights),
-        out_specs=(IN_VMEM, IN_VMEM, IN_VMEM),
+        in_specs=[IN_SMEM, IN_VMEM] + [IN_HBM] * len(operands),
+        out_specs=(IN_VMEM, IN_VMEM),
         scratch_shapes=[
-            pltpu.VMEM(hidden.shape, jnp.bfloat16),
-            pltpu.VMEM((2, LANES), jnp.float32),
             pltpu.SMEM(lengths.shape, jnp.int32),
-            pltpu.SemaphoreType.DMA((4 + pieces,)),
+            pltpu.VMEM((1, LANES), jnp.float32),
+            pltpu.SemaphoreType.DMA((len(operands),)),
         ],
         compiler_params=pltpu.CompilerParams(vmem_limit_bytes=8 << 20),
         cost_estimate=pl.CostEstimate(flops=2_000_000, bytes_accessed=1_000_000, transcendentals=0),
-        name="opening",
-    )(decay, *in_hbm[:4], inverse[None], *in_hbm[4:])
+        name="later",
+    )(decay, inverse[None], *operands)
 
 
 def rotated_by(vectors, cosine, sine):
@@ -178,7 +217,7 @@
     seqs, _, _, value_width = state.shape
     out_shape = jax.ShapeDtypeStruct((arrived.shape[0], seqs, value_width), jnp.bfloat16)
     operands = (arrived, table, state, keys, values, group_gain[None])
-    return call(retain_kernel, out_shape, operands, [], "retain")
+    return call(retain_kernel, out_shape, operands, [])
 
 
 def activate_kernel(units, pad, arrived, activated):
@@ -195,7 +234,7 @@
 def activate(arrived, units, pad):
     out_shape = jax.ShapeDtypeStruct((*arrived.shape[:2], units), jnp.bfloat16)
     kernel = functools.partial(activate_kernel, units, pad)
-    return call(kernel, out_shape, (arrived,), [], "activate")
+    return call(kernel, out_shape, (arrived,), [])
 
 
 def transposed_dot(left, right):
@@ -226,27 +265,19 @@
         stream[0, span] = arrived[side, i].astype(jnp.float32)
         stream[1, span] = arrived[1 - side, i].astype(jnp.float32)
     parts = [stream[i] for i in range(2)]
-    end = own.shape[0]
-    scaled = jnp.concatenate(
-        [
-            (part * from_thirds(weights[end - 2 * GAIN_ROWS : end - GAIN_ROWS])).astype(
-                jnp.bfloat16
-            )
-            for part, weights in zip(parts, (own, partner))
-        ],
-        axis=1,
-    )
-    for i in range(width // LANES):
-        span = slice(features * i, features * (i + 1))
-        columns = jnp.concatenate([own[span], partner[span]], axis=0)
-        wide[:, LANES * i : LANES * (i + 1)] = wide_dot(scaled, columns)
+    total = None
+    for part, weights in zip(parts, (own, partner)):
+        gain = from_thirds(weights[features : features + GAIN_ROWS, :features])
+        term = wide_dot((part * gain).astype(jnp.bfloat16), weights[:features])
+        total = term if total is None else total + term
+    wide[:, :width] = total
     squares = jnp.sum(parts[0] * parts[0] + parts[1] * parts[1], axis=1, keepdims=True)
     lane = lax.broadcasted_iota(jnp.int32, (rows, LANES), 1)
     wide[:, width:] = jnp.where(lane == 0, squares, 0.0)
     store_by_peer(terms, wide)
 
 
-def call(kernel, out_shape, operands, scratch, name):
+def call(kernel, out_shape, operands, scratch):
     return pl.pallas_call(
         kernel,
         out_shape=out_shape,
@@ -255,20 +286,19 @@
         scratch_shapes=scratch,
         compiler_params=pltpu.CompilerParams(vmem_limit_bytes=8 << 20),
         cost_estimate=pl.CostEstimate(flops=8_000_000, bytes_accessed=1_000_000, transcendentals=0),
-        name=name,
     )(*operands)
 
 
-def project(arrived, own, partner, width, z):
+def project(arrived, own, partner, z):
     _, kv, half, features = arrived.shape
     rows = kv * half
-    width = width + LANES
+    width = own.shape[1] + LANES
     out_shape = (
         jax.ShapeDtypeStruct((z, rows // z, width), jnp.bfloat16),
         jax.ShapeDtypeStruct((2, rows, features), jnp.float32),
     )
     scratch = [pltpu.VMEM((rows, width), jnp.float32)]
-    return call(project_kernel, out_shape, (arrived, own, partner), scratch, "project")
+    return call(project_kernel, out_shape, (arrived, own, partner), scratch)
 
 
 def mix_kernel(head, arrived, own, partner, terms, wide):
@@ -286,9 +316,7 @@
     rows = z * half
     out_shape = jax.ShapeDtypeStruct((kv, rows, 2 * LANES), jnp.bfloat16)
     scratch = [pltpu.VMEM((rows, width), jnp.float32)]
-    return call(
-        functools.partial(mix_kernel, head), out_shape, (arrived, own, partner), scratch, "mix"
-    )
+    return call(functools.partial(mix_kernel, head), out_shape, (arrived, own, partner), scratch)
 
 
 def finish_kernel(down, arrived, own, partner, residual, sent, wide):
@@ -314,7 +342,6 @@
         out_shape,
         (arrived, own, partner, residual),
         scratch,
-        "finish",
     )
 
 
@@ -366,7 +393,6 @@
         out_shape,
         (parts, stream, own_weights, partner),
         [pltpu.VMEM((rows, width), jnp.float32)],
-        "channel",
     )
 
 
@@ -393,30 +419,23 @@
     own_rows, features = hidden_in.shape
     half = own_rows // 2
     head_width, units = output_weight.shape[0], hidden_gate.shape[1]
-    weights = (
-        query_weight,
-        key_weight,
-        value_weight,
-        gate_weight,
-        output_weight,
-        hidden_gate.T,
-        hidden_up.T,
-        hidden_down,
-    )
-    width = sum(array.shape[1] for array in weights[:4])
-    inner = width + head_width
-    sent, own, table = opening(
-        hidden_in, lengths, decay_rate, mixer_gain, channel_gain, weights, 2 * kv
-    )
-    partner = lax.ppermute(own, "core", [(0, 1), (1, 0)])
+    sent, first = opening(
+        hidden_in, mixer_gain, (query_weight, key_weight, value_weight, gate_weight), 2 * kv
+    )
     rows = exchange(sent, ("core", "kv")).reshape(2, kv, half, features)
-    terms, stream = project(rows, own, partner, width, z)
-    mixed = retain(exchange(terms, "z"), table, prior_state, key_block, value_block, group_gain)
-    parts = exchange(mix(exchange(mixed, "z"), own, partner, width, kv), "kv")
-    terms, residual = channel(parts, stream, own, partner, inner, units, z)
+    first_partner = from_partner(first)
+    terms, stream = project(rows, first, first_partner, z)
+    arrived = exchange(terms, "z")
+    later = (output_weight, hidden_gate.T, hidden_up.T, hidden_down)
+    own, table = join_later(decay_rate, lengths, channel_gain, later)
+    partner = from_partner(own)
+    mixed = retain(arrived, table, prior_state, key_block, value_block, group_gain)
+    mixed = exchange(mixed, "z")
+    parts = exchange(mix(mixed, own, partner, 0, kv), "kv")
+    terms, residual = channel(parts, stream, own, partner, head_width, units, z)
     activated = activate(exchange(terms, "z"), units, -units % LANES)
     total = finish(
-        exchange(activated, "z"), own, partner, residual, inner + 2 * units, kv
+        exchange(activated, "z"), own, partner, residual, head_width + 2 * units, kv
     )
     total = exchange(total, ("core", "kv")).reshape(2, kv, half, features)
     return jnp.sum(total, axis=1).reshape(own_rows, features).astype(jnp.bfloat16)

time: 121 us -> 126 us (1.041)
  blocking collectives: 107 us -> 91.6 us
  waiting for transfers between devices: 0.01 us -> 11.5 us
  starting transfers between devices: 8.75 us -> 15.6 us
  Pallas kernels: 3.46 us -> 4.98 us
    all_to_all x7 -> x6, blocking collectives: 107 us -> 91.6 us  [exchange(): return lax.all_to_all(parts, axes, split_axis=0, concat_axis=0, tiled=True)]
    all_to_all x0 -> x1, waiting for transfers between devices: none -> 11.5 us  [exchange(): return lax.all_to_all(parts, axes, split_axis=0, concat_axis=0, tiled=True)]
    all_to_all x0 -> x1, starting transfers between devices: none -> 4.9 us  [exchange(): return lax.all_to_all(parts, axes, split_axis=0, concat_axis=0, tiled=True)]
    ppermute x1 -> x2, starting transfers between devices: 8.75 us -> 10.7 us  [from_partner(): return lax.ppermute(value, 'core', [(0, 1), (1, 0)])]
  transfers between devices with their start and end apart: 1 -> 3, of which waited for: 0 -> 1; matrix products, arithmetic and copies ran while one was open for 0% -> 0% of each run, Pallas kernels for 0% -> 2%
where the time goes in v6:
time: 126 us
  blocking collectives  91.6 us (73%)
  starting transfers between devices  15.6 us (12%)
  waiting for transfers between devices  11.5 us (9%)
  Pallas kernels  4.98 us (4%)
    all_to_all x6, blocking collectives, exchange(): return lax.all_to_all(parts, axes, split_axis=0, concat_axis=0, tiled=True)  91.6 us
    all_to_all x1, waiting for transfers between devices, exchange(): return lax.all_to_all(parts, axes, split_axis=0, concat_axis=0, tiled=True)  11.5 us
    ppermute x2, starting transfers between devices, from_partner(): return lax.ppermute(value, 'core', [(0, 1), (1, 0)])  10.7 us
    all_to_all x1, starting transfers between devices, exchange(): return lax.all_to_all(parts, axes, split_axis=0, concat_axis=0, tiled=True)  4.9 us
    pallas_call x6, Pallas kernels, call(): pl.pallas_call(kernel, out_shape=out_shape, in_specs=[IN_VMEM] * len(oper...  2.53 us
  transfers between devices with their start and end apart: 3, of which 1 were waited for; matrix products, arithmetic and copies ran while one was open for 0% of the time, Pallas kernels for 2%

profile of v6, /device:TPU:1, one launch (start us, length us, event | category | flops | bytes accessed | tf_op | source)
XLA Modules:
  0.0 125.7 jit_solution(14430132975076547979)
XLA Ops:
  0.0 0.0 copy-start
  0.0 1.2 opening.1
  1.2 8.7 %collective-permute-start = (bf16[144,1536]{1,0:T(8,128)(2,1)S(1)}, bf16[144,1536]{1,0:T(8,128)(2,1)S(1)}, u32[]{:S(2)}, u32[]{:S(2)}) collective-permute-start(bf16[144,1536]{1,0:T(8,128)(2,1)S(1)} %get-tuple-element.14.own), channel_id=1, source_target_pairs={{0,1},{1,0},{2,3},{3,2},{4,5},{5,4},{6,7},{7,6},{8,9},{9,8},{10,11... | collective-permute-start | bytes 1327112 | tf_op jit(solution)/shard_map/ppermute | solution.py:24
  10.6 1.2 later.1
  11.9 1.9 %collective-permute-start.1 = (bf16[2640,128]{1,0:T(8,128)(2,1)S(1)}, bf16[2640,128]{1,0:T(8,128)(2,1)S(1)}, u32[]{:S(2)}, u32[]{:S(2)}) collective-permute-start(bf16[2640,128]{1,0:T(8,128)(2,1)S(1)} %get-tuple-element.17.own.own_weights), channel_id=1, source_target_pairs={{0,1},{1,0},{2,3},{3,2},{4,5},{5,4},{6,7},{7,6},{8,9},{9,8},{10,11... | collective-permute-start | bytes 2027528 | tf_op jit(solution)/shard_map/ppermute | solution.py:24
  13.8 10.1 %all_to_all.35 = bf16[32,2,128]{2,1,0:T(2,128)(2,1)S(1)} all-to-all(bf16[32,2,128]{2,1,0:T(2,128)(2,1)S(1)} %get-tuple-element.13), channel_id=1, replica_groups=mesh['kv'=16,'z'=16,'core'=2] {'core','kv'}, dimensions={0} | all-to-all | bytes 32768 | tf_op jit(solution)/shard_map/all_to_all | solution.py:20
  23.9 0.0 collective-permute-done.partner
  23.9 0.0 copy-start.1
  23.9 0.3 shard_map.163
  24.2 0.0 copy-start.2
  24.2 25.6 %all_to_all.36.arrived = bf16[16,2,1664]{2,1,0:T(2,128)(2,1)S(1)} all-to-all(bf16[16,2,1664]{2,1,0:T(2,128)(2,1)S(1)} %get-tuple-element.15), channel_id=1, replica_groups=mesh['kv'=16,'z'=16,'core'=2] {'z'}, dimensions={0} | all-to-all | bytes 212992 | tf_op jit(solution)/shard_map/all_to_all | solution.py:20
  49.7 0.0 copy-start.3
  49.7 0.0 copy-done
  49.7 0.0 copy-done.1
  49.7 0.0 copy-done.2
  49.7 0.7 copy-done.3
  50.4 1.3 %shard_map.164 = bf16[16,2,512]{2,1,0:T(2,128)(2,1)} custom-call(bf16[16,2,1664]{2,1,0:T(2,128)(2,1)S(1)} %all_to_all.36.arrived, f32[8,128]{1,0:T(8,128)S(1)} %get-tuple-element.16.table, f32[2,1,256,512]{3,2,1,0:T(8,128)S(1)} %copy-done, bf16[2,1,128,256]{3,2,1,0:T(8,128)(2,1)S(1)} %copy-done.2, bf16[2,1,128,512]{3,2,1,0:T(8,128)(2,1)S(1)} %copy-done.1, ...), custom_call_target="tpu_custom_call" | custom-call | flops 8000000 | bytes 1000000 | tf_op jit(solution)/shard_map/pallas_call | solution.py:281
  51.7 4.9 %all-to-all-start.2 = ((bf16[16,2,512]{2,1,0:T(2,128)(2,1)}), bf16[16,2,512]{2,1,0:T(2,128)(2,1)S(1)}, u32[]{:S(2)}, u32[]{:S(2)}) async-start(bf16[16,2,512]{2,1,0:T(2,128)(2,1)} %shard_map.164), calls=%async_computation.2 | async-start | bytes 65536 | tf_op jit(solution)/shard_map/all_to_all | solution.py:20
  56.6 0.0 collective-permute-done.1.partner
  56.6 11.5 %all-to-all-done.2.arrived = bf16[16,2,512]{2,1,0:T(2,128)(2,1)S(1)} async-done(((bf16[16,2,512]{2,1,0:T(2,128)(2,1)}), bf16[16,2,512]{2,1,0:T(2,128)(2,1)S(1)}, u32[]{:S(2)}, u32[]{:S(2)}) %all-to-all-start.2) | async-done | bytes 32800 | tf_op jit(solution)/shard_map/all_to_all | solution.py:20
  68.1 0.2 shard_map.165
  68.3 10.4 %all_to_all.37.parts = bf16[16,32,256]{2,1,0:T(8,128)(2,1)S(1)} all-to-all(bf16[16,32,256]{2,1,0:T(8,128)(2,1)S(1)} %shard_map.165), channel_id=1, replica_groups=mesh['kv'=16,'z'=16,'core'=2] {'kv'}, dimensions={0} | all-to-all | bytes 524288 | tf_op jit(solution)/shard_map/all_to_all | solution.py:20
  78.7 0.4 shard_map.166
  79.1 14.3 %all_to_all.38.arrived = bf16[16,2,1472]{2,1,0:T(2,128)(2,1)S(1)} all-to-all(bf16[16,2,1472]{2,1,0:T(2,128)(2,1)S(1)} %get-tuple-element.19), channel_id=1, replica_groups=mesh['kv'=16,'z'=16,'core'=2] {'z'}, dimensions={0} | all-to-all | bytes 188416 | tf_op jit(solution)/shard_map/all_to_all | solution.py:20
  93.5 0.2 shard_map.167
  93.7 14.9 %all_to_all.39.arrived = bf16[16,2,704]{2,1,0:T(2,128)(2,1)S(1)} all-to-all(bf16[16,2,704]{2,1,0:T(2,128)(2,1)S(1)} %shard_map.167), channel_id=1, replica_groups=mesh['kv'=16,'z'=16,'core'=2] {'z'}, dimensions={0} | all-to-all | bytes 90112 | tf_op jit(solution)/shard_map/all_to_all | solution.py:20
  108.5 0.2 shard_map.168
  108.8 16.3 %all_to_all.40 = f32[32,2,128]{2,1,0:T(2,128)S(1)} all-to-all(f32[32,2,128]{2,1,0:T(2,128)S(1)} %shard_map.168), channel_id=1, replica_groups=mesh['kv'=16,'z'=16,'core'=2] {'core','kv'}, dimensions={0} | all-to-all | bytes 65536 | tf_op jit(solution)/shard_map/all_to_all | solution.py:20
  125.1 0.6 bitcast_reduce_fusion
  (1 shorter events, 0.0 us)
Async XLA Ops:
  0.0 49.7 %copy-start = (f32[2,1,256,512]{3,2,1,0:T(8,128)S(1)}, f32[2,1,256,512]{3,2,1,0:T(8,128)}, u32[]{:S(2)}) copy-start(f32[2,1,256,512]{3,2,1,0:T(8,128)} %state.1) | copy-start | bytes 3145732
  1.2 22.7 %collective-permute-start = (bf16[144,1536]{1,0:T(8,128)(2,1)S(1)}, bf16[144,1536]{1,0:T(8,128)(2,1)S(1)}, u32[]{:S(2)}, u32[]{:S(2)}) collective-permute-start(bf16[144,1536]{1,0:T(8,128)(2,1)S(1)} %get-tuple-element.14.own), channel_id=1, source_target_pairs={{0,1},{1,0},{2,3},{3,2},{4,5},{5,4},{6,7},{7,6},{8,9},{9,8},{10,11... | collective-permute-start | bytes 1327112 | tf_op jit(solution)/shard_map/ppermute | solution.py:24
  11.9 44.7 %collective-permute-start.1 = (bf16[2640,128]{1,0:T(8,128)(2,1)S(1)}, bf16[2640,128]{1,0:T(8,128)(2,1)S(1)}, u32[]{:S(2)}, u32[]{:S(2)}) collective-permute-start(bf16[2640,128]{1,0:T(8,128)(2,1)S(1)} %get-tuple-element.17.own.own_weights), channel_id=1, source_target_pairs={{0,1},{1,0},{2,3},{3,2},{4,5},{5,4},{6,7},{7,6},{8,9},{9,8},{10,11... | collective-permute-start | bytes 2027528 | tf_op jit(solution)/shard_map/ppermute | solution.py:24
  23.9 25.9 %copy-start.1 = (bf16[2,1,128,512]{3,2,1,0:T(8,128)(2,1)S(1)}, bf16[2,1,128,512]{3,2,1,0:T(8,128)(2,1)}, u32[]{:S(2)}) copy-start(bf16[2,1,128,512]{3,2,1,0:T(8,128)(2,1)} %values.1) | copy-start | bytes 786436
  24.2 25.6 %copy-start.2 = (bf16[2,1,128,256]{3,2,1,0:T(8,128)(2,1)S(1)}, bf16[2,1,128,256]{3,2,1,0:T(8,128)(2,1)}, u32[]{:S(2)}) copy-start(bf16[2,1,128,256]{3,2,1,0:T(8,128)(2,1)} %keys.1) | copy-start | bytes 393220
  49.7 0.7 copy-start.3
  51.7 16.4 %all-to-all-start.2 = ((bf16[16,2,512]{2,1,0:T(2,128)(2,1)}), bf16[16,2,512]{2,1,0:T(2,128)(2,1)S(1)}, u32[]{:S(2)}, u32[]{:S(2)}) async-start(bf16[16,2,512]{2,1,0:T(2,128)(2,1)} %shard_map.164), calls=%async_computation.2 | async-start | bytes 65536 | tf_op jit(solution)/shard_map/all_to_all | solution.py:20

commit v7 on v6

--- a/solution.py
+++ b/solution.py
@@ -11,13 +11,21 @@
 D = 4096
 LANES = 128
 BLOCK = 128
+FIRST_KV = 10
+FIRST_Z = 8
 
 
 epsilon = 1e-06
 
 
-def exchange(parts, axes):
-    return lax.all_to_all(parts, axes, split_axis=0, concat_axis=0, tiled=True)
+def exchange(parts, axes, order):
+    return lax.all_to_all(
+        parts, axes, split_axis=0, concat_axis=0, axis_index_groups=[order], tiled=True
+    )
+
+
+def turned(count, first):
+    return [(member + first) % count for member in range(count)]
 
 
 def from_partner(value):
@@ -262,8 +270,9 @@
     side = lax.axis_index("core")
     for i in range(rows // half):
         span = slice(half * i, half * (i + 1))
-        stream[0, span] = arrived[side, i].astype(jnp.float32)
-        stream[1, span] = arrived[1 - side, i].astype(jnp.float32)
+        source = (i + FIRST_Z - FIRST_KV) % (rows // half)
+        stream[0, span] = arrived[side, source].astype(jnp.float32)
+        stream[1, span] = arrived[1 - side, source].astype(jnp.float32)
     parts = [stream[i] for i in range(2)]
     total = None
     for part, weights in zip(parts, (own, partner)):
@@ -329,7 +338,8 @@
         total = wide_dot(every, weights[span]) + residual[i]
         to = side if i == 0 else 1 - side
         for peer in range(peers // 2):
-            sent[to * (peers // 2) + peer] = total[half * peer : half * (peer + 1)]
+            at = half * ((peer + FIRST_KV - FIRST_Z) % (peers // 2))
+            sent[to * (peers // 2) + peer] = total[at : at + half]
 
 
 def finish(arrived, own, partner, residual, down, kv):
@@ -375,7 +385,8 @@
     )
     store_by_peer(terms, wide)
     row = lax.broadcasted_iota(jnp.int32, (rows, features), 0)
-    here = row // half == lax.axis_index("kv")
+    peers = rows // half
+    here = lax.rem(row // half + FIRST_Z, peers) == lax.axis_index("kv")
     residual[0] = jnp.where(here, own, 0.0)
     residual[1] = jnp.where(here, other, 0.0)
 
@@ -419,25 +430,27 @@
     own_rows, features = hidden_in.shape
     half = own_rows // 2
     head_width, units = output_weight.shape[0], hidden_gate.shape[1]
+    line = turned(z, FIRST_Z)
+    plane = [side * kv + member for side in range(2) for member in turned(kv, FIRST_KV)]
     sent, first = opening(
         hidden_in, mixer_gain, (query_weight, key_weight, value_weight, gate_weight), 2 * kv
     )
-    rows = exchange(sent, ("core", "kv")).reshape(2, kv, half, features)
+    rows = exchange(sent, ("core", "kv"), plane).reshape(2, kv, half, features)
     first_partner = from_partner(first)
     terms, stream = project(rows, first, first_partner, z)
-    arrived = exchange(terms, "z")
+    arrived = exchange(terms, "z", line)
     later = (output_weight, hidden_gate.T, hidden_up.T, hidden_down)
     own, table = join_later(decay_rate, lengths, channel_gain, later)
     partner = from_partner(own)
     mixed = retain(arrived, table, prior_state, key_block, value_block, group_gain)
-    mixed = exchange(mixed, "z")
-    parts = exchange(mix(mixed, own, partner, 0, kv), "kv")
+    mixed = exchange(mixed, "z", line)
+    parts = exchange(mix(mixed, own, partner, 0, kv), "kv", turned(kv, FIRST_KV))
     terms, residual = channel(parts, stream, own, partner, head_width, units, z)
-    activated = activate(exchange(terms, "z"), units, -units % LANES)
+    activated = activate(exchange(terms, "z", line), units, -units % LANES)
     total = finish(
-        exchange(activated, "z"), own, partner, residual, head_width + 2 * units, kv
-    )
-    total = exchange(total, ("core", "kv")).reshape(2, kv, half, features)
+        exchange(activated, "z", line), own, partner, residual, head_width + 2 * units, kv
+    )
+    total = exchange(total, ("core", "kv"), plane).reshape(2, kv, half, features)
     return jnp.sum(total, axis=1).reshape(own_rows, features).astype(jnp.bfloat16)
 
 

time: 126 us -> 117 us (0.929)
  waiting for transfers between devices: 11.5 us -> 2.43 us
  blocking collectives: 91.6 us -> 84.9 us
  starting transfers between devices: 15.6 us -> 22.1 us
    all_to_all x1, waiting for transfers between devices: 11.5 us -> 2.43 us  [exchange(): lax.all_to_all(parts, axes, split_axis=0, concat_axis=0, axis_index_group...]
    all_to_all x6, blocking collectives: 91.6 us -> 84.9 us  [exchange(): lax.all_to_all(parts, axes, split_axis=0, concat_axis=0, axis_index_group...]
    all_to_all x1, starting transfers between devices: 4.9 us -> 11.5 us  [exchange(): lax.all_to_all(parts, axes, split_axis=0, concat_axis=0, axis_index_group...]
where the time goes in v7:
time: 117 us; the launch traced here: 116 us
  blocking collectives  84.9 us (73%)
  starting transfers between devices  22.1 us (19%)
  Pallas kernels  4.98 us (4%)
  waiting for transfers between devices  2.43 us (2%)
    all_to_all x6, blocking collectives, exchange(): lax.all_to_all(parts, axes, split_axis=0, concat_axis=0, axis_index_group...  84.9 us
    all_to_all x1, starting transfers between devices, exchange(): lax.all_to_all(parts, axes, split_axis=0, concat_axis=0, axis_index_group...  11.5 us
    ppermute x2, starting transfers between devices, from_partner(): return lax.ppermute(value, 'core', [(0, 1), (1, 0)])  10.7 us
    pallas_call x6, Pallas kernels, call(): pl.pallas_call(kernel, out_shape=out_shape, in_specs=[IN_VMEM] * len(oper...  2.54 us
    all_to_all x1, waiting for transfers between devices, exchange(): lax.all_to_all(parts, axes, split_axis=0, concat_axis=0, axis_index_group...  2.43 us
  transfers between devices with their start and end apart: 3, of which 1 were waited for; matrix products, arithmetic and copies ran while one was open for 0% of the time, Pallas kernels for 2%

profile of v7, /device:TPU:1, one launch (start us, length us, event | category | flops | bytes accessed | tf_op | source)
XLA Modules:
  0.0 116.4 jit_solution(1447340772378711560)
XLA Ops:
  0.0 0.0 copy-start
  0.0 1.2 %opening.1 = (bf16[32,2,128]{2,1,0:T(2,128)(2,1)S(1)}, bf16[144,1536]{1,0:T(8,128)(2,1)S(1)}) custom-call(bf16[4,128]{1,0:T(4,128)(2,1)} %hidden.1, f32[1,128]{1,0:T(1,128)} %bitcast.13, bf16[128,256]{1,0:T(8,128)(2,1)} %refs_0_.2, bf16[128,256]{1,0:T(8,128)(2,1)} %refs_1_.1, bf16[128,512]{1,0:T(8,128)(2,1)} %refs_2_.1, bf16[128,512]{1,0:T(8,128)(2,1)} %refs_3_.2), custom_call_target="tpu_custom_call" | custom-call | flops 2000000 | bytes 1000000 | tf_op jit(solution)/shard_map/opening/pallas_call | solution.py:105
  1.2 8.7 %collective-permute-start = (bf16[144,1536]{1,0:T(8,128)(2,1)S(1)}, bf16[144,1536]{1,0:T(8,128)(2,1)S(1)}, u32[]{:S(2)}, u32[]{:S(2)}) collective-permute-start(bf16[144,1536]{1,0:T(8,128)(2,1)S(1)} %get-tuple-element.14.own), channel_id=1, source_target_pairs={{0,1},{1,0},{2,3},{3,2},{4,5},{5,4},{6,7},{7,6},{8,9},{9,8},{10,11... | collective-permute-start | bytes 1327112 | tf_op jit(solution)/shard_map/ppermute | solution.py:32
  10.6 1.2 %later.1 = (bf16[2640,128]{1,0:T(8,128)(2,1)S(1)}, f32[8,128]{1,0:T(8,128)S(1)}) custom-call(f32[1]{0:T(128)S(6)} %copy.18.decay, f32[1,128]{1,0:T(1,128)S(1)} %multiply_power_fusion.inverse, s32[2]{0:T(128)} %lengths.1, f32[1,128]{1,0:T(1,128)} %bitcast.14, bf16[512,128]{1,0:T(8,128)(2,1)} %refs_0_.3, bf16[704,128]{1,0:T(8,128)(2,1)} %bitcast.11, ...), custom_call_target="tpu_custom_call" | custom-call | flops 2000000 | bytes 1000000 | tf_op jit(solution)/shard_map/later/pallas_call | solution.py:156
  11.9 1.9 %collective-permute-start.1 = (bf16[2640,128]{1,0:T(8,128)(2,1)S(1)}, bf16[2640,128]{1,0:T(8,128)(2,1)S(1)}, u32[]{:S(2)}, u32[]{:S(2)}) collective-permute-start(bf16[2640,128]{1,0:T(8,128)(2,1)S(1)} %get-tuple-element.17.own.own_weights), channel_id=1, source_target_pairs={{0,1},{1,0},{2,3},{3,2},{4,5},{5,4},{6,7},{7,6},{8,9},{9,8},{10,11... | collective-permute-start | bytes 2027528 | tf_op jit(solution)/shard_map/ppermute | solution.py:32
  13.8 9.3 %all_to_all.35 = bf16[32,2,128]{2,1,0:T(2,128)(2,1)S(1)} all-to-all(bf16[32,2,128]{2,1,0:T(2,128)(2,1)S(1)} %get-tuple-element.13), channel_id=1, replica_groups={{320,352,384,416,448,480,0,32,64,96,128,160,192,224,256,288,321,353,385..., dimensions={0} | all-to-all | bytes 32768 | tf_op jit(solution)/shard_map/all_to_all | solution.py:22
  23.1 0.0 collective-permute-done.partner
  23.1 0.0 copy-start.1
  23.1 0.3 shard_map.163
  23.4 0.0 copy-start.2
  23.4 19.9 %all_to_all.36.arrived = bf16[16,2,1664]{2,1,0:T(2,128)(2,1)S(1)} all-to-all(bf16[16,2,1664]{2,1,0:T(2,128)(2,1)S(1)} %get-tuple-element.15), channel_id=1, replica_groups={{16,18,20,22,24,26,28,30,0,2,4,6,8,10,12,14},{17,19,21,23,25,27,29,31,1..., dimensions={0} | all-to-all | bytes 212992 | tf_op jit(solution)/shard_map/all_to_all | solution.py:22
  43.3 0.0 copy-start.3
  43.3 0.0 copy-done
  43.3 0.0 copy-done.1
  43.3 0.0 copy-done.2
  43.3 0.7 copy-done.3
  44.0 1.3 %shard_map.164 = bf16[16,2,512]{2,1,0:T(2,128)(2,1)} custom-call(bf16[16,2,1664]{2,1,0:T(2,128)(2,1)S(1)} %all_to_all.36.arrived, f32[8,128]{1,0:T(8,128)S(1)} %get-tuple-element.16.table, f32[2,1,256,512]{3,2,1,0:T(8,128)S(1)} %copy-done, bf16[2,1,128,256]{3,2,1,0:T(8,128)(2,1)S(1)} %copy-done.2, bf16[2,1,128,512]{3,2,1,0:T(8,128)(2,1)S(1)} %copy-done.1, ...), custom_call_target="tpu_custom_call" | custom-call | flops 8000000 | bytes 1000000 | tf_op jit(solution)/shard_map/pallas_call | solution.py:290
  45.3 11.5 %all-to-all-start.2 = ((bf16[16,2,512]{2,1,0:T(2,128)(2,1)}), bf16[16,2,512]{2,1,0:T(2,128)(2,1)S(1)}, u32[]{:S(2)}, u32[]{:S(2)}) async-start(bf16[16,2,512]{2,1,0:T(2,128)(2,1)} %shard_map.164), calls=%async_computation.2 | async-start | bytes 65536 | tf_op jit(solution)/shard_map/all_to_all | solution.py:22
  56.8 0.0 collective-permute-done.1.partner
  56.8 2.4 %all-to-all-done.2.arrived = bf16[16,2,512]{2,1,0:T(2,128)(2,1)S(1)} async-done(((bf16[16,2,512]{2,1,0:T(2,128)(2,1)}), bf16[16,2,512]{2,1,0:T(2,128)(2,1)S(1)}, u32[]{:S(2)}, u32[]{:S(2)}) %all-to-all-start.2) | async-done | bytes 32800 | tf_op jit(solution)/shard_map/all_to_all | solution.py:22
  59.2 0.2 shard_map.165
  59.4 10.4 %all_to_all.37.parts = bf16[16,32,256]{2,1,0:T(8,128)(2,1)S(1)} all-to-all(bf16[16,32,256]{2,1,0:T(8,128)(2,1)S(1)} %shard_map.165), channel_id=1, replica_groups={{320,352,384,416,448,480,0,32,64,96,128,160,192,224,256,288},{321,353,3..., dimensions={0} | all-to-all | bytes 524288 | tf_op jit(solution)/shard_map/all_to_all | solution.py:22
  69.8 0.4 shard_map.166
  70.2 15.3 %all_to_all.38.arrived = bf16[16,2,1472]{2,1,0:T(2,128)(2,1)S(1)} all-to-all(bf16[16,2,1472]{2,1,0:T(2,128)(2,1)S(1)} %get-tuple-element.19), channel_id=1, replica_groups={{16,18,20,22,24,26,28,30,0,2,4,6,8,10,12,14},{17,19,21,23,25,27,29,31,1..., dimensions={0} | all-to-all | bytes 188416 | tf_op jit(solution)/shard_map/all_to_all | solution.py:22
  85.5 0.2 shard_map.167
  85.7 13.8 %all_to_all.39.arrived = bf16[16,2,704]{2,1,0:T(2,128)(2,1)S(1)} all-to-all(bf16[16,2,704]{2,1,0:T(2,128)(2,1)S(1)} %shard_map.167), channel_id=1, replica_groups={{16,18,20,22,24,26,28,30,0,2,4,6,8,10,12,14},{17,19,21,23,25,27,29,31,1..., dimensions={0} | all-to-all | bytes 90112 | tf_op jit(solution)/shard_map/all_to_all | solution.py:22
  99.5 0.2 shard_map.168
  99.7 16.2 %all_to_all.40 = f32[32,2,128]{2,1,0:T(2,128)S(1)} all-to-all(f32[32,2,128]{2,1,0:T(2,128)S(1)} %shard_map.168), channel_id=1, replica_groups={{320,352,384,416,448,480,0,32,64,96,128,160,192,224,256,288,321,353,385..., dimensions={0} | all-to-all | bytes 65536 | tf_op jit(solution)/shard_map/all_to_all | solution.py:22
  115.8 0.6 bitcast_reduce_fusion
  (1 shorter events, 0.0 us)
Async XLA Ops:
  0.0 43.3 %copy-start = (f32[2,1,256,512]{3,2,1,0:T(8,128)S(1)}, f32[2,1,256,512]{3,2,1,0:T(8,128)}, u32[]{:S(2)}) copy-start(f32[2,1,256,512]{3,2,1,0:T(8,128)} %state.1) | copy-start | bytes 3145732
  1.2 21.9 %collective-permute-start = (bf16[144,1536]{1,0:T(8,128)(2,1)S(1)}, bf16[144,1536]{1,0:T(8,128)(2,1)S(1)}, u32[]{:S(2)}, u32[]{:S(2)}) collective-permute-start(bf16[144,1536]{1,0:T(8,128)(2,1)S(1)} %get-tuple-element.14.own), channel_id=1, source_target_pairs={{0,1},{1,0},{2,3},{3,2},{4,5},{5,4},{6,7},{7,6},{8,9},{9,8},{10,11... | collective-permute-start | bytes 1327112 | tf_op jit(solution)/shard_map/ppermute | solution.py:32
  11.9 44.9 %collective-permute-start.1 = (bf16[2640,128]{1,0:T(8,128)(2,1)S(1)}, bf16[2640,128]{1,0:T(8,128)(2,1)S(1)}, u32[]{:S(2)}, u32[]{:S(2)}) collective-permute-start(bf16[2640,128]{1,0:T(8,128)(2,1)S(1)} %get-tuple-element.17.own.own_weights), channel_id=1, source_target_pairs={{0,1},{1,0},{2,3},{3,2},{4,5},{5,4},{6,7},{7,6},{8,9},{9,8},{10,11... | collective-permute-start | bytes 2027528 | tf_op jit(solution)/shard_map/ppermute | solution.py:32
  23.1 20.2 %copy-start.1 = (bf16[2,1,128,512]{3,2,1,0:T(8,128)(2,1)S(1)}, bf16[2,1,128,512]{3,2,1,0:T(8,128)(2,1)}, u32[]{:S(2)}) copy-start(bf16[2,1,128,512]{3,2,1,0:T(8,128)(2,1)} %values.1) | copy-start | bytes 786436
  23.4 20.0 %copy-start.2 = (bf16[2,1,128,256]{3,2,1,0:T(8,128)(2,1)S(1)}, bf16[2,1,128,256]{3,2,1,0:T(8,128)(2,1)}, u32[]{:S(2)}) copy-start(bf16[2,1,128,256]{3,2,1,0:T(8,128)(2,1)} %keys.1) | copy-start | bytes 393220
  43.3 0.7 copy-start.3
  45.3 13.9 %all-to-all-start.2 = ((bf16[16,2,512]{2,1,0:T(2,128)(2,1)}), bf16[16,2,512]{2,1,0:T(2,128)(2,1)S(1)}, u32[]{:S(2)}, u32[]{:S(2)}) async-start(bf16[16,2,512]{2,1,0:T(2,128)(2,1)} %shard_map.164), calls=%async_computation.2 | async-start | bytes 65536 | tf_op jit(solution)/shard_map/all_to_all | solution.py:22

commit v8 on v7

--- a/solution.py
+++ b/solution.py
@@ -11,8 +11,9 @@
 D = 4096
 LANES = 128
 BLOCK = 128
-FIRST_KV = 10
-FIRST_Z = 8
+SPREAD_AT, SUM_AT, RETURN_AT = 10, 10, 10
+HEADS_AT, MIXED_AT, UNITS_AT, ACTIVE_AT = 9, 9, 9, 9
+SPREAD_SIDES, RETURN_SIDES = (1, 0), (0, 1)
 
 
 epsilon = 1e-06
@@ -83,7 +84,7 @@
     peers, half, _ = many.shape
     wide = rows[...].astype(jnp.float32)
     for i in range(peers):
-        first = half * (2 * i // peers)
+        first = half * SPREAD_SIDES[2 * i // peers]
         many[i] = wide[first : first + half].astype(jnp.bfloat16)
     out = pltpu.make_async_copy(many, sent, arrived.at[len(moves)])
     out.start()
@@ -251,16 +252,18 @@
     )
 
 
-def store_by_peer(terms, wide):
-    half = terms.shape[1]
-    for i in range(terms.shape[0]):
-        terms[i] = wide[half * i : half * (i + 1)].astype(jnp.bfloat16)
-
-
-def gathered_rows(arrived, wide):
-    half = arrived.shape[1]
-    for i in range(arrived.shape[0]):
-        wide[half * i : half * (i + 1)] = arrived[i].astype(jnp.float32)
+def store_by_peer(terms, wide, first):
+    peers, half, _ = terms.shape
+    for i in range(peers):
+        at = half * ((i + first) % peers)
+        terms[i] = wide[at : at + half].astype(jnp.bfloat16)
+
+
+def gathered_rows(arrived, wide, first):
+    peers, half, _ = arrived.shape
+    for i in range(peers):
+        at = half * ((i + first) % peers)
+        wide[at : at + half] = arrived[i].astype(jnp.float32)
 
 
 def project_kernel(arrived, own, partner, terms, stream, wide):
@@ -268,11 +271,12 @@
     half = terms.shape[1]
     width = wide.shape[1] - LANES
     side = lax.axis_index("core")
+    place = side if SPREAD_SIDES[0] == 0 else 1 - side
     for i in range(rows // half):
         span = slice(half * i, half * (i + 1))
-        source = (i + FIRST_Z - FIRST_KV) % (rows // half)
-        stream[0, span] = arrived[side, source].astype(jnp.float32)
-        stream[1, span] = arrived[1 - side, source].astype(jnp.float32)
+        source = (i - SPREAD_AT) % (rows // half)
+        stream[0, span] = arrived[place, source].astype(jnp.float32)
+        stream[1, span] = arrived[1 - place, source].astype(jnp.float32)
     parts = [stream[i] for i in range(2)]
     total = None
     for part, weights in zip(parts, (own, partner)):
@@ -283,7 +287,7 @@
     squares = jnp.sum(parts[0] * parts[0] + parts[1] * parts[1], axis=1, keepdims=True)
     lane = lax.broadcasted_iota(jnp.int32, (rows, LANES), 1)
     wide[:, width:] = jnp.where(lane == 0, squares, 0.0)
-    store_by_peer(terms, wide)
+    store_by_peer(terms, wide, HEADS_AT)
 
 
 def call(kernel, out_shape, operands, scratch):
@@ -311,7 +315,7 @@
 
 
 def mix_kernel(head, arrived, own, partner, terms, wide):
-    gathered_rows(arrived, wide)
+    gathered_rows(arrived, wide, MIXED_AT)
     every = wide[...].astype(jnp.bfloat16)
     span = slice(head, head + wide.shape[1])
     both = jnp.concatenate([wide_dot(every, own[span]), wide_dot(every, partner[span])], axis=1)
@@ -329,16 +333,17 @@
 
 
 def finish_kernel(down, arrived, own, partner, residual, sent, wide):
-    gathered_rows(arrived, wide)
+    gathered_rows(arrived, wide, ACTIVE_AT)
     every = wide[...].astype(jnp.bfloat16)
     span = slice(down, down + wide.shape[1])
     side = lax.axis_index("core")
+    place = side if RETURN_SIDES[0] == 0 else 1 - side
     peers, half, _ = sent.shape
     for i, weights in enumerate((own, partner)):
         total = wide_dot(every, weights[span]) + residual[i]
-        to = side if i == 0 else 1 - side
+        to = place if i == 0 else 1 - place
         for peer in range(peers // 2):
-            at = half * ((peer + FIRST_KV - FIRST_Z) % (peers // 2))
+            at = half * ((peer + RETURN_AT) % (peers // 2))
             sent[to * (peers // 2) + peer] = total[at : at + half]
 
 
@@ -383,10 +388,9 @@
     ) + transposed_dot(
         scaled_other, partner[head + units : head + 2 * units]
     )
-    store_by_peer(terms, wide)
+    store_by_peer(terms, wide, UNITS_AT)
     row = lax.broadcasted_iota(jnp.int32, (rows, features), 0)
-    peers = rows // half
-    here = lax.rem(row // half + FIRST_Z, peers) == lax.axis_index("kv")
+    here = row // half == lax.axis_index("kv")
     residual[0] = jnp.where(here, own, 0.0)
     residual[1] = jnp.where(here, other, 0.0)
 
@@ -430,27 +434,30 @@
     own_rows, features = hidden_in.shape
     half = own_rows // 2
     head_width, units = output_weight.shape[0], hidden_gate.shape[1]
-    line = turned(z, FIRST_Z)
-    plane = [side * kv + member for side in range(2) for member in turned(kv, FIRST_KV)]
+    spread, back = (
+        [side * kv + member for side in sides for member in turned(kv, first)]
+        for sides, first in ((SPREAD_SIDES, SPREAD_AT), (RETURN_SIDES, RETURN_AT))
+    )
     sent, first = opening(
         hidden_in, mixer_gain, (query_weight, key_weight, value_weight, gate_weight), 2 * kv
     )
-    rows = exchange(sent, ("core", "kv"), plane).reshape(2, kv, half, features)
+    rows = exchange(sent, ("core", "kv"), spread).reshape(2, kv, half, features)
     first_partner = from_partner(first)
     terms, stream = project(rows, first, first_partner, z)
-    arrived = exchange(terms, "z", line)
+    arrived = exchange(terms, "z", turned(z, HEADS_AT))
     later = (output_weight, hidden_gate.T, hidden_up.T, hidden_down)
     own, table = join_later(decay_rate, lengths, channel_gain, later)
     partner = from_partner(own)
     mixed = retain(arrived, table, prior_state, key_block, value_block, group_gain)
-    mixed = exchange(mixed, "z", line)
-    parts = exchange(mix(mixed, own, partner, 0, kv), "kv", turned(kv, FIRST_KV))
+    mixed = exchange(mixed, "z", turned(z, MIXED_AT))
+    parts = exchange(mix(mixed, own, partner, 0, kv), "kv", turned(kv, SUM_AT))
     terms, residual = channel(parts, stream, own, partner, head_width, units, z)
-    activated = activate(exchange(terms, "z", line), units, -units % LANES)
+    activated = activate(exchange(terms, "z", turned(z, UNITS_AT)), units, -units % LANES)
     total = finish(
-        exchange(activated, "z", line), own, partner, residual, head_width + 2 * units, kv
-    )
-    total = exchange(total, ("core", "kv"), plane).reshape(2, kv, half, features)
+        exchange(activated, "z", turned(z, ACTIVE_AT)), own, partner, residual, head_width + 2 * units, kv
+    )
+    total = exchange(total, ("core", "kv"), back).reshape(2, kv, half, features)
+    total = total if RETURN_SIDES[0] == 0 else total[::-1]
     return jnp.sum(total, axis=1).reshape(own_rows, features).astype(jnp.bfloat16)
 
 

time: 117 us -> 116 us (level)
  no operation moved by 1% of the time
where the time goes in v8:
time: 116 us
  blocking collectives  84.1 us (72%)
  starting transfers between devices  21.5 us (19%)
  Pallas kernels  4.98 us (4%)
  waiting for transfers between devices  3.33 us (3%)
    all_to_all x6, blocking collectives, exchange(): lax.all_to_all(parts, axes, split_axis=0, concat_axis=0, axis_index_group...  84.1 us
    all_to_all x1, starting transfers between devices, exchange(): lax.all_to_all(parts, axes, split_axis=0, concat_axis=0, axis_index_group...  10.9 us
    ppermute x2, starting transfers between devices, from_partner(): return lax.ppermute(value, 'core', [(0, 1), (1, 0)])  10.7 us
    all_to_all x1, waiting for transfers between devices, exchange(): lax.all_to_all(parts, axes, split_axis=0, concat_axis=0, axis_index_group...  3.33 us
    pallas_call x6, Pallas kernels, call(): pl.pallas_call(kernel, out_shape=out_shape, in_specs=[IN_VMEM] * len(oper...  2.53 us
  transfers between devices with their start and end apart: 3, of which 1 were waited for; matrix products, arithmetic and copies ran while one was open for 0% of the time, Pallas kernels for 2%

profile of v8, /device:TPU:1, one launch (start us, length us, event | category | flops | bytes accessed | tf_op | source)
XLA Modules:
  0.0 115.9 jit_solution(10348075384028386277)
XLA Ops:
  0.0 0.0 copy-start
  0.0 1.2 %opening.1 = (bf16[32,2,128]{2,1,0:T(2,128)(2,1)S(1)}, bf16[144,1536]{1,0:T(8,128)(2,1)S(1)}) custom-call(bf16[4,128]{1,0:T(4,128)(2,1)} %hidden.1, f32[1,128]{1,0:T(1,128)} %bitcast.13, bf16[128,256]{1,0:T(8,128)(2,1)} %refs_0_.2, bf16[128,256]{1,0:T(8,128)(2,1)} %refs_1_.1, bf16[128,512]{1,0:T(8,128)(2,1)} %refs_2_.1, bf16[128,512]{1,0:T(8,128)(2,1)} %refs_3_.2), custom_call_target="tpu_custom_call" | custom-call | flops 2000000 | bytes 1000000 | tf_op jit(solution)/shard_map/opening/pallas_call | solution.py:106
  1.2 8.7 %collective-permute-start = (bf16[144,1536]{1,0:T(8,128)(2,1)S(1)}, bf16[144,1536]{1,0:T(8,128)(2,1)S(1)}, u32[]{:S(2)}, u32[]{:S(2)}) collective-permute-start(bf16[144,1536]{1,0:T(8,128)(2,1)S(1)} %get-tuple-element.14.own), channel_id=1, source_target_pairs={{0,1},{1,0},{2,3},{3,2},{4,5},{5,4},{6,7},{7,6},{8,9},{9,8},{10,11... | collective-permute-start | bytes 1327112 | tf_op jit(solution)/shard_map/ppermute | solution.py:33
  10.6 1.2 %later.1 = (bf16[2640,128]{1,0:T(8,128)(2,1)S(1)}, f32[8,128]{1,0:T(8,128)S(1)}) custom-call(f32[1]{0:T(128)S(6)} %copy.18.decay, f32[1,128]{1,0:T(1,128)S(1)} %multiply_power_fusion.inverse, s32[2]{0:T(128)} %lengths.1, f32[1,128]{1,0:T(1,128)} %bitcast.14, bf16[512,128]{1,0:T(8,128)(2,1)} %refs_0_.3, bf16[704,128]{1,0:T(8,128)(2,1)} %bitcast.11, ...), custom_call_target="tpu_custom_call" | custom-call | flops 2000000 | bytes 1000000 | tf_op jit(solution)/shard_map/later/pallas_call | solution.py:157
  11.9 1.9 %collective-permute-start.1 = (bf16[2640,128]{1,0:T(8,128)(2,1)S(1)}, bf16[2640,128]{1,0:T(8,128)(2,1)S(1)}, u32[]{:S(2)}, u32[]{:S(2)}) collective-permute-start(bf16[2640,128]{1,0:T(8,128)(2,1)S(1)} %get-tuple-element.17.own.own_weights), channel_id=1, source_target_pairs={{0,1},{1,0},{2,3},{3,2},{4,5},{5,4},{6,7},{7,6},{8,9},{9,8},{10,11... | collective-permute-start | bytes 2027528 | tf_op jit(solution)/shard_map/ppermute | solution.py:33
  13.8 9.1 %all_to_all.35 = bf16[32,2,128]{2,1,0:T(2,128)(2,1)S(1)} all-to-all(bf16[32,2,128]{2,1,0:T(2,128)(2,1)S(1)} %get-tuple-element.13), channel_id=1, replica_groups={{321,353,385,417,449,481,1,33,65,97,129,161,193,225,257,289,320,352,384..., dimensions={0} | all-to-all | bytes 32768 | tf_op jit(solution)/shard_map/all_to_all | solution.py:23
  22.9 0.0 collective-permute-done.partner
  22.9 0.0 copy-start.1
  22.9 0.3 shard_map.163
  23.2 0.0 copy-start.2
  23.2 19.6 %all_to_all.36.arrived = bf16[16,2,1664]{2,1,0:T(2,128)(2,1)S(1)} all-to-all(bf16[16,2,1664]{2,1,0:T(2,128)(2,1)S(1)} %get-tuple-element.15), channel_id=1, replica_groups={{18,20,22,24,26,28,30,0,2,4,6,8,10,12,14,16},{19,21,23,25,27,29,31,1,3,..., dimensions={0} | all-to-all | bytes 212992 | tf_op jit(solution)/shard_map/all_to_all | solution.py:23
  42.8 0.0 copy-start.3
  42.8 0.0 copy-done
  42.8 0.0 copy-done.1
  42.8 0.0 copy-done.2
  42.8 0.7 copy-done.3
  43.5 1.3 %shard_map.164 = bf16[16,2,512]{2,1,0:T(2,128)(2,1)} custom-call(bf16[16,2,1664]{2,1,0:T(2,128)(2,1)S(1)} %all_to_all.36.arrived, f32[8,128]{1,0:T(8,128)S(1)} %get-tuple-element.16.table, f32[2,1,256,512]{3,2,1,0:T(8,128)S(1)} %copy-done, bf16[2,1,128,256]{3,2,1,0:T(8,128)(2,1)S(1)} %copy-done.2, bf16[2,1,128,512]{3,2,1,0:T(8,128)(2,1)S(1)} %copy-done.1, ...), custom_call_target="tpu_custom_call" | custom-call | flops 8000000 | bytes 1000000 | tf_op jit(solution)/shard_map/pallas_call | solution.py:294
  44.8 10.9 %all-to-all-start.2 = ((bf16[16,2,512]{2,1,0:T(2,128)(2,1)}), bf16[16,2,512]{2,1,0:T(2,128)(2,1)S(1)}, u32[]{:S(2)}, u32[]{:S(2)}) async-start(bf16[16,2,512]{2,1,0:T(2,128)(2,1)} %shard_map.164), calls=%async_computation.2 | async-start | bytes 65536 | tf_op jit(solution)/shard_map/all_to_all | solution.py:23
  55.6 0.0 collective-permute-done.1.partner
  55.6 3.3 %all-to-all-done.2.arrived = bf16[16,2,512]{2,1,0:T(2,128)(2,1)S(1)} async-done(((bf16[16,2,512]{2,1,0:T(2,128)(2,1)}), bf16[16,2,512]{2,1,0:T(2,128)(2,1)S(1)}, u32[]{:S(2)}, u32[]{:S(2)}) %all-to-all-start.2) | async-done | bytes 32800 | tf_op jit(solution)/shard_map/all_to_all | solution.py:23
  59.0 0.2 shard_map.165
  59.1 10.5 %all_to_all.37.parts = bf16[16,32,256]{2,1,0:T(8,128)(2,1)S(1)} all-to-all(bf16[16,32,256]{2,1,0:T(8,128)(2,1)S(1)} %shard_map.165), channel_id=1, replica_groups={{320,352,384,416,448,480,0,32,64,96,128,160,192,224,256,288},{321,353,3..., dimensions={0} | all-to-all | bytes 524288 | tf_op jit(solution)/shard_map/all_to_all | solution.py:23
  69.6 0.4 shard_map.166
  70.0 15.2 %all_to_all.38.arrived = bf16[16,2,1472]{2,1,0:T(2,128)(2,1)S(1)} all-to-all(bf16[16,2,1472]{2,1,0:T(2,128)(2,1)S(1)} %get-tuple-element.19), channel_id=1, replica_groups={{18,20,22,24,26,28,30,0,2,4,6,8,10,12,14,16},{19,21,23,25,27,29,31,1,3,..., dimensions={0} | all-to-all | bytes 188416 | tf_op jit(solution)/shard_map/all_to_all | solution.py:23
  85.3 0.2 shard_map.167
  85.4 14.0 %all_to_all.39.arrived = bf16[16,2,704]{2,1,0:T(2,128)(2,1)S(1)} all-to-all(bf16[16,2,704]{2,1,0:T(2,128)(2,1)S(1)} %shard_map.167), channel_id=1, replica_groups={{18,20,22,24,26,28,30,0,2,4,6,8,10,12,14,16},{19,21,23,25,27,29,31,1,3,..., dimensions={0} | all-to-all | bytes 90112 | tf_op jit(solution)/shard_map/all_to_all | solution.py:23
  99.5 0.2 shard_map.168
  99.7 15.7 %all_to_all.40 = f32[32,2,128]{2,1,0:T(2,128)S(1)} all-to-all(f32[32,2,128]{2,1,0:T(2,128)S(1)} %shard_map.168), channel_id=1, replica_groups={{320,352,384,416,448,480,0,32,64,96,128,160,192,224,256,288,321,353,385..., dimensions={0} | all-to-all | bytes 65536 | tf_op jit(solution)/shard_map/all_to_all | solution.py:23
  115.4 0.6 bitcast_reduce_fusion
  (1 shorter events, 0.0 us)
Async XLA Ops:
  0.0 42.8 %copy-start = (f32[2,1,256,512]{3,2,1,0:T(8,128)S(1)}, f32[2,1,256,512]{3,2,1,0:T(8,128)}, u32[]{:S(2)}) copy-start(f32[2,1,256,512]{3,2,1,0:T(8,128)} %state.1) | copy-start | bytes 3145732
  1.2 21.7 %collective-permute-start = (bf16[144,1536]{1,0:T(8,128)(2,1)S(1)}, bf16[144,1536]{1,0:T(8,128)(2,1)S(1)}, u32[]{:S(2)}, u32[]{:S(2)}) collective-permute-start(bf16[144,1536]{1,0:T(8,128)(2,1)S(1)} %get-tuple-element.14.own), channel_id=1, source_target_pairs={{0,1},{1,0},{2,3},{3,2},{4,5},{5,4},{6,7},{7,6},{8,9},{9,8},{10,11... | collective-permute-start | bytes 1327112 | tf_op jit(solution)/shard_map/ppermute | solution.py:33
  11.9 43.7 %collective-permute-start.1 = (bf16[2640,128]{1,0:T(8,128)(2,1)S(1)}, bf16[2640,128]{1,0:T(8,128)(2,1)S(1)}, u32[]{:S(2)}, u32[]{:S(2)}) collective-permute-start(bf16[2640,128]{1,0:T(8,128)(2,1)S(1)} %get-tuple-element.17.own.own_weights), channel_id=1, source_target_pairs={{0,1},{1,0},{2,3},{3,2},{4,5},{5,4},{6,7},{7,6},{8,9},{9,8},{10,11... | collective-permute-start | bytes 2027528 | tf_op jit(solution)/shard_map/ppermute | solution.py:33
  22.9 19.9 %copy-start.1 = (bf16[2,1,128,512]{3,2,1,0:T(8,128)(2,1)S(1)}, bf16[2,1,128,512]{3,2,1,0:T(8,128)(2,1)}, u32[]{:S(2)}) copy-start(bf16[2,1,128,512]{3,2,1,0:T(8,128)(2,1)} %values.1) | copy-start | bytes 786436
  23.2 19.6 %copy-start.2 = (bf16[2,1,128,256]{3,2,1,0:T(8,128)(2,1)S(1)}, bf16[2,1,128,256]{3,2,1,0:T(8,128)(2,1)}, u32[]{:S(2)}) copy-start(bf16[2,1,128,256]{3,2,1,0:T(8,128)(2,1)} %keys.1) | copy-start | bytes 393220
  42.8 0.7 copy-start.3
  44.8 14.2 %all-to-all-start.2 = ((bf16[16,2,512]{2,1,0:T(2,128)(2,1)}), bf16[16,2,512]{2,1,0:T(2,128)(2,1)S(1)}, u32[]{:S(2)}, u32[]{:S(2)}) async-start(bf16[16,2,512]{2,1,0:T(2,128)(2,1)} %shard_map.164), calls=%async_computation.2 | async-start | bytes 65536 | tf_op jit(solution)/shard_map/all_to_all | solution.py:23

commit v9 on v8

--- a/solution.py
+++ b/solution.py
@@ -77,8 +77,9 @@
     pairs, at = [(hidden, rows), (gain, own_gain)], 0
     for source in sources:
         depth, columns = source.shape
-        pairs.append((source, joined.at[:depth, at : at + columns]))
-        at += columns
+        for lane in range(0, columns, LANES):
+            pairs.append((source.at[:, lane : lane + LANES], joined.at[at : at + depth]))
+            at += depth
     moves = started(pairs, arrived)
     moves[0].wait()
     peers, half, _ = many.shape
@@ -101,7 +102,8 @@
 
 def opening(hidden, gain, weights, peers):
     many = (peers, hidden.shape[0] // 2, LANES)
-    joined = (LANES + GAIN_ROWS, sum(array.shape[1] for array in weights))
+    joined = (sum(array.size for array in weights) // LANES + GAIN_ROWS, LANES)
+    pieces = sum(array.shape[1] for array in weights) // LANES
     operands = held_in_hbm(hidden, gain[None], *weights)
     return pl.pallas_call(
         open_kernel,
@@ -115,7 +117,7 @@
             pltpu.VMEM(hidden.shape, jnp.bfloat16),
             pltpu.VMEM((1, LANES), jnp.float32),
             pltpu.VMEM(many, jnp.bfloat16),
-            pltpu.SemaphoreType.DMA((len(operands) + 1,)),
+            pltpu.SemaphoreType.DMA((pieces + 3,)),
         ],
         compiler_params=pltpu.CompilerParams(vmem_limit_bytes=8 << 20),
         cost_estimate=pl.CostEstimate(flops=2_000_000, bytes_accessed=1_000_000, transcendentals=0),
@@ -278,12 +280,17 @@
         stream[0, span] = arrived[place, source].astype(jnp.float32)
         stream[1, span] = arrived[1 - place, source].astype(jnp.float32)
     parts = [stream[i] for i in range(2)]
-    total = None
-    for part, weights in zip(parts, (own, partner)):
-        gain = from_thirds(weights[features : features + GAIN_ROWS, :features])
-        term = wide_dot((part * gain).astype(jnp.bfloat16), weights[:features])
-        total = term if total is None else total + term
-    wide[:, :width] = total
+    scaled = jnp.concatenate(
+        [
+            (part * from_thirds(weights[weights.shape[0] - GAIN_ROWS :])).astype(jnp.bfloat16)
+            for part, weights in zip(parts, (own, partner))
+        ],
+        axis=1,
+    )
+    for i in range(width // LANES):
+        span = slice(features * i, features * (i + 1))
+        columns = jnp.concatenate([own[span], partner[span]], axis=0)
+        wide[:, LANES * i : LANES * (i + 1)] = wide_dot(scaled, columns)
     squares = jnp.sum(parts[0] * parts[0] + parts[1] * parts[1], axis=1, keepdims=True)
     lane = lax.broadcasted_iota(jnp.int32, (rows, LANES), 1)
     wide[:, width:] = jnp.where(lane == 0, squares, 0.0)
@@ -305,7 +312,7 @@
 def project(arrived, own, partner, z):
     _, kv, half, features = arrived.shape
     rows = kv * half
-    width = own.shape[1] + LANES
+    width = (own.shape[0] - GAIN_ROWS) * LANES // features + LANES
     out_shape = (
         jax.ShapeDtypeStruct((z, rows // z, width), jnp.bfloat16),
         jax.ShapeDtypeStruct((2, rows, features), jnp.float32),

time: 116 us -> 116 us (level)
  no operation moved by 1% of the time
where the time goes in v9:
time: 116 us
  blocking collectives  84.1 us (72%)
  starting transfers between devices  21.5 us (19%)
  Pallas kernels  4.95 us (4%)
  waiting for transfers between devices  3.33 us (3%)
    all_to_all x6, blocking collectives, exchange(): lax.all_to_all(parts, axes, split_axis=0, concat_axis=0, axis_index_group...  84.1 us
    all_to_all x1, starting transfers between devices, exchange(): lax.all_to_all(parts, axes, split_axis=0, concat_axis=0, axis_index_group...  10.9 us
    ppermute x2, starting transfers between devices, from_partner(): return lax.ppermute(value, 'core', [(0, 1), (1, 0)])  10.7 us
    all_to_all x1, waiting for transfers between devices, exchange(): lax.all_to_all(parts, axes, split_axis=0, concat_axis=0, axis_index_group...  3.33 us
    pallas_call x6, Pallas kernels, call(): pl.pallas_call(kernel, out_shape=out_shape, in_specs=[IN_VMEM] * len(oper...  2.53 us
  transfers between devices with their start and end apart: 3, of which 1 were waited for; matrix products, arithmetic and copies ran while one was open for 0% of the time, Pallas kernels for 2%

profile of v9, /device:TPU:1, one launch (start us, length us, event | category | flops | bytes accessed | tf_op | source)
XLA Modules:
  0.0 115.9 jit_solution(11235514482044936266)
XLA Ops:
  0.0 0.0 copy-start
  0.0 1.2 %opening.1 = (bf16[32,2,128]{2,1,0:T(2,128)(2,1)S(1)}, bf16[1552,128]{1,0:T(8,128)(2,1)S(1)}) custom-call(bf16[4,128]{1,0:T(4,128)(2,1)} %hidden.1, f32[1,128]{1,0:T(1,128)} %bitcast.13, bf16[128,256]{1,0:T(8,128)(2,1)} %refs_0_.2, bf16[128,256]{1,0:T(8,128)(2,1)} %refs_1_.1, bf16[128,512]{1,0:T(8,128)(2,1)} %refs_2_.1, bf16[128,512]{1,0:T(8,128)(2,1)} %refs_3_.2), custom_call_target="tpu_custom_call" | custom-call | flops 2000000 | bytes 1000000 | tf_op jit(solution)/shard_map/opening/pallas_call | solution.py:108
  1.2 8.7 %collective-permute-start = (bf16[1552,128]{1,0:T(8,128)(2,1)S(1)}, bf16[1552,128]{1,0:T(8,128)(2,1)S(1)}, u32[]{:S(2)}, u32[]{:S(2)}) collective-permute-start(bf16[1552,128]{1,0:T(8,128)(2,1)S(1)} %get-tuple-element.14.own), channel_id=1, source_target_pairs={{0,1},{1,0},{2,3},{3,2},{4,5},{5,4},{6,7},{7,6},{8,9},{9,8},{10,11... | collective-permute-start | bytes 1191944 | tf_op jit(solution)/shard_map/ppermute | solution.py:33
  10.6 1.2 %later.1 = (bf16[2640,128]{1,0:T(8,128)(2,1)S(1)}, f32[8,128]{1,0:T(8,128)S(1)}) custom-call(f32[1]{0:T(128)S(6)} %copy.18.decay, f32[1,128]{1,0:T(1,128)S(1)} %multiply_power_fusion.inverse, s32[2]{0:T(128)} %lengths.1, f32[1,128]{1,0:T(1,128)} %bitcast.14, bf16[512,128]{1,0:T(8,128)(2,1)} %refs_0_.3, bf16[704,128]{1,0:T(8,128)(2,1)} %bitcast.11, ...), custom_call_target="tpu_custom_call" | custom-call | flops 2000000 | bytes 1000000 | tf_op jit(solution)/shard_map/later/pallas_call | solution.py:159
  11.9 1.9 %collective-permute-start.1 = (bf16[2640,128]{1,0:T(8,128)(2,1)S(1)}, bf16[2640,128]{1,0:T(8,128)(2,1)S(1)}, u32[]{:S(2)}, u32[]{:S(2)}) collective-permute-start(bf16[2640,128]{1,0:T(8,128)(2,1)S(1)} %get-tuple-element.17.own.own_weights), channel_id=1, source_target_pairs={{0,1},{1,0},{2,3},{3,2},{4,5},{5,4},{6,7},{7,6},{8,9},{9,8},{10,11... | collective-permute-start | bytes 2027528 | tf_op jit(solution)/shard_map/ppermute | solution.py:33
  13.8 9.1 %all_to_all.35 = bf16[32,2,128]{2,1,0:T(2,128)(2,1)S(1)} all-to-all(bf16[32,2,128]{2,1,0:T(2,128)(2,1)S(1)} %get-tuple-element.13), channel_id=1, replica_groups={{321,353,385,417,449,481,1,33,65,97,129,161,193,225,257,289,320,352,384..., dimensions={0} | all-to-all | bytes 32768 | tf_op jit(solution)/shard_map/all_to_all | solution.py:23
  22.9 0.0 collective-permute-done.partner
  22.9 0.0 copy-start.1
  22.9 0.3 shard_map.163
  23.1 0.0 copy-start.2
  23.1 19.6 %all_to_all.36.arrived = bf16[16,2,1664]{2,1,0:T(2,128)(2,1)S(1)} all-to-all(bf16[16,2,1664]{2,1,0:T(2,128)(2,1)S(1)} %get-tuple-element.15), channel_id=1, replica_groups={{18,20,22,24,26,28,30,0,2,4,6,8,10,12,14,16},{19,21,23,25,27,29,31,1,3,..., dimensions={0} | all-to-all | bytes 212992 | tf_op jit(solution)/shard_map/all_to_all | solution.py:23
  42.7 0.0 copy-start.3
  42.7 0.0 copy-done
  42.8 0.0 copy-done.1
  42.8 0.0 copy-done.2
  42.8 0.7 copy-done.3
  43.4 1.3 %shard_map.164 = bf16[16,2,512]{2,1,0:T(2,128)(2,1)} custom-call(bf16[16,2,1664]{2,1,0:T(2,128)(2,1)S(1)} %all_to_all.36.arrived, f32[8,128]{1,0:T(8,128)S(1)} %get-tuple-element.16.table, f32[2,1,256,512]{3,2,1,0:T(8,128)S(1)} %copy-done, bf16[2,1,128,256]{3,2,1,0:T(8,128)(2,1)S(1)} %copy-done.2, bf16[2,1,128,512]{3,2,1,0:T(8,128)(2,1)S(1)} %copy-done.1, ...), custom_call_target="tpu_custom_call" | custom-call | flops 8000000 | bytes 1000000 | tf_op jit(solution)/shard_map/pallas_call | solution.py:301
  44.7 10.9 %all-to-all-start.2 = ((bf16[16,2,512]{2,1,0:T(2,128)(2,1)}), bf16[16,2,512]{2,1,0:T(2,128)(2,1)S(1)}, u32[]{:S(2)}, u32[]{:S(2)}) async-start(bf16[16,2,512]{2,1,0:T(2,128)(2,1)} %shard_map.164), calls=%async_computation.2 | async-start | bytes 65536 | tf_op jit(solution)/shard_map/all_to_all | solution.py:23
  55.6 0.0 collective-permute-done.1.partner
  55.6 3.3 %all-to-all-done.2.arrived = bf16[16,2,512]{2,1,0:T(2,128)(2,1)S(1)} async-done(((bf16[16,2,512]{2,1,0:T(2,128)(2,1)}), bf16[16,2,512]{2,1,0:T(2,128)(2,1)S(1)}, u32[]{:S(2)}, u32[]{:S(2)}) %all-to-all-start.2) | async-done | bytes 32800 | tf_op jit(solution)/shard_map/all_to_all | solution.py:23
  58.9 0.2 shard_map.165
  59.1 10.5 %all_to_all.37.parts = bf16[16,32,256]{2,1,0:T(8,128)(2,1)S(1)} all-to-all(bf16[16,32,256]{2,1,0:T(8,128)(2,1)S(1)} %shard_map.165), channel_id=1, replica_groups={{320,352,384,416,448,480,0,32,64,96,128,160,192,224,256,288},{321,353,3..., dimensions={0} | all-to-all | bytes 524288 | tf_op jit(solution)/shard_map/all_to_all | solution.py:23
  69.6 0.4 shard_map.166
  70.0 15.2 %all_to_all.38.arrived = bf16[16,2,1472]{2,1,0:T(2,128)(2,1)S(1)} all-to-all(bf16[16,2,1472]{2,1,0:T(2,128)(2,1)S(1)} %get-tuple-element.19), channel_id=1, replica_groups={{18,20,22,24,26,28,30,0,2,4,6,8,10,12,14,16},{19,21,23,25,27,29,31,1,3,..., dimensions={0} | all-to-all | bytes 188416 | tf_op jit(solution)/shard_map/all_to_all | solution.py:23
  85.2 0.2 shard_map.167
  85.4 14.0 %all_to_all.39.arrived = bf16[16,2,704]{2,1,0:T(2,128)(2,1)S(1)} all-to-all(bf16[16,2,704]{2,1,0:T(2,128)(2,1)S(1)} %shard_map.167), channel_id=1, replica_groups={{18,20,22,24,26,28,30,0,2,4,6,8,10,12,14,16},{19,21,23,25,27,29,31,1,3,..., dimensions={0} | all-to-all | bytes 90112 | tf_op jit(solution)/shard_map/all_to_all | solution.py:23
  99.5 0.2 shard_map.168
  99.7 15.7 %all_to_all.40 = f32[32,2,128]{2,1,0:T(2,128)S(1)} all-to-all(f32[32,2,128]{2,1,0:T(2,128)S(1)} %shard_map.168), channel_id=1, replica_groups={{320,352,384,416,448,480,0,32,64,96,128,160,192,224,256,288,321,353,385..., dimensions={0} | all-to-all | bytes 65536 | tf_op jit(solution)/shard_map/all_to_all | solution.py:23
  115.3 0.6 bitcast_reduce_fusion
  (1 shorter events, 0.0 us)
Async XLA Ops:
  0.0 42.7 %copy-start = (f32[2,1,256,512]{3,2,1,0:T(8,128)S(1)}, f32[2,1,256,512]{3,2,1,0:T(8,128)}, u32[]{:S(2)}) copy-start(f32[2,1,256,512]{3,2,1,0:T(8,128)} %state.1) | copy-start | bytes 3145732
  1.2 21.7 %collective-permute-start = (bf16[1552,128]{1,0:T(8,128)(2,1)S(1)}, bf16[1552,128]{1,0:T(8,128)(2,1)S(1)}, u32[]{:S(2)}, u32[]{:S(2)}) collective-permute-start(bf16[1552,128]{1,0:T(8,128)(2,1)S(1)} %get-tuple-element.14.own), channel_id=1, source_target_pairs={{0,1},{1,0},{2,3},{3,2},{4,5},{5,4},{6,7},{7,6},{8,9},{9,8},{10,11... | collective-permute-start | bytes 1191944 | tf_op jit(solution)/shard_map/ppermute | solution.py:33
  11.9 43.7 %collective-permute-start.1 = (bf16[2640,128]{1,0:T(8,128)(2,1)S(1)}, bf16[2640,128]{1,0:T(8,128)(2,1)S(1)}, u32[]{:S(2)}, u32[]{:S(2)}) collective-permute-start(bf16[2640,128]{1,0:T(8,128)(2,1)S(1)} %get-tuple-element.17.own.own_weights), channel_id=1, source_target_pairs={{0,1},{1,0},{2,3},{3,2},{4,5},{5,4},{6,7},{7,6},{8,9},{9,8},{10,11... | collective-permute-start | bytes 2027528 | tf_op jit(solution)/shard_map/ppermute | solution.py:33
  22.9 19.9 %copy-start.1 = (bf16[2,1,128,512]{3,2,1,0:T(8,128)(2,1)S(1)}, bf16[2,1,128,512]{3,2,1,0:T(8,128)(2,1)}, u32[]{:S(2)}) copy-start(bf16[2,1,128,512]{3,2,1,0:T(8,128)(2,1)} %values.1) | copy-start | bytes 786436
  23.1 19.6 %copy-start.2 = (bf16[2,1,128,256]{3,2,1,0:T(8,128)(2,1)S(1)}, bf16[2,1,128,256]{3,2,1,0:T(8,128)(2,1)}, u32[]{:S(2)}) copy-start(bf16[2,1,128,256]{3,2,1,0:T(8,128)(2,1)} %keys.1) | copy-start | bytes 393220
  42.7 0.7 copy-start.3
  44.7 14.2 %all-to-all-start.2 = ((bf16[16,2,512]{2,1,0:T(2,128)(2,1)}), bf16[16,2,512]{2,1,0:T(2,128)(2,1)S(1)}, u32[]{:S(2)}, u32[]{:S(2)}) async-start(bf16[16,2,512]{2,1,0:T(2,128)(2,1)} %shard_map.164), calls=%async_computation.2 | async-start | bytes 65536 | tf_op jit(solution)/shard_map/all_to_all | solution.py:23
